TPU v7x, 256 devices: a whole 4x4x8 slice. The times are simulated.
256 devices in a mesh: gr: 2 (over z_hi), fs: 16 (over z_lo, y), tp: 8 (over x, core).
Axes of the slice: x: 4, y: 4, z: 8 (z_hi: 2, z_lo: 4; z = z_hi * 4 + z_lo), core: 2. Of those that a mesh axis runs over, the one named last changes fastest.
Arguments:
- tokens: bfloat16 [32768, 2048], P(('gr', 'fs', 'tp')), may hold values from -6 to 6
- routes: int32 [32768, 8], P(('gr', 'fs', 'tp')), may hold values from 0 to 127, all different within a row; in each aligned block of 128 rows (0 to 127, 128 to 255, ...) at most 12 rows name the same one
- route_weights: float32 [32768, 8], P(('gr', 'fs', 'tp')), may hold values from 0.1 to 0.6
- norm_gain: float32 [2048], P(('gr', 'tp')), may hold values from 0.1 to 1.9
- gate_trained: float32 [128, 384, 2048], P(None, 'fs', ('gr', 'tp')), may hold values from -0.125 to 0.125
- up_trained: float32 [128, 384, 2048], P(None, 'fs', ('gr', 'tp')), may hold values from -0.125 to 0.125
- down_trained: float32 [128, 384, 2048], P(None, 'fs', ('gr', 'tp')), may hold values from -0.3125 to 0.3125
- shared_gate_trained: float32 [512, 2048], P('fs', ('gr', 'tp')), may hold values from -0.125 to 0.125
- shared_up_trained: float32 [512, 2048], P('fs', ('gr', 'tp')), may hold values from -0.125 to 0.125
- shared_down_trained: float32 [512, 2048], P('fs', ('gr', 'tp')), may hold values from -0.25 to 0.25
Outputs:
- combined: bfloat16 [32768, 2048], P(('gr', 'fs', 'tp'))
- expert_gate: bfloat16 [128, 384, 2048], P(('fs', 'tp'))
- expert_up: bfloat16 [128, 384, 2048], P(('fs', 'tp'))
- expert_down: bfloat16 [128, 384, 2048], P(('fs', 'tp'))
- shared_gate: bfloat16 [512, 2048], P('fs')
- shared_up: bfloat16 [512, 2048], P('fs')
- shared_down: bfloat16 [512, 2048], P('fs')
Inputs may be any that keep to these rules, and one draw needn't show every extreme that they name: `routes`: each row names 8 different experts. Among the rows of one device no expert is named more than 12 times, and that many is reached in every draw.
All inputs are finite; a program needn't handle non-finite values.
Results may differ from a plain program's by a relative error of at most 0.0084.
Values may be sent and summed in bfloat16 or wider, within the bound.
No kernel may reach another device: no remote copies, remote signals or barrier semaphores. Data moves between devices by JAX's collectives and lax.ppermute only.
A program may use at most 128 MiB of HBM per device.

v0:
```python
import functools

import jax
import jax.numpy as jnp
from jax import lax
from jax.experimental import pallas as pl
from jax.experimental.pallas import tpu as pltpu
from jax.sharding import Mesh, PartitionSpec as P


epsilon = 1e-06
ALL = ("gr", "zl", "y", "x", "c")
PLANE = ("y", "x", "c")
bf16 = jnp.bfloat16
f32 = jnp.float32


def swapped(array, axis, size, k):
    return lax.ppermute(array, axis, [(r, r ^ k) for r in range(size)])


def plane_exchange(array):
    return lax.all_to_all(array, PLANE, split_axis=0, concat_axis=0, tiled=True)


def ffn_rows(x, gate, up, down):
    contract = (((1,), (1,)), ((), ()))
    g = lax.dot_general(x, gate, contract, preferred_element_type=f32)
    u = lax.dot_general(x, up, contract, preferred_element_type=f32)
    hidden = (jax.nn.silu(g) * u).astype(bf16)
    return jnp.dot(hidden, down, preferred_element_type=f32)


def cast_kernel(place, gain, gate, up, down, out):
    n = gate.shape[1]
    scale = gain[...][None]
    out[:, :n, :] = (gate[...] * scale).astype(bf16)
    out[:, n : 2 * n, :] = (up[...] * scale).astype(bf16)
    out[:, 2 * n :, :] = down[...].astype(bf16)


def cast(place, gain, gate, up, down, n_plane):
    experts, n, cols = gate.shape
    n_zl = experts // n_plane
    piece = pl.BlockSpec((n_plane, n, cols), lambda j, p: (p[0] ^ j, 0, 0))
    spec = pltpu.PrefetchScalarGridSpec(
        num_scalar_prefetch=1,
        grid=(n_zl,),
        in_specs=[pl.BlockSpec((1, cols), lambda j, p: (0, 0)), piece, piece, piece],
        out_specs=pl.BlockSpec((n_plane, 3 * n, cols), lambda j, p: (0, j, 0)),
    )
    return pl.pallas_call(
        cast_kernel,
        grid_spec=spec,
        out_shape=jax.ShapeDtypeStruct((n_plane, n_zl * 3 * n, cols), bf16),
        cost_estimate=pl.CostEstimate(
            flops=3 * gate.size, bytes_accessed=18 * gate.size, transcendentals=0
        ),
        name="cast",
    )(place, gain, gate, up, down)


def ffn_assemble_kernel(place, x, *refs, blocks, n_y, n_xc, own_hidden, cols):
    parts, refs = refs[:blocks], refs[blocks:]
    out, outs, held, sems = refs[0], refs[1:4], refs[4:7], refs[7]
    step = pl.program_id(0)
    n_cols = held[0].shape[0]

    def writes():
        return [
            pltpu.make_async_copy(
                held[m].at[f],
                outs[m].at[0, :, pl.ds(f * cols, cols)],
                sems.at[blocks * 3 * n_y + m * n_cols + f],
            )
            for m in range(3)
            for f in range(n_cols)
        ]

    @pl.when(step == 0)
    def _():
        reads = []
        for k in range(blocks):
            row = place[2 * k] * (n_y * own_hidden)
            col = place[2 * k + 1] * n_xc
            for m in range(3):
                for y in range(n_y):
                    at = pl.multiple_of(row + y * own_hidden, 8)
                    reads.append(
                        pltpu.make_async_copy(
                            parts[k].at[pl.ds(y * n_xc, n_xc), pl.ds(m * own_hidden, own_hidden)],
                            held[m].at[pl.ds(col, n_xc), pl.ds(at, own_hidden)],
                            sems.at[(k * 3 + m) * n_y + y],
                        )
                    )
        for r in reads:
            r.start()
        for r in reads:
            r.wait()
        for w in writes():
            w.start()

    gate, up, down = (
        jnp.concatenate([held[m][f] for f in range(n_cols)], axis=1) for m in range(3)
    )
    out[...] = ffn_rows(x[...], gate, up, down).astype(bf16)

    @pl.when(step == pl.num_programs(0) - 1)
    def _():
        for w in writes():
            w.wait()


def ffn_assemble(place, x, parts, n_y, n_xc, own_hidden, tile):
    count, features = x.shape
    cols = parts[0].shape[2]
    n_cols = features // cols
    hidden = len(parts) * n_y * n_xc * own_hidden * cols // features
    matrix = jax.ShapeDtypeStruct((1, hidden, features), bf16)
    hbm = pl.BlockSpec(memory_space=pl.ANY)
    spec = pltpu.PrefetchScalarGridSpec(
        num_scalar_prefetch=1,
        grid=(count // tile,),
        in_specs=[pl.BlockSpec((tile, features), lambda i, p: (i, 0))] + [hbm] * len(parts),
        out_specs=[pl.BlockSpec((tile, features), lambda i, p: (i, 0))] + [hbm] * 3,
        scratch_shapes=[pltpu.VMEM((n_cols, hidden, cols), bf16)] * 3
        + [pltpu.SemaphoreType.DMA((len(parts) * 3 * n_y + 3 * n_cols,))],
    )
    return pl.pallas_call(
        functools.partial(
            ffn_assemble_kernel,
            blocks=len(parts),
            n_y=n_y,
            n_xc=n_xc,
            own_hidden=own_hidden,
            cols=cols,
        ),
        grid_spec=spec,
        out_shape=[jax.ShapeDtypeStruct((count, features), bf16)] + [matrix] * 3,
        cost_estimate=pl.CostEstimate(
            flops=6 * count * hidden * features,
            bytes_accessed=4 * count * features + 12 * hidden * features,
            transcendentals=count * hidden,
        ),
        name="ffn_assemble",
    )(place, x, *parts)


def ffn_kernel(x, gate, up, down, out):
    out[...] = ffn_rows(x[...], gate[0], up[0], down[0]).astype(bf16)


def ffn(x, gate, up, down, tile):
    count, features = x.shape
    hidden = gate.shape[1]
    whole = pl.BlockSpec((1, hidden, features), lambda i: (0, 0, 0))
    rows = pl.BlockSpec((tile, features), lambda i: (i, 0))
    return pl.pallas_call(
        ffn_kernel,
        grid=(count // tile,),
        in_specs=[rows, whole, whole, whole],
        out_specs=rows,
        out_shape=jax.ShapeDtypeStruct((count, features), bf16),
        cost_estimate=pl.CostEstimate(
            flops=6 * count * hidden * features,
            bytes_accessed=4 * count * features + 6 * hidden * features,
            transcendentals=count * hidden,
        ),
        name="ffn_rows",
    )(x, gate, up, down)


def selection(metas, first, experts, top, capacity):
    codes, weights = [], []
    for k, meta in enumerate(metas):
        names = meta[:top] - first.astype(f32)
        hits = names[:, None, :] == jnp.arange(experts, dtype=f32)[None, :, None]
        chosen = jnp.sum(hits.astype(f32), axis=0)
        weight = jnp.sum(jnp.where(hits, meta[top:, None, :], 0.0), axis=0)
        n = chosen.shape[1]
        before = (jnp.arange(n)[:, None] < jnp.arange(n)[None, :]).astype(bf16)
        place = jnp.dot(chosen.astype(bf16), before, preferred_element_type=f32)
        codes.append(jnp.where(chosen > 0, place + float(k * capacity), -1.0))
        weights.append(weight)
    code = jnp.concatenate(codes, axis=1).astype(bf16)
    weight = jnp.concatenate(weights, axis=1)
    high = weight.astype(bf16)
    low = (weight - high.astype(f32)).astype(bf16)
    span = len(metas) * capacity
    slot = jnp.arange(experts * span, dtype=jnp.int32)
    within = (slot % span).astype(f32)
    spread = (slot[:, None] // span == jnp.arange(experts, dtype=jnp.int32)[None, :]).astype(bf16)

    def by_token(values):
        return lax.dot_general(
            values, spread, (((0,), (1,)), ((), ())), preferred_element_type=f32
        )

    held = by_token(code) == within[None, :]
    high = jnp.where(held, by_token(high), 0.0).astype(bf16)
    low = jnp.where(held, by_token(low), 0.0).astype(bf16)
    return code, high, low


def pick_kernel(code, one, two, out, *, span, tile):
    slot = lax.broadcasted_iota(jnp.int32, (tile, 1), 0) + pl.program_id(0) * tile
    expert = slot // span
    within = (slot - expert * span).astype(f32)
    names = lax.broadcasted_iota(jnp.int32, (tile, code.shape[0]), 1)
    spread = (names == expert).astype(f32).astype(bf16)
    held = jnp.dot(spread, code[...], preferred_element_type=f32) == within
    held = held.astype(f32).astype(bf16)
    n = one.shape[0]
    total = jnp.dot(held[:, :n], one[...], preferred_element_type=f32)
    total += jnp.dot(held[:, n:], two[...], preferred_element_type=f32)
    out[...] = total.astype(bf16)


def pick(code, one, two, span, tile):
    experts, count = code.shape
    features = one.shape[1]
    slots = experts * span
    whole = lambda a: pl.BlockSpec(a.shape, lambda i: (0, 0))
    return pl.pallas_call(
        functools.partial(pick_kernel, span=span, tile=tile),
        grid=(slots // tile,),
        in_specs=[whole(code), whole(one), whole(two)],
        out_specs=pl.BlockSpec((tile, features), lambda i: (i, 0)),
        out_shape=jax.ShapeDtypeStruct((slots, features), bf16),
        cost_estimate=pl.CostEstimate(
            flops=2 * slots * count * features,
            bytes_accessed=2 * (slots + count) * features,
            transcendentals=0,
        ),
        name="pick",
    )(code, one, two)


def combine_kernel(high, low, back, hidden, down, out):
    rows = back[...]
    total = jnp.dot(high[...], rows, preferred_element_type=f32)
    total += jnp.dot(low[...], rows, preferred_element_type=f32)
    total += jnp.dot(hidden[...], down[...], preferred_element_type=f32)
    out[...] = total.astype(out.dtype)


def combine(high, low, back, hidden, down, dtype, tile):
    count, slots = high.shape
    features = back.shape[1]
    units = hidden.shape[1]
    whole = lambda *shape: pl.BlockSpec(shape, lambda i: (0, 0))
    part = lambda rows: pl.BlockSpec((rows, tile), lambda i: (0, i))
    return pl.pallas_call(
        combine_kernel,
        grid=(features // tile,),
        in_specs=[
            whole(count, slots),
            whole(count, slots),
            part(slots),
            whole(count, units),
            part(units),
        ],
        out_specs=part(count),
        out_shape=jax.ShapeDtypeStruct((count, features), dtype),
        cost_estimate=pl.CostEstimate(
            flops=2 * count * features * (2 * slots + units),
            bytes_accessed=4 * count * slots + 2 * slots * features + 4 * count * features,
            transcendentals=0,
        ),
        name="combine",
    )(high, low, back, hidden, down)


def body(
    tokens,
    routes,
    route_weights,
    norm_gain,
    gate_trained,
    up_trained,
    down_trained,
    shared_gate_trained,
    shared_up_trained,
    shared_down_trained,
):
    gr, zl, y = (lax.axis_index(a) for a in ("gr", "zl", "y"))
    n_gr, n_zl, n_y = (lax.axis_size(a) for a in ("gr", "zl", "y"))
    n_xc = lax.axis_size("x") * lax.axis_size("c")
    n_plane = n_y * n_xc
    row_count, features = tokens.shape
    top = routes.shape[1]
    experts, own_hidden, own_cols = gate_trained.shape
    capacity = max(2, 3 * row_count * top // (2 * experts))

    meta = jnp.concatenate([routes.T.astype(f32), route_weights.T], axis=0)
    metas = [meta] + [swapped(meta, "zl", n_zl, k) for k in range(1, n_zl)]
    values = tokens.astype(f32)
    normed = (
        values * lax.rsqrt(jnp.mean(values * values, axis=1, keepdims=True) + epsilon)
    ).astype(bf16)
    blocks = [normed] + [swapped(normed, "zl", n_zl, k) for k in range(1, n_zl)]

    gain = norm_gain[None, :]
    shared = jnp.stack(
        [shared_gate_trained * gain, shared_up_trained * gain, shared_down_trained], axis=0
    ).astype(bf16)
    other = swapped(shared, "gr", n_gr, 1)
    shared = jnp.where(gr == 0, jnp.stack([shared, other]), jnp.stack([other, shared]))

    steps = range(n_gr * n_zl)
    place = jnp.stack([v for k in steps for v in (zl ^ (k % n_zl), gr ^ (k // n_zl))])
    place = place.astype(jnp.int32)
    sent = cast(place, norm_gain[None, :], gate_trained, up_trained, down_trained, n_plane)
    landed = plane_exchange(sent)
    piece = 3 * own_hidden
    moved = [landed[:, j * piece : (j + 1) * piece] for j in range(n_zl)]
    parts = [moved[0]] + [swapped(moved[k % n_zl], ("gr", "zl"), n_gr * n_zl, k) for k in steps[1:]]

    first = zl * n_plane
    near_picks = selection(metas[:2], first, n_plane, top, capacity)
    far_picks = selection(metas[2:], first, n_plane, top, capacity)

    def dispatched(code, rows, after):
        out = pick(code, *rows, 2 * capacity, 256)
        out, _ = lax.optimization_barrier((out, after))
        return plane_exchange(out.reshape(n_plane, 2 * capacity, features))

    near_in = dispatched(near_picks[0], blocks[:2], landed)
    far_in = dispatched(far_picks[0], blocks[2:], near_in)

    share = shared.shape[2]
    extra = jnp.broadcast_to(
        shared.reshape(1, -1, own_cols), (n_plane, shared.size // own_cols, own_cols)
    )
    extra, _ = lax.optimization_barrier((extra, far_in))
    quarter = plane_exchange(extra).reshape(n_y, n_xc, n_gr, 3, share, own_cols)
    quarter = quarter.transpose(3, 0, 4, 2, 1, 5).reshape(3, n_y * share, features)
    shared_out = [
        lax.dynamic_slice_in_dim(quarter[m], y * share, share, axis=0) for m in range(3)
    ]

    def shared_hidden(pair):
        contract = (((1,), (1,)), ((), ()))
        done = []
        for rows in pair:
            g = lax.dot_general(rows, quarter[0], contract, preferred_element_type=f32)
            u = lax.dot_general(rows, quarter[1], contract, preferred_element_type=f32)
            done.append((jax.nn.silu(g) * u).astype(bf16))
        return jnp.concatenate(done, axis=0)

    near_hidden = shared_hidden(blocks[:2])
    far_hidden = shared_hidden(blocks[2:])
    shared_down = quarter[2]
    far_in, near_hidden, far_hidden, shared_down = lax.optimization_barrier(
        (far_in, near_hidden, far_hidden, shared_down)
    )

    far_result, expert_gate, expert_up, expert_down = ffn_assemble(
        place, far_in.reshape(-1, features), parts, n_y, n_xc, own_hidden, 256
    )
    far_back = plane_exchange(far_result.reshape(n_plane, 2 * capacity, features))
    near_result = ffn(near_in.reshape(-1, features), expert_gate, expert_up, expert_down, 256)
    near_back = plane_exchange(near_result.reshape(n_plane, 2 * capacity, features))

    far_sum = combine(
        *far_picks[1:], far_back.reshape(-1, features), far_hidden, shared_down, bf16, 512
    )
    third = swapped(far_sum[:row_count], "zl", n_zl, 2)
    fourth = swapped(far_sum[row_count:], "zl", n_zl, 3)
    near_sum = combine(
        *near_picks[1:], near_back.reshape(-1, features), near_hidden, shared_down, f32, 512
    )
    second = swapped(near_sum[row_count:].astype(bf16), "zl", n_zl, 1)
    combined = (
        near_sum[:row_count] + second.astype(f32) + third.astype(f32) + fourth.astype(f32)
    ).astype(bf16)
    return (combined, expert_gate, expert_up, expert_down, *shared_out)


def solution(mesh):
    fine = Mesh(mesh.devices.reshape(2, 4, 4, 4, 2), ALL)
    cols = ("gr", "x", "c")
    in_specs = (
        P(ALL, None),
        P(ALL, None),
        P(ALL, None),
        P(cols),
        P(None, ("zl", "y"), cols),
        P(None, ("zl", "y"), cols),
        P(None, ("zl", "y"), cols),
        P(("zl", "y"), cols),
        P(("zl", "y"), cols),
        P(("zl", "y"), cols),
    )
    out_specs = (
        P(ALL, None),
        P(("zl", "y", "x", "c"), None, None),
        P(("zl", "y", "x", "c"), None, None),
        P(("zl", "y", "x", "c"), None, None),
        P(("zl", "y"), None),
        P(("zl", "y"), None),
        P(("zl", "y"), None),
    )

    def step(*args):
        return body(*args)

    step = jax.shard_map(step, mesh=fine, in_specs=in_specs, out_specs=out_specs, check_vma=False)
    return step
```

profile of v0, /device:TPU:77, one launch (start us, length us, event | category | flops | bytes accessed | tf_op | source)
XLA Modules:
  0.0 405.5 jit_solution(15352210290810831989)
XLA Ops:
  1.3 5.1 %cast.1 = bf16[32,288,128]{2,1,0:T(8,128)(2,1)} custom-call(s32[16]{0:T(128)} %stack.73.place, f32[1,128]{1,0:T(1,128)} %bitcast.67, f32[128,24,128]{2,1,0:T(8,128)} %gate.1, f32[128,24,128]{2,1,0:T(8,128)} %up.1, f32[128,24,128]{2,1,0:T(8,128)} %down.1), custom_call_target="tpu_custom_call" | custom-call | flops 1179648 | bytes 7077888 | tf_op jit(solution)/shard_map/cast/pallas_call | solution.py:52
  6.5 7.9 %all-to-all-start = ((bf16[32,288,128]{2,1,0:T(8,128)(2,1)}), bf16[32,288,128]{2,1,0:T(8,128)(2,1)S(1)}, u32[]{:S(2)}, u32[]{:S(2)}) async-start(bf16[32,288,128]{2,1,0:T(8,128)(2,1)} %cast.1), calls=%async_computation | async-start | bytes 4718592 | tf_op jit(solution)/shard_map/all_to_all | solution.py:23
  18.3 11.1 %collective-permute-done.1.two = bf16[128,2048]{1,0:T(8,128)(2,1)S(1)} collective-permute-done((bf16[128,2048]{1,0:T(8,128)(2,1)S(1)}, bf16[128,2048]{1,0:T(8,128)(2,1)S(1)}, u32[]{:S(2)}, u32[]{:S(2)}) %collective-permute-start.1) | collective-permute-done | bytes 524320 | tf_op jit(solution)/shard_map/ppermute | solution.py:19
  30.2 4.8 %pick.2 = bf16[768,2048]{1,0:T(8,128)(2,1)} custom-call(bf16[32,256]{1,0:T(8,128)(2,1)} %pad_maximum_fusion.5.code, bf16[128,2048]{1,0:T(8,128)(2,1)} %copy-done, bf16[128,2048]{1,0:T(8,128)(2,1)} %copy-done.3), custom_call_target="tpu_custom_call" | custom-call | flops 805306368 | bytes 4194304 | tf_op jit(solution)/shard_map/pick/pallas_call | solution.py:224
  35.1 7.5 %all-to-all-done = bf16[32,288,128]{2,1,0:T(8,128)(2,1)S(1)} async-done(((bf16[32,288,128]{2,1,0:T(8,128)(2,1)}), bf16[32,288,128]{2,1,0:T(8,128)(2,1)S(1)}, u32[]{:S(2)}, u32[]{:S(2)}) %all-to-all-start) | async-done | bytes 2359328 | tf_op jit(solution)/shard_map/all_to_all | solution.py:23
  42.6 9.8 %all-to-all-start.1 = ((bf16[32,24,2048]{2,1,0:T(8,128)(2,1)}), bf16[32,24,2048]{2,1,0:T(8,128)(2,1)}, u32[]{:S(2)}, u32[]{:S(2)}) async-start(bf16[32,24,2048]{2,1,0:T(8,128)(2,1)} %bitcast.59), calls=%async_computation.1 | async-start | bytes 6291456 | tf_op jit(solution)/shard_map/all_to_all | solution.py:23
  52.5 3.7 collective-permute-start.2
  58.7 31.7 %collective-permute-done.4.one = bf16[128,2048]{1,0:T(8,128)(2,1)S(1)} collective-permute-done((bf16[128,2048]{1,0:T(8,128)(2,1)S(1)}, bf16[128,2048]{1,0:T(8,128)(2,1)S(1)}, u32[]{:S(2)}, u32[]{:S(2)}) %collective-permute-start.4) | collective-permute-done | bytes 524320 | tf_op jit(solution)/shard_map/ppermute | solution.py:19
  90.4 11.5 %collective-permute-done.5.two = bf16[128,2048]{1,0:T(8,128)(2,1)} collective-permute-done((bf16[128,2048]{1,0:T(8,128)(2,1)S(1)}, bf16[128,2048]{1,0:T(8,128)(2,1)}, u32[]{:S(2)}, u32[]{:S(2)}) %collective-permute-start.5) | collective-permute-done | bytes 524320 | tf_op jit(solution)/shard_map/ppermute | solution.py:19
  101.9 4.8 %pick.3 = bf16[768,2048]{1,0:T(8,128)(2,1)} custom-call(bf16[32,256]{1,0:T(8,128)(2,1)} %pad_maximum_fusion.6.code, bf16[128,2048]{1,0:T(8,128)(2,1)} %copy-done.5, bf16[128,2048]{1,0:T(8,128)(2,1)} %collective-permute-done.5.two), custom_call_target="tpu_custom_call" | custom-call | flops 805306368 | bytes 4194304 | tf_op jit(solution)/shard_map/pick/pallas_call | solution.py:224
  106.7 8.7 %all-to-all-start.2 = ((bf16[32,24,2048]{2,1,0:T(8,128)(2,1)}), bf16[32,24,2048]{2,1,0:T(8,128)(2,1)}, u32[]{:S(2)}, u32[]{:S(2)}) async-start(bf16[32,24,2048]{2,1,0:T(8,128)(2,1)} %bitcast.60), calls=%async_computation.2 | async-start | bytes 6291456 | tf_op jit(solution)/shard_map/all_to_all | solution.py:23
  115.5 5.1 %collective-permute-start.6 = (bf16[3,32,128]{2,1,0:T(8,128)(2,1)S(1)}, bf16[3,32,128]{2,1,0:T(8,128)(2,1)S(1)}, u32[]{:S(2)}, u32[]{:S(2)}) collective-permute-start(bf16[3,32,128]{2,1,0:T(8,128)(2,1)S(1)} %pad_maximum_fusion.4), channel_id=1, source_target_pairs={{0,128},{128,0},{1,129},{129,1},{2,130},{130,2},{3,131},{131,3},{4... | collective-permute-start | bytes 73736 | tf_op jit(solution)/shard_map/ppermute | solution.py:19
  122.2 30.0 %all-to-all-done.2 = bf16[32,24,2048]{2,1,0:T(8,128)(2,1)} async-done(((bf16[32,24,2048]{2,1,0:T(8,128)(2,1)}), bf16[32,24,2048]{2,1,0:T(8,128)(2,1)}, u32[]{:S(2)}, u32[]{:S(2)}) %all-to-all-start.2) | async-done | bytes 3145760 | tf_op jit(solution)/shard_map/all_to_all | solution.py:23
  153.7 9.9 %all-to-all-start.3 = ((bf16[32,192,128]{2,1,0:T(8,128)(2,1)}), bf16[32,192,128]{2,1,0:T(8,128)(2,1)}, u32[]{:S(2)}, u32[]{:S(2)}) async-start(bf16[32,192,128]{2,1,0:T(8,128)(2,1)} %broadcast_in_dim.86), calls=%async_computation.3 | async-start | bytes 3145728 | tf_op jit(solution)/shard_map/all_to_all | solution.py:23
  165.1 5.2 %collective-permute-start.7 = (bf16[32,72,128]{2,1,0:T(8,128)(2,1)}, bf16[32,72,128]{2,1,0:T(8,128)(2,1)}, u32[]{:S(2)}, u32[]{:S(2)}) collective-permute-start(bf16[32,72,128]{2,1,0:T(8,128)(2,1)} %get-tuple-element.39), channel_id=1, source_target_pairs={{0,32},{32,0},{64,96},{96,64},{128,160},{160,128},{192,224},{224,1... | collective-permute-start | bytes 1769480 | tf_op jit(solution)/shard_map/ppermute | solution.py:19
  171.0 5.0 %collective-permute-start.10 = (bf16[32,72,128]{2,1,0:T(8,128)(2,1)}, bf16[32,72,128]{2,1,0:T(8,128)(2,1)}, u32[]{:S(2)}, u32[]{:S(2)}) collective-permute-start(bf16[32,72,128]{2,1,0:T(8,128)(2,1)} %get-tuple-element.40.refs_0_), channel_id=1, source_target_pairs={{0,128},{32,160},{64,192},{96,224},{128,0},{160,32},{192,64},{224,... | collective-permute-start | bytes 1769480 | tf_op jit(solution)/shard_map/ppermute | solution.py:19
  176.0 7.6 %all-to-all-done.3 = bf16[32,192,128]{2,1,0:T(8,128)(2,1)} async-done(((bf16[32,192,128]{2,1,0:T(8,128)(2,1)}), bf16[32,192,128]{2,1,0:T(8,128)(2,1)}, u32[]{:S(2)}, u32[]{:S(2)}) %all-to-all-start.3) | async-done | bytes 1572896 | tf_op jit(solution)/shard_map/all_to_all | solution.py:23
  192.9 46.2 %collective-permute-done.10.refs_4_ = bf16[32,72,128]{2,1,0:T(8,128)(2,1)} collective-permute-done((bf16[32,72,128]{2,1,0:T(8,128)(2,1)}, bf16[32,72,128]{2,1,0:T(8,128)(2,1)}, u32[]{:S(2)}, u32[]{:S(2)}) %collective-permute-start.10) | collective-permute-done | bytes 589856 | tf_op jit(solution)/shard_map/ppermute | solution.py:19
  242.1 19.2 %collective-permute-done.13.refs_7_ = bf16[32,72,128]{2,1,0:T(8,128)(2,1)S(1)} collective-permute-done((bf16[32,72,128]{2,1,0:T(8,128)(2,1)}, bf16[32,72,128]{2,1,0:T(8,128)(2,1)S(1)}, u32[]{:S(2)}, u32[]{:S(2)}) %collective-permute-start.13) | collective-permute-done | bytes 589856 | tf_op jit(solution)/shard_map/ppermute | solution.py:19
  262.3 12.4 %ffn_assemble.1 = (bf16[768,2048]{1,0:T(8,128)(2,1)}, bf16[1,384,2048]{2,1,0:T(8,128)(2,1)}, bf16[1,384,2048]{2,1,0:T(8,128)(2,1)}, bf16[1,384,2048]{2,1,0:T(8,128)(2,1)}) custom-call(s32[16]{0:T(128)} %stack.73.place, bf16[768,2048]{1,0:T(8,128)(2,1)} %bitcast.23.x, bf16[32,72,128]{2,1,0:T(8,128)(2,1)} %get-tuple-element.40.refs_0_, ...), custom_call_target="tpu_custom_call" | custom-call | flops 3623878656 | bytes 15728640 | tf_op jit(solution)/shard_map/ffn_assemble/pallas_call | solution.py:129
  274.7 7.6 %all-to-all-start.5 = ((bf16[32,24,2048]{2,1,0:T(8,128)(2,1)}), bf16[32,24,2048]{2,1,0:T(8,128)(2,1)}, u32[]{:S(2)}, u32[]{:S(2)}) async-start(bf16[32,24,2048]{2,1,0:T(8,128)(2,1)} %bitcast.62), calls=%async_computation.5 | async-start | bytes 6291456 | tf_op jit(solution)/shard_map/all_to_all | solution.py:23
  282.3 9.4 %ffn_rows.1 = bf16[768,2048]{1,0:T(8,128)(2,1)} custom-call(bf16[768,2048]{1,0:T(8,128)(2,1)} %bitcast.10.x, bf16[1,384,2048]{2,1,0:T(8,128)(2,1)} %get-tuple-element.12.gate, bf16[1,384,2048]{2,1,0:T(8,128)(2,1)} %get-tuple-element.13.up, bf16[1,384,2048]{2,1,0:T(8,128)(2,1)} %get-tuple-element.14.down), custom_call_target="tpu_custom_call" | custom-call | flops 3623878656 | bytes 11010048 | tf_op jit(solution)/shard_map/ffn_rows/pallas_call | solution.py:158
  291.7 27.4 %all-to-all-done.5 = bf16[32,24,2048]{2,1,0:T(8,128)(2,1)} async-done(((bf16[32,24,2048]{2,1,0:T(8,128)(2,1)}), bf16[32,24,2048]{2,1,0:T(8,128)(2,1)}, u32[]{:S(2)}, u32[]{:S(2)}) %all-to-all-start.5) | async-done | bytes 3145760 | tf_op jit(solution)/shard_map/all_to_all | solution.py:23
  319.1 10.0 %all-to-all-start.4 = ((bf16[32,24,2048]{2,1,0:T(8,128)(2,1)}), bf16[32,24,2048]{2,1,0:T(8,128)(2,1)}, u32[]{:S(2)}, u32[]{:S(2)}) async-start(bf16[32,24,2048]{2,1,0:T(8,128)(2,1)} %bitcast.61), calls=%async_computation.4 | async-start | bytes 6291456 | tf_op jit(solution)/shard_map/all_to_all | solution.py:23
  334.8 5.4 %combine.3 = bf16[256,2048]{1,0:T(8,128)(2,1)} custom-call(bf16[256,768]{1,0:T(8,128)(2,1)} %fusion.2.high, bf16[256,768]{1,0:T(8,128)(2,1)} %fusion.3.low, bf16[768,2048]{1,0:T(8,128)(2,1)} %bitcast.27.back, bf16[256,128]{1,0:T(8,128)(2,1)} %get-tuple-element.28.hidden, bf16[128,2048]{1,0:T(8,128)(2,1)} %squeeze.8.down), custom_call_target="tpu_custom_call" | custom-call | flops 1744830464 | bytes 6029312 | tf_op jit(solution)/shard_map/combine/pallas_call | solution.py:253
  340.2 2.1 fusion.48
  342.3 14.4 %collective-permute-start.15 = (bf16[128,2048]{1,0:T(8,128)(2,1)}, bf16[128,2048]{1,0:T(8,128)(2,1)S(1)}, u32[]{:S(2)}, u32[]{:S(2)}) collective-permute-start(bf16[128,2048]{1,0:T(8,128)(2,1)} %get-tuple-element.44), channel_id=1, source_target_pairs={{0,64},{32,96},{64,0},{96,32},{1,65},{33,97},{65,1},{97,33},{2,66}... | collective-permute-start | bytes 1572872 | tf_op jit(solution)/shard_map/ppermute | solution.py:19
  357.4 8.5 %all-to-all-done.4 = bf16[32,24,2048]{2,1,0:T(8,128)(2,1)} async-done(((bf16[32,24,2048]{2,1,0:T(8,128)(2,1)}), bf16[32,24,2048]{2,1,0:T(8,128)(2,1)}, u32[]{:S(2)}, u32[]{:S(2)}) %all-to-all-start.4) | async-done | bytes 3145760 | tf_op jit(solution)/shard_map/all_to_all | solution.py:23
  365.9 5.6 %combine.2 = f32[256,2048]{1,0:T(8,128)} custom-call(bf16[256,768]{1,0:T(8,128)(2,1)} %fusion.high, bf16[256,768]{1,0:T(8,128)(2,1)} %fusion.1.low, bf16[768,2048]{1,0:T(8,128)(2,1)} %bitcast.25.back, bf16[256,128]{1,0:T(8,128)(2,1)} %get-tuple-element.25.hidden, bf16[128,2048]{1,0:T(8,128)(2,1)} %squeeze.8.down), custom_call_target="tpu_custom_call" | custom-call | flops 1744830464 | bytes 6029312 | tf_op jit(solution)/shard_map/combine/pallas_call | solution.py:253
  372.8 14.0 %collective-permute-start.14 = (bf16[128,2048]{1,0:T(8,128)(2,1)S(1)}, bf16[128,2048]{1,0:T(8,128)(2,1)}, u32[]{:S(2)}, u32[]{:S(2)}) collective-permute-start(bf16[128,2048]{1,0:T(8,128)(2,1)S(1)} %slice.109), channel_id=1, source_target_pairs={{0,32},{32,0},{64,96},{96,64},{1,33},{33,1},{65,97},{97,65},{2,34}... | collective-permute-start | bytes 1572872 | tf_op jit(solution)/shard_map/ppermute | solution.py:19
  390.5 12.6 %collective-permute-done.16 = bf16[128,2048]{1,0:T(8,128)(2,1)S(1)} collective-permute-done((bf16[128,2048]{1,0:T(8,128)(2,1)S(1)}, bf16[128,2048]{1,0:T(8,128)(2,1)S(1)}, u32[]{:S(2)}, u32[]{:S(2)}) %collective-permute-start.16) | collective-permute-done | bytes 524320 | tf_op jit(solution)/shard_map/ppermute | solution.py:19
  403.1 2.4 fusion.15
  (110 shorter events, 37.6 us)
Async XLA Ops:
  6.5 9.7 %copy-start.2 = (bf16[128,2048]{1,0:T(8,128)(2,1)S(1)}, bf16[128,2048]{1,0:T(8,128)(2,1)}, u32[]{:S(2)}) copy-start(bf16[128,2048]{1,0:T(8,128)(2,1)} %param.10) | copy-start | bytes 1572868
  6.5 36.1 %all-to-all-start = ((bf16[32,288,128]{2,1,0:T(8,128)(2,1)}), bf16[32,288,128]{2,1,0:T(8,128)(2,1)S(1)}, u32[]{:S(2)}, u32[]{:S(2)}) async-start(bf16[32,288,128]{2,1,0:T(8,128)(2,1)} %cast.1), calls=%async_computation | async-start | bytes 4718592 | tf_op jit(solution)/shard_map/all_to_all | solution.py:23
  14.4 3.1 collective-permute-start
  16.5 12.9 %copy-start = (bf16[128,2048]{1,0:T(8,128)(2,1)}, bf16[128,2048]{1,0:T(8,128)(2,1)S(1)}, u32[]{:S(2)}) copy-start(bf16[128,2048]{1,0:T(8,128)(2,1)S(1)} %fusion.12.one) | copy-start | bytes 1572868
  16.5 12.9 %collective-permute-start.1 = (bf16[128,2048]{1,0:T(8,128)(2,1)S(1)}, bf16[128,2048]{1,0:T(8,128)(2,1)S(1)}, u32[]{:S(2)}, u32[]{:S(2)}) collective-permute-start(bf16[128,2048]{1,0:T(8,128)(2,1)S(1)} %fusion.12.one), channel_id=1, source_target_pairs={{0,32},{32,0},{64,96},{96,64},{1,33},{33,1},{65,97},{97,65},{2,34}... | collective-permute-start | bytes 1572872 | tf_op jit(solution)/shard_map/ppermute | solution.py:19
  42.6 13.7 %copy-start.1 = (bf16[128,2048]{1,0:T(8,128)(2,1)S(1)}, bf16[128,2048]{1,0:T(8,128)(2,1)}, u32[]{:S(2)}) copy-start(bf16[128,2048]{1,0:T(8,128)(2,1)} %copy-done) | copy-start | bytes 1572868
  42.6 64.2 %all-to-all-start.1 = ((bf16[32,24,2048]{2,1,0:T(8,128)(2,1)}), bf16[32,24,2048]{2,1,0:T(8,128)(2,1)}, u32[]{:S(2)}, u32[]{:S(2)}) async-start(bf16[32,24,2048]{2,1,0:T(8,128)(2,1)} %bitcast.59), calls=%async_computation.1 | async-start | bytes 6291456 | tf_op jit(solution)/shard_map/all_to_all | solution.py:23
  52.4 3.9 collective-permute-start.3
  52.5 5.2 %collective-permute-start.2 = (f32[16,128]{1,0:T(8,128)S(1)}, f32[16,128]{1,0:T(8,128)S(1)}, u32[]{:S(2)}, u32[]{:S(2)}) collective-permute-start(f32[16,128]{1,0:T(8,128)S(1)} %pad_maximum_fusion.7), channel_id=1, source_target_pairs={{0,64},{32,96},{64,0},{96,32},{1,65},{33,97},{65,1},{97,33},{2,66}... | collective-permute-start | bytes 24584 | tf_op jit(solution)/shard_map/ppermute | solution.py:19
  56.2 34.2 %collective-permute-start.4 = (bf16[128,2048]{1,0:T(8,128)(2,1)S(1)}, bf16[128,2048]{1,0:T(8,128)(2,1)S(1)}, u32[]{:S(2)}, u32[]{:S(2)}) collective-permute-start(bf16[128,2048]{1,0:T(8,128)(2,1)S(1)} %copy-done.1), channel_id=1, source_target_pairs={{0,64},{32,96},{64,0},{96,32},{1,65},{33,97},{65,1},{97,33},{2,66}... | collective-permute-start | bytes 1572872 | tf_op jit(solution)/shard_map/ppermute | solution.py:19
  56.2 45.6 %collective-permute-start.5 = (bf16[128,2048]{1,0:T(8,128)(2,1)S(1)}, bf16[128,2048]{1,0:T(8,128)(2,1)}, u32[]{:S(2)}, u32[]{:S(2)}) collective-permute-start(bf16[128,2048]{1,0:T(8,128)(2,1)S(1)} %copy-done.1), channel_id=1, source_target_pairs={{0,96},{32,64},{64,32},{96,0},{1,97},{33,65},{65,33},{97,1},{2,98}... | collective-permute-start | bytes 1572872 | tf_op jit(solution)/shard_map/ppermute | solution.py:19
  90.4 11.5 %copy-start.5 = (bf16[128,2048]{1,0:T(8,128)(2,1)}, bf16[128,2048]{1,0:T(8,128)(2,1)S(1)}, u32[]{:S(2)}) copy-start(bf16[128,2048]{1,0:T(8,128)(2,1)S(1)} %collective-permute-done.4.one) | copy-start | bytes 1572868
  106.7 8.7 %copy-start.9 = (f32[32,128]{1,0:T(8,128)S(1)}, f32[32,128]{1,0:T(8,128)}, u32[]{:S(2)}) copy-start(f32[32,128]{1,0:T(8,128)} %param.19) | copy-start | bytes 49156
  106.7 8.8 %copy-start.12 = (f32[32,128]{1,0:T(8,128)S(1)}, f32[32,128]{1,0:T(8,128)}, u32[]{:S(2)}) copy-start(f32[32,128]{1,0:T(8,128)} %param.17) | copy-start | bytes 49156
  106.7 8.8 %copy-start.13 = (f32[32,128]{1,0:T(8,128)S(1)}, f32[32,128]{1,0:T(8,128)}, u32[]{:S(2)}) copy-start(f32[32,128]{1,0:T(8,128)} %param.18) | copy-start | bytes 49156
  106.7 8.8 %copy-start.14 = (f32[128]{0:T(128)S(1)}, f32[128]{0:T(128)}, u32[]{:S(2)}) copy-start(f32[128]{0:T(128)} %param.13) | copy-start | bytes 1540
  106.7 45.5 %all-to-all-start.2 = ((bf16[32,24,2048]{2,1,0:T(8,128)(2,1)}), bf16[32,24,2048]{2,1,0:T(8,128)(2,1)}, u32[]{:S(2)}, u32[]{:S(2)}) async-start(bf16[32,24,2048]{2,1,0:T(8,128)(2,1)} %bitcast.60), calls=%async_computation.2 | async-start | bytes 6291456 | tf_op jit(solution)/shard_map/all_to_all | solution.py:23
  115.5 6.7 %collective-permute-start.6 = (bf16[3,32,128]{2,1,0:T(8,128)(2,1)S(1)}, bf16[3,32,128]{2,1,0:T(8,128)(2,1)S(1)}, u32[]{:S(2)}, u32[]{:S(2)}) collective-permute-start(bf16[3,32,128]{2,1,0:T(8,128)(2,1)S(1)} %pad_maximum_fusion.4), channel_id=1, source_target_pairs={{0,128},{128,0},{1,129},{129,1},{2,130},{130,2},{3,131},{131,3},{4... | collective-permute-start | bytes 73736 | tf_op jit(solution)/shard_map/ppermute | solution.py:19
  153.7 29.8 %all-to-all-start.3 = ((bf16[32,192,128]{2,1,0:T(8,128)(2,1)}), bf16[32,192,128]{2,1,0:T(8,128)(2,1)}, u32[]{:S(2)}, u32[]{:S(2)}) async-start(bf16[32,192,128]{2,1,0:T(8,128)(2,1)} %broadcast_in_dim.86), calls=%async_computation.3 | async-start | bytes 3145728 | tf_op jit(solution)/shard_map/all_to_all | solution.py:23
  165.1 74.0 %collective-permute-start.11 = (bf16[32,72,128]{2,1,0:T(8,128)(2,1)}, bf16[32,72,128]{2,1,0:T(8,128)(2,1)}, u32[]{:S(2)}, u32[]{:S(2)}) collective-permute-start(bf16[32,72,128]{2,1,0:T(8,128)(2,1)} %get-tuple-element.39), channel_id=1, source_target_pairs={{0,160},{32,128},{64,224},{96,192},{128,32},{160,0},{192,96},{224,... | collective-permute-start | bytes 1769480 | tf_op jit(solution)/shard_map/ppermute | solution.py:19
  165.1 96.2 %collective-permute-start.7 = (bf16[32,72,128]{2,1,0:T(8,128)(2,1)}, bf16[32,72,128]{2,1,0:T(8,128)(2,1)}, u32[]{:S(2)}, u32[]{:S(2)}) collective-permute-start(bf16[32,72,128]{2,1,0:T(8,128)(2,1)} %get-tuple-element.39), channel_id=1, source_target_pairs={{0,32},{32,0},{64,96},{96,64},{128,160},{160,128},{192,224},{224,1... | collective-permute-start | bytes 1769480 | tf_op jit(solution)/shard_map/ppermute | solution.py:19
  170.3 71.7 %collective-permute-start.12 = (bf16[32,72,128]{2,1,0:T(8,128)(2,1)}, bf16[32,72,128]{2,1,0:T(8,128)(2,1)}, u32[]{:S(2)}, u32[]{:S(2)}) collective-permute-start(bf16[32,72,128]{2,1,0:T(8,128)(2,1)} %get-tuple-element.38), channel_id=1, source_target_pairs={{0,192},{32,224},{64,128},{96,160},{128,64},{160,96},{192,0},{224,... | collective-permute-start | bytes 1769480 | tf_op jit(solution)/shard_map/ppermute | solution.py:19
  170.3 90.9 %collective-permute-start.8 = (bf16[32,72,128]{2,1,0:T(8,128)(2,1)}, bf16[32,72,128]{2,1,0:T(8,128)(2,1)}, u32[]{:S(2)}, u32[]{:S(2)}) collective-permute-start(bf16[32,72,128]{2,1,0:T(8,128)(2,1)} %get-tuple-element.38), channel_id=1, source_target_pairs={{0,64},{32,96},{64,0},{96,32},{128,192},{160,224},{192,128},{224,1... | collective-permute-start | bytes 1769480 | tf_op jit(solution)/shard_map/ppermute | solution.py:19
  171.0 68.1 %collective-permute-start.10 = (bf16[32,72,128]{2,1,0:T(8,128)(2,1)}, bf16[32,72,128]{2,1,0:T(8,128)(2,1)}, u32[]{:S(2)}, u32[]{:S(2)}) collective-permute-start(bf16[32,72,128]{2,1,0:T(8,128)(2,1)} %get-tuple-element.40.refs_0_), channel_id=1, source_target_pairs={{0,128},{32,160},{64,192},{96,224},{128,0},{160,32},{192,64},{224,... | collective-permute-start | bytes 1769480 | tf_op jit(solution)/shard_map/ppermute | solution.py:19
  188.8 52.0 %copy-start.4 = (bf16[128,2048]{1,0:T(8,128)(2,1)S(1)}, bf16[128,2048]{1,0:T(8,128)(2,1)}, u32[]{:S(2)}) copy-start(bf16[128,2048]{1,0:T(8,128)(2,1)} %copy-done.3) | copy-start | bytes 1572868
  239.1 22.1 %collective-permute-start.13 = (bf16[32,72,128]{2,1,0:T(8,128)(2,1)}, bf16[32,72,128]{2,1,0:T(8,128)(2,1)S(1)}, u32[]{:S(2)}, u32[]{:S(2)}) collective-permute-start(bf16[32,72,128]{2,1,0:T(8,128)(2,1)} %get-tuple-element.37), channel_id=1, source_target_pairs={{0,224},{32,192},{64,160},{96,128},{128,96},{160,64},{192,32},{224... | collective-permute-start | bytes 1769480 | tf_op jit(solution)/shard_map/ppermute | solution.py:19
  239.1 22.1 %collective-permute-start.9 = (bf16[32,72,128]{2,1,0:T(8,128)(2,1)}, bf16[32,72,128]{2,1,0:T(8,128)(2,1)S(1)}, u32[]{:S(2)}, u32[]{:S(2)}) collective-permute-start(bf16[32,72,128]{2,1,0:T(8,128)(2,1)} %get-tuple-element.37), channel_id=1, source_target_pairs={{0,96},{32,64},{64,32},{96,0},{128,224},{160,192},{192,160},{224,1... | collective-permute-start | bytes 1769480 | tf_op jit(solution)/shard_map/ppermute | solution.py:19
  274.7 44.4 %all-to-all-start.5 = ((bf16[32,24,2048]{2,1,0:T(8,128)(2,1)}), bf16[32,24,2048]{2,1,0:T(8,128)(2,1)}, u32[]{:S(2)}, u32[]{:S(2)}) async-start(bf16[32,24,2048]{2,1,0:T(8,128)(2,1)} %bitcast.62), calls=%async_computation.5 | async-start | bytes 6291456 | tf_op jit(solution)/shard_map/all_to_all | solution.py:23
  319.1 46.8 %all-to-all-start.4 = ((bf16[32,24,2048]{2,1,0:T(8,128)(2,1)}), bf16[32,24,2048]{2,1,0:T(8,128)(2,1)}, u32[]{:S(2)}, u32[]{:S(2)}) async-start(bf16[32,24,2048]{2,1,0:T(8,128)(2,1)} %bitcast.61), calls=%async_computation.4 | async-start | bytes 6291456 | tf_op jit(solution)/shard_map/all_to_all | solution.py:23
  342.3 48.2 %collective-permute-start.15 = (bf16[128,2048]{1,0:T(8,128)(2,1)}, bf16[128,2048]{1,0:T(8,128)(2,1)S(1)}, u32[]{:S(2)}, u32[]{:S(2)}) collective-permute-start(bf16[128,2048]{1,0:T(8,128)(2,1)} %get-tuple-element.44), channel_id=1, source_target_pairs={{0,64},{32,96},{64,0},{96,32},{1,65},{33,97},{65,1},{97,33},{2,66}... | collective-permute-start | bytes 1572872 | tf_op jit(solution)/shard_map/ppermute | solution.py:19
  356.7 46.4 %collective-permute-start.16 = (bf16[128,2048]{1,0:T(8,128)(2,1)S(1)}, bf16[128,2048]{1,0:T(8,128)(2,1)S(1)}, u32[]{:S(2)}, u32[]{:S(2)}) collective-permute-start(bf16[128,2048]{1,0:T(8,128)(2,1)S(1)} %get-tuple-element.45), channel_id=1, source_target_pairs={{0,96},{32,64},{64,32},{96,0},{1,97},{33,65},{65,33},{97,1},{2,98}... | collective-permute-start | bytes 1572872 | tf_op jit(solution)/shard_map/ppermute | solution.py:19
  372.8 30.3 %collective-permute-start.14 = (bf16[128,2048]{1,0:T(8,128)(2,1)S(1)}, bf16[128,2048]{1,0:T(8,128)(2,1)}, u32[]{:S(2)}, u32[]{:S(2)}) collective-permute-start(bf16[128,2048]{1,0:T(8,128)(2,1)S(1)} %slice.109), channel_id=1, source_target_pairs={{0,32},{32,0},{64,96},{96,64},{1,33},{33,1},{65,97},{97,65},{2,34}... | collective-permute-start | bytes 1572872 | tf_op jit(solution)/shard_map/ppermute | solution.py:19
  (8 other events, 23.4 us)
where the time goes:
time: 409 us; the launch traced here: 405 us
  waiting for transfers between devices  218 us (53%)
  starting transfers between devices  106 us (26%)
  Pallas kernels  47.6 us (12%)
  local copies, waits for them, and re-layouts  15.4 us (4%)
  matrix products  11.7 us (3%)
  other arithmetic  4.9 us (1%)
    ppermute x17, waiting for transfers between devices, swapped(): return lax.ppermute(array, axis, [(r, r ^ k) for r in range(size)])  137 us
    all_to_all x6, waiting for transfers between devices, plane_exchange(): return lax.all_to_all(array, PLANE, split_axis=0, concat_axis=0, tiled=True)  81 us
    all_to_all x6, starting transfers between devices, plane_exchange(): return lax.all_to_all(array, PLANE, split_axis=0, concat_axis=0, tiled=True)  53.9 us
    ppermute x17, starting transfers between devices, swapped(): return lax.ppermute(array, axis, [(r, r ^ k) for r in range(size)])  52.5 us
    pallas_call x1, Pallas kernels, ffn_assemble(): pl.pallas_call(functools.partial(ffn_assemble_kernel, blocks=len(parts),...  12.4 us
    pallas_call x2, Pallas kernels, combine(): pl.pallas_call(combine_kernel, grid=(features // tile,), in_specs=[whole(...  11 us
    pallas_call x2, Pallas kernels, pick(): pl.pallas_call(functools.partial(pick_kernel, span=span, tile=tile), grid...  9.69 us
    pallas_call x1, Pallas kernels, ffn(): pl.pallas_call(ffn_kernel, grid=(count // tile,), in_specs=[rows, whole,...  9.4 us
  transfers between devices with their start and end apart: 23, of which 15 were waited for; matrix products, arithmetic and copies ran while one was open for 6% of the time, Pallas kernels for 7%

commit v1 on v0

--- a/solution.py
+++ b/solution.py
@@ -236,15 +236,44 @@
     )(code, one, two)
 
 
-def combine_kernel(high, low, back, hidden, down, out):
+def lay_kernel(place, stack, out):
+    n, groups, _, _, cols = stack.shape
+    for g in range(groups):
+        for i in range(n):
+            at = (g * n + i) * cols
+            out[:, :, at : at + cols] = stack[i ^ place[0], g]
+
+
+def lay(place, stack):
+    n, groups, matrices, rows, cols = stack.shape
+    spec = pltpu.PrefetchScalarGridSpec(
+        num_scalar_prefetch=1,
+        grid=(1,),
+        in_specs=[pl.BlockSpec(stack.shape, lambda i, p: (0,) * 5)],
+        out_specs=pl.BlockSpec((matrices, rows, groups * n * cols), lambda i, p: (0, 0, 0)),
+    )
+    return pl.pallas_call(
+        lay_kernel,
+        grid_spec=spec,
+        out_shape=jax.ShapeDtypeStruct((matrices, rows, groups * n * cols), bf16),
+        cost_estimate=pl.CostEstimate(
+            flops=stack.size, bytes_accessed=4 * stack.size, transcendentals=0
+        ),
+        name="lay",
+    )(place, stack)
+
+
+def combine_kernel(high, low, back, hidden, down, one, two):
     rows = back[...]
     total = jnp.dot(high[...], rows, preferred_element_type=f32)
     total += jnp.dot(low[...], rows, preferred_element_type=f32)
     total += jnp.dot(hidden[...], down[...], preferred_element_type=f32)
-    out[...] = total.astype(out.dtype)
-
-
-def combine(high, low, back, hidden, down, dtype, tile):
+    n = one.shape[0]
+    one[...] = total[:n].astype(one.dtype)
+    two[...] = total[n:].astype(two.dtype)
+
+
+def combine(high, low, back, hidden, down, dtypes, tile):
     count, slots = high.shape
     features = back.shape[1]
     units = hidden.shape[1]
@@ -260,8 +289,8 @@
             whole(count, units),
             part(units),
         ],
-        out_specs=part(count),
-        out_shape=jax.ShapeDtypeStruct((count, features), dtype),
+        out_specs=[part(count // 2)] * 2,
+        out_shape=[jax.ShapeDtypeStruct((count // 2, features), d) for d in dtypes],
         cost_estimate=pl.CostEstimate(
             flops=2 * count * features * (2 * slots + units),
             bytes_accessed=4 * count * slots + 2 * slots * features + 4 * count * features,
@@ -283,13 +312,13 @@
     shared_up_trained,
     shared_down_trained,
 ):
-    gr, zl, y = (lax.axis_index(a) for a in ("gr", "zl", "y"))
+    gr, zl, _ = (lax.axis_index(a) for a in ("gr", "zl", "y"))
     n_gr, n_zl, n_y = (lax.axis_size(a) for a in ("gr", "zl", "y"))
     n_xc = lax.axis_size("x") * lax.axis_size("c")
     n_plane = n_y * n_xc
     row_count, features = tokens.shape
     top = routes.shape[1]
-    experts, own_hidden, own_cols = gate_trained.shape
+    experts, own_hidden, _ = gate_trained.shape
     capacity = max(2, 3 * row_count * top // (2 * experts))
 
     meta = jnp.concatenate([routes.T.astype(f32), route_weights.T], axis=0)
@@ -328,16 +357,11 @@
     near_in = dispatched(near_picks[0], blocks[:2], landed)
     far_in = dispatched(far_picks[0], blocks[2:], near_in)
 
-    share = shared.shape[2]
-    extra = jnp.broadcast_to(
-        shared.reshape(1, -1, own_cols), (n_plane, shared.size // own_cols, own_cols)
-    )
-    extra, _ = lax.optimization_barrier((extra, far_in))
-    quarter = plane_exchange(extra).reshape(n_y, n_xc, n_gr, 3, share, own_cols)
-    quarter = quarter.transpose(3, 0, 4, 2, 1, 5).reshape(3, n_y * share, features)
-    shared_out = [
-        lax.dynamic_slice_in_dim(quarter[m], y * share, share, axis=0) for m in range(3)
-    ]
+    laid = [shared] + [swapped(shared, ("x", "c"), n_xc, k) for k in range(1, n_xc)]
+    across = (lax.axis_index("x") * lax.axis_size("c") + lax.axis_index("c"))[None]
+    own = lay(across.astype(jnp.int32), jnp.stack(laid))
+    quarter = jnp.concatenate([own] + [swapped(own, "y", n_y, k) for k in range(1, n_y)], axis=1)
+    shared_out = [own[m] for m in range(3)]
 
     def shared_hidden(pair):
         contract = (((1,), (1,)), ((), ()))
@@ -359,20 +383,32 @@
         place, far_in.reshape(-1, features), parts, n_y, n_xc, own_hidden, 256
     )
     far_back = plane_exchange(far_result.reshape(n_plane, 2 * capacity, features))
-    near_result = ffn(near_in.reshape(-1, features), expert_gate, expert_up, expert_down, 256)
+    near_result = ffn(
+        near_in.reshape(-1, features), expert_gate, expert_up, expert_down, 256
+    )
     near_back = plane_exchange(near_result.reshape(n_plane, 2 * capacity, features))
 
-    far_sum = combine(
-        *far_picks[1:], far_back.reshape(-1, features), far_hidden, shared_down, bf16, 512
-    )
-    third = swapped(far_sum[:row_count], "zl", n_zl, 2)
-    fourth = swapped(far_sum[row_count:], "zl", n_zl, 3)
-    near_sum = combine(
-        *near_picks[1:], near_back.reshape(-1, features), near_hidden, shared_down, f32, 512
-    )
-    second = swapped(near_sum[row_count:].astype(bf16), "zl", n_zl, 1)
+    third, fourth = combine(
+        *far_picks[1:],
+        far_back.reshape(-1, features),
+        far_hidden,
+        shared_down,
+        (bf16, bf16),
+        512,
+    )
+    third = swapped(third, "zl", n_zl, 2)
+    fourth = swapped(fourth, "zl", n_zl, 3)
+    kept, second = combine(
+        *near_picks[1:],
+        near_back.reshape(-1, features),
+        near_hidden,
+        shared_down,
+        (f32, bf16),
+        512,
+    )
+    second = swapped(second, "zl", n_zl, 1)
     combined = (
-        near_sum[:row_count] + second.astype(f32) + third.astype(f32) + fourth.astype(f32)
+        kept + second.astype(f32) + third.astype(f32) + fourth.astype(f32)
     ).astype(bf16)
     return (combined, expert_gate, expert_up, expert_down, *shared_out)
 

time: 409 us -> 446 us (1.090)
  blocking collectives: 0 us -> 69.4 us
  starting transfers between devices: 106 us -> 84.6 us
  local copies, waits for them, and re-layouts: 15.4 us -> 4.34 us
    all_to_all x0 -> x1, blocking collectives: none -> 69.4 us  [plane_exchange(): return lax.all_to_all(array, PLANE, split_axis=0, concat_axis=0, tiled=True)]
    all_to_all x6 -> x4, waiting for transfers between devices: 81 us -> 19 us  [plane_exchange(): return lax.all_to_all(array, PLANE, split_axis=0, concat_axis=0, tiled=True)]
    ppermute x17 -> x27, waiting for transfers between devices: 137 us -> 195 us  [swapped(): return lax.ppermute(array, axis, [(r, r ^ k) for r in range(size)])]
    all_to_all x6 -> x4, starting transfers between devices: 53.9 us -> 34.1 us  [plane_exchange(): return lax.all_to_all(array, PLANE, split_axis=0, concat_axis=0, tiled=True)]
    slice x6 -> x0, local copies, waits for them, and re-layouts: 6.19 us -> none  [the longest x1 2.12 us: body(): third = swapped(far_sum[:row_count], 'zl', n_zl, 2)]
    ppermute x17 -> x27, starting transfers between devices: 52.5 us -> 50.5 us  [swapped(): return lax.ppermute(array, axis, [(r, r ^ k) for r in range(size)])]
  transfers between devices with their start and end apart: 23 -> 31, of which waited for: 15 -> 15; matrix products, arithmetic and copies ran while one was open for 6% -> 5% of each run, Pallas kernels for 7% -> 5%
where the time goes in v1:
time: 446 us; the launch traced here: 441 us
  waiting for transfers between devices  214 us (48%)
  starting transfers between devices  84.6 us (19%)
  blocking collectives  69.4 us (16%)
  Pallas kernels  49.4 us (11%)
  matrix products  12.6 us (3%)
  other arithmetic  6.06 us (1%)
    ppermute x27, waiting for transfers between devices, swapped(): return lax.ppermute(array, axis, [(r, r ^ k) for r in range(size)])  195 us
    all_to_all x1, blocking collectives, plane_exchange(): return lax.all_to_all(array, PLANE, split_axis=0, concat_axis=0, tiled=True)  69.4 us
    ppermute x27, starting transfers between devices, swapped(): return lax.ppermute(array, axis, [(r, r ^ k) for r in range(size)])  50.5 us
    all_to_all x4, starting transfers between devices, plane_exchange(): return lax.all_to_all(array, PLANE, split_axis=0, concat_axis=0, tiled=True)  34.1 us
    all_to_all x4, waiting for transfers between devices, plane_exchange(): return lax.all_to_all(array, PLANE, split_axis=0, concat_axis=0, tiled=True)  19 us
    pallas_call x1, Pallas kernels, ffn_assemble(): pl.pallas_call(functools.partial(ffn_assemble_kernel, blocks=len(parts),...  12.4 us
    pallas_call x2, Pallas kernels, combine(): pl.pallas_call(combine_kernel, grid=(features // tile,), in_specs=[whole(...  10.9 us
    pallas_call x2, Pallas kernels, pick(): pl.pallas_call(functools.partial(pick_kernel, span=span, tile=tile), grid...  9.71 us
  transfers between devices with their start and end apart: 31, of which 15 were waited for; matrix products, arithmetic and copies ran while one was open for 5% of the time, Pallas kernels for 5%

profile of v1, /device:TPU:77, one launch (start us, length us, event | category | flops | bytes accessed | tf_op | source)
XLA Modules:
  0.0 441.2 jit_solution(9112906148751974651)
XLA Ops:
  1.3 5.1 %cast.1 = bf16[32,288,128]{2,1,0:T(8,128)(2,1)} custom-call(s32[16]{0:T(128)} %stack.106.place, f32[1,128]{1,0:T(1,128)} %bitcast.96, f32[128,24,128]{2,1,0:T(8,128)} %gate.1, f32[128,24,128]{2,1,0:T(8,128)} %up.1, f32[128,24,128]{2,1,0:T(8,128)} %down.1), custom_call_target="tpu_custom_call" | custom-call | flops 1179648 | bytes 7077888 | tf_op jit(solution)/shard_map/cast/pallas_call | solution.py:52
  6.4 7.9 %all-to-all-start = ((bf16[32,288,128]{2,1,0:T(8,128)(2,1)}), bf16[32,288,128]{2,1,0:T(8,128)(2,1)S(1)}, u32[]{:S(2)}, u32[]{:S(2)}) async-start(bf16[32,288,128]{2,1,0:T(8,128)(2,1)} %cast.1), calls=%async_computation | async-start | bytes 4718592 | tf_op jit(solution)/shard_map/all_to_all | solution.py:23
  14.9 2.8 collective-permute-start.5
  21.1 30.2 %collective-permute-done = f32[16,128]{1,0:T(8,128)S(1)} collective-permute-done((f32[16,128]{1,0:T(8,128)S(1)}, f32[16,128]{1,0:T(8,128)S(1)}, u32[]{:S(2)}, u32[]{:S(2)}) %collective-permute-start) | collective-permute-done | bytes 8224 | tf_op jit(solution)/shard_map/ppermute | solution.py:19
  52.9 5.0 %collective-permute-start.6 = (bf16[3,32,128]{2,1,0:T(8,128)(2,1)S(1)}, bf16[3,32,128]{2,1,0:T(8,128)(2,1)S(1)}, u32[]{:S(2)}, u32[]{:S(2)}) collective-permute-start(bf16[3,32,128]{2,1,0:T(8,128)(2,1)S(1)} %pad_maximum_fusion.5), channel_id=1, source_target_pairs={{0,128},{128,0},{1,129},{129,1},{2,130},{130,2},{3,131},{131,3},{4... | collective-permute-start | bytes 73736 | tf_op jit(solution)/shard_map/ppermute | solution.py:19
  58.0 4.8 %pick.2 = bf16[768,2048]{1,0:T(8,128)(2,1)} custom-call(bf16[32,256]{1,0:T(8,128)(2,1)} %pad_maximum_fusion.6.code, bf16[128,2048]{1,0:T(8,128)(2,1)} %copy-done, bf16[128,2048]{1,0:T(8,128)(2,1)} %copy-done.4), custom_call_target="tpu_custom_call" | custom-call | flops 805306368 | bytes 4194304 | tf_op jit(solution)/shard_map/pick/pallas_call | solution.py:224
  62.8 8.9 %all-to-all-start.1 = ((bf16[32,24,2048]{2,1,0:T(8,128)(2,1)}), bf16[32,24,2048]{2,1,0:T(8,128)(2,1)}, u32[]{:S(2)}, u32[]{:S(2)}) async-start(bf16[32,24,2048]{2,1,0:T(8,128)(2,1)} %bitcast.87), calls=%async_computation.1 | async-start | bytes 6291456 | tf_op jit(solution)/shard_map/all_to_all | solution.py:23
  74.7 34.4 %collective-permute-done.8 = bf16[2,3,32,128]{3,2,1,0:T(8,128)(2,1)S(1)} collective-permute-done((bf16[2,3,32,128]{3,2,1,0:T(8,128)(2,1)S(1)}, bf16[2,3,32,128]{3,2,1,0:T(8,128)(2,1)S(1)}, u32[]{:S(2)}, u32[]{:S(2)}) %collective-permute-start.8) | collective-permute-done | bytes 49184 | tf_op jit(solution)/shard_map/ppermute | solution.py:19
  109.1 2.2 collective-permute-start.11
  111.5 2.4 collective-permute-start.12
  114.1 1.9 collective-permute-done.12
  123.5 4.9 %pick.3 = bf16[768,2048]{1,0:T(8,128)(2,1)} custom-call(bf16[32,256]{1,0:T(8,128)(2,1)} %pad_maximum_fusion.7.code, bf16[128,2048]{1,0:T(8,128)(2,1)} %collective-permute-done.4.one, bf16[128,2048]{1,0:T(8,128)(2,1)} %collective-permute-done.5.two), custom_call_target="tpu_custom_call" | custom-call | flops 805306368 | bytes 4194304 | tf_op jit(solution)/shard_map/pick/pallas_call | solution.py:224
  128.4 9.5 %all-to-all-start.2 = ((bf16[32,24,2048]{2,1,0:T(8,128)(2,1)}), bf16[32,24,2048]{2,1,0:T(8,128)(2,1)}, u32[]{:S(2)}, u32[]{:S(2)}) async-start(bf16[32,24,2048]{2,1,0:T(8,128)(2,1)} %bitcast.88), calls=%async_computation.2 | async-start | bytes 6291456 | tf_op jit(solution)/shard_map/all_to_all | solution.py:23
  137.9 1.9 collective-permute-done.15
  147.5 3.1 collective-permute-start.17
  155.4 3.1 collective-permute-start.22
  159.2 4.1 collective-permute-done.17.refs_1_
  163.4 16.0 %collective-permute-done.18.refs_2_ = bf16[32,72,128]{2,1,0:T(8,128)(2,1)S(1)} collective-permute-done((bf16[32,72,128]{2,1,0:T(8,128)(2,1)}, bf16[32,72,128]{2,1,0:T(8,128)(2,1)S(1)}, u32[]{:S(2)}, u32[]{:S(2)}) %collective-permute-start.18) | collective-permute-done | bytes 589856 | tf_op jit(solution)/shard_map/ppermute | solution.py:19
  179.4 6.0 %collective-permute-start.20 = (bf16[32,72,128]{2,1,0:T(8,128)(2,1)S(1)}, bf16[32,72,128]{2,1,0:T(8,128)(2,1)}, u32[]{:S(2)}, u32[]{:S(2)}) collective-permute-start(bf16[32,72,128]{2,1,0:T(8,128)(2,1)S(1)} %get-tuple-element.46.refs_0_), channel_id=1, source_target_pairs={{0,128},{32,160},{64,192},{96,224},{128,0},{160,32},{192,64},{224,... | collective-permute-start | bytes 1769480 | tf_op jit(solution)/shard_map/ppermute | solution.py:19
  186.6 52.6 %collective-permute-done.19.refs_3_ = bf16[32,72,128]{2,1,0:T(8,128)(2,1)} collective-permute-done((bf16[32,72,128]{2,1,0:T(8,128)(2,1)}, bf16[32,72,128]{2,1,0:T(8,128)(2,1)}, u32[]{:S(2)}, u32[]{:S(2)}) %collective-permute-start.19) | collective-permute-done | bytes 589856 | tf_op jit(solution)/shard_map/ppermute | solution.py:19
  239.3 5.9 %collective-permute-done.20.refs_4_ = bf16[32,72,128]{2,1,0:T(8,128)(2,1)} collective-permute-done((bf16[32,72,128]{2,1,0:T(8,128)(2,1)S(1)}, bf16[32,72,128]{2,1,0:T(8,128)(2,1)}, u32[]{:S(2)}, u32[]{:S(2)}) %collective-permute-start.20) | collective-permute-done | bytes 589856 | tf_op jit(solution)/shard_map/ppermute | solution.py:19
  245.2 12.4 %ffn_assemble.1 = (bf16[768,2048]{1,0:T(8,128)(2,1)}, bf16[1,384,2048]{2,1,0:T(8,128)(2,1)}, bf16[1,384,2048]{2,1,0:T(8,128)(2,1)}, bf16[1,384,2048]{2,1,0:T(8,128)(2,1)}) custom-call(s32[16]{0:T(128)} %stack.106.place, bf16[768,2048]{1,0:T(8,128)(2,1)} %bitcast.32.x, bf16[32,72,128]{2,1,0:T(8,128)(2,1)} %copy-done.7, bf16[32,72,128]{2,1,0:T(8,128)(2,1)} %copy-done.14, ...), custom_call_target="tpu_custom_call" | custom-call | flops 3623878656 | bytes 15728640 | tf_op jit(solution)/shard_map/ffn_assemble/pallas_call | solution.py:129
  257.6 9.4 %ffn_rows.1 = bf16[768,2048]{1,0:T(8,128)(2,1)} custom-call(bf16[768,2048]{1,0:T(8,128)(2,1)} %bitcast.10.x, bf16[1,384,2048]{2,1,0:T(8,128)(2,1)} %get-tuple-element.15.gate, bf16[1,384,2048]{2,1,0:T(8,128)(2,1)} %get-tuple-element.16.up, bf16[1,384,2048]{2,1,0:T(8,128)(2,1)} %get-tuple-element.17.down), custom_call_target="tpu_custom_call" | custom-call | flops 3623878656 | bytes 11010048 | tf_op jit(solution)/shard_map/ffn_rows/pallas_call | solution.py:158
  267.1 69.4 %all_to_all.25 = bf16[32,24,2048]{2,1,0:T(8,128)(2,1)} all-to-all(bf16[32,24,2048]{2,1,0:T(8,128)(2,1)} %bitcast.91), channel_id=1, replica_groups=mesh['gr'=2,'zl'=4,'y'=4,'x'=4,'c'=2] {'y','x','c'}, dimensions={0} | all-to-all | bytes 6291456 | tf_op jit(solution)/shard_map/all_to_all | solution.py:23
  336.4 7.8 %all-to-all-start.4 = ((bf16[32,24,2048]{2,1,0:T(8,128)(2,1)}), bf16[32,24,2048]{2,1,0:T(8,128)(2,1)}, u32[]{:S(2)}, u32[]{:S(2)}) async-start(bf16[32,24,2048]{2,1,0:T(8,128)(2,1)} %bitcast.89), calls=%async_computation.4 | async-start | bytes 6291456 | tf_op jit(solution)/shard_map/all_to_all | solution.py:23
  349.8 5.4 %combine.2 = (f32[128,2048]{1,0:T(8,128)}, bf16[128,2048]{1,0:T(8,128)(2,1)}) custom-call(bf16[256,768]{1,0:T(8,128)(2,1)} %fusion.high, bf16[256,768]{1,0:T(8,128)(2,1)} %fusion.1.low, bf16[768,2048]{1,0:T(8,128)(2,1)} %bitcast.90, bf16[256,128]{1,0:T(8,128)(2,1)} %pad_maximum_fusion.1.hidden, bf16[128,2048]{1,0:T(8,128)(2,1)} %slice_bitcast_fusion.down), custom_call_target="tpu_custom_call" | custom-call | flops 1744830464 | bytes 6029312 | tf_op jit(solution)/shard_map/combine/pallas_call | solution.py:282
  355.3 6.8 %collective-permute-start.24 = (bf16[128,2048]{1,0:T(8,128)(2,1)}, bf16[128,2048]{1,0:T(8,128)(2,1)S(1)}, u32[]{:S(2)}, u32[]{:S(2)}) collective-permute-start(bf16[128,2048]{1,0:T(8,128)(2,1)} %get-tuple-element.30), channel_id=1, source_target_pairs={{0,32},{32,0},{64,96},{96,64},{1,33},{33,1},{65,97},{97,65},{2,34}... | collective-permute-start | bytes 1572872 | tf_op jit(solution)/shard_map/ppermute | solution.py:19
  362.1 19.0 %all-to-all-done.4 = bf16[32,24,2048]{2,1,0:T(8,128)(2,1)} async-done(((bf16[32,24,2048]{2,1,0:T(8,128)(2,1)}), bf16[32,24,2048]{2,1,0:T(8,128)(2,1)}, u32[]{:S(2)}, u32[]{:S(2)}) %all-to-all-start.4) | async-done | bytes 3145760 | tf_op jit(solution)/shard_map/all_to_all | solution.py:23
  381.1 5.5 %combine.3 = (bf16[128,2048]{1,0:T(8,128)(2,1)}, bf16[128,2048]{1,0:T(8,128)(2,1)}) custom-call(bf16[256,768]{1,0:T(8,128)(2,1)} %fusion.2.high, bf16[256,768]{1,0:T(8,128)(2,1)} %fusion.3.low, bf16[768,2048]{1,0:T(8,128)(2,1)} %bitcast.36.back, bf16[256,128]{1,0:T(8,128)(2,1)} %pad_maximum_fusion.2.hidden, bf16[128,2048]{1,0:T(8,128)(2,1)} %slice_bitcast_fusion.down), custom_call_target="tpu_custom_call" | custom-call | flops 1744830464 | bytes 6029312 | tf_op jit(solution)/shard_map/combine/pallas_call | solution.py:282
  386.5 7.3 %collective-permute-start.25 = (bf16[128,2048]{1,0:T(8,128)(2,1)}, bf16[128,2048]{1,0:T(8,128)(2,1)S(1)}, u32[]{:S(2)}, u32[]{:S(2)}) collective-permute-start(bf16[128,2048]{1,0:T(8,128)(2,1)} %get-tuple-element.33), channel_id=1, source_target_pairs={{0,64},{32,96},{64,0},{96,32},{1,65},{33,97},{65,1},{97,33},{2,66}... | collective-permute-start | bytes 1572872 | tf_op jit(solution)/shard_map/ppermute | solution.py:19
  395.3 32.2 %collective-permute-done.25 = bf16[128,2048]{1,0:T(8,128)(2,1)S(1)} collective-permute-done((bf16[128,2048]{1,0:T(8,128)(2,1)}, bf16[128,2048]{1,0:T(8,128)(2,1)S(1)}, u32[]{:S(2)}, u32[]{:S(2)}) %collective-permute-start.25) | collective-permute-done | bytes 524320 | tf_op jit(solution)/shard_map/ppermute | solution.py:19
  427.5 12.6 %collective-permute-done.26 = bf16[128,2048]{1,0:T(8,128)(2,1)S(1)} collective-permute-done((bf16[128,2048]{1,0:T(8,128)(2,1)}, bf16[128,2048]{1,0:T(8,128)(2,1)S(1)}, u32[]{:S(2)}, u32[]{:S(2)}) %collective-permute-start.26) | collective-permute-done | bytes 524320 | tf_op jit(solution)/shard_map/ppermute | solution.py:19
  (126 shorter events, 39.5 us)
Async XLA Ops:
  6.4 56.4 %all-to-all-start = ((bf16[32,288,128]{2,1,0:T(8,128)(2,1)}), bf16[32,288,128]{2,1,0:T(8,128)(2,1)S(1)}, u32[]{:S(2)}, u32[]{:S(2)}) async-start(bf16[32,288,128]{2,1,0:T(8,128)(2,1)} %cast.1), calls=%async_computation | async-start | bytes 4718592 | tf_op jit(solution)/shard_map/all_to_all | solution.py:23
  14.8 108.8 %collective-permute-start.4 = (bf16[128,2048]{1,0:T(8,128)(2,1)S(1)}, bf16[128,2048]{1,0:T(8,128)(2,1)}, u32[]{:S(2)}, u32[]{:S(2)}) collective-permute-start(bf16[128,2048]{1,0:T(8,128)(2,1)S(1)} %fusion.11.one), channel_id=1, source_target_pairs={{0,64},{32,96},{64,0},{96,32},{1,65},{33,97},{65,1},{97,33},{2,66}... | collective-permute-start | bytes 1572872 | tf_op jit(solution)/shard_map/ppermute | solution.py:19
  14.9 108.7 %collective-permute-start.5 = (bf16[128,2048]{1,0:T(8,128)(2,1)S(1)}, bf16[128,2048]{1,0:T(8,128)(2,1)}, u32[]{:S(2)}, u32[]{:S(2)}) collective-permute-start(bf16[128,2048]{1,0:T(8,128)(2,1)S(1)} %fusion.11.one), channel_id=1, source_target_pairs={{0,96},{32,64},{64,32},{96,0},{1,97},{33,65},{65,33},{97,1},{2,98}... | collective-permute-start | bytes 1572872 | tf_op jit(solution)/shard_map/ppermute | solution.py:19
  17.7 35.3 %collective-permute-start.1 = (bf16[128,2048]{1,0:T(8,128)(2,1)S(1)}, bf16[128,2048]{1,0:T(8,128)(2,1)S(1)}, u32[]{:S(2)}, u32[]{:S(2)}) collective-permute-start(bf16[128,2048]{1,0:T(8,128)(2,1)S(1)} %fusion.11.one), channel_id=1, source_target_pairs={{0,32},{32,0},{64,96},{96,64},{1,33},{33,1},{65,97},{97,65},{2,34}... | collective-permute-start | bytes 1572872 | tf_op jit(solution)/shard_map/ppermute | solution.py:19
  18.4 53.3 %collective-permute-start.2 = (f32[16,128]{1,0:T(8,128)S(1)}, f32[16,128]{1,0:T(8,128)S(1)}, u32[]{:S(2)}, u32[]{:S(2)}) collective-permute-start(f32[16,128]{1,0:T(8,128)S(1)} %pad_maximum_fusion.8), channel_id=1, source_target_pairs={{0,64},{32,96},{64,0},{96,32},{1,65},{33,97},{65,1},{97,33},{2,66}... | collective-permute-start | bytes 24584 | tf_op jit(solution)/shard_map/ppermute | solution.py:19
  19.0 32.3 %collective-permute-start = (f32[16,128]{1,0:T(8,128)S(1)}, f32[16,128]{1,0:T(8,128)S(1)}, u32[]{:S(2)}, u32[]{:S(2)}) collective-permute-start(f32[16,128]{1,0:T(8,128)S(1)} %pad_maximum_fusion.8), channel_id=1, source_target_pairs={{0,32},{32,0},{64,96},{96,64},{1,33},{33,1},{65,97},{97,65},{2,34}... | collective-permute-start | bytes 24584 | tf_op jit(solution)/shard_map/ppermute | solution.py:19
  51.3 20.5 %collective-permute-start.3 = (f32[16,128]{1,0:T(8,128)S(1)}, f32[16,128]{1,0:T(8,128)S(1)}, u32[]{:S(2)}, u32[]{:S(2)}) collective-permute-start(f32[16,128]{1,0:T(8,128)S(1)} %pad_maximum_fusion.8), channel_id=1, source_target_pairs={{0,96},{32,64},{64,32},{96,0},{1,97},{33,65},{65,33},{97,1},{2,98}... | collective-permute-start | bytes 24584 | tf_op jit(solution)/shard_map/ppermute | solution.py:19
  52.9 19.1 %collective-permute-start.6 = (bf16[3,32,128]{2,1,0:T(8,128)(2,1)S(1)}, bf16[3,32,128]{2,1,0:T(8,128)(2,1)S(1)}, u32[]{:S(2)}, u32[]{:S(2)}) collective-permute-start(bf16[3,32,128]{2,1,0:T(8,128)(2,1)S(1)} %pad_maximum_fusion.5), channel_id=1, source_target_pairs={{0,128},{128,0},{1,129},{129,1},{2,130},{130,2},{3,131},{131,3},{4... | collective-permute-start | bytes 73736 | tf_op jit(solution)/shard_map/ppermute | solution.py:19
  62.8 65.6 %all-to-all-start.1 = ((bf16[32,24,2048]{2,1,0:T(8,128)(2,1)}), bf16[32,24,2048]{2,1,0:T(8,128)(2,1)}, u32[]{:S(2)}, u32[]{:S(2)}) async-start(bf16[32,24,2048]{2,1,0:T(8,128)(2,1)} %bitcast.87), calls=%async_computation.1 | async-start | bytes 6291456 | tf_op jit(solution)/shard_map/all_to_all | solution.py:23
  72.0 2.2 collective-permute-start.7
  72.5 36.6 %collective-permute-start.8 = (bf16[2,3,32,128]{3,2,1,0:T(8,128)(2,1)S(1)}, bf16[2,3,32,128]{3,2,1,0:T(8,128)(2,1)S(1)}, u32[]{:S(2)}, u32[]{:S(2)}) collective-permute-start(bf16[2,3,32,128]{3,2,1,0:T(8,128)(2,1)S(1)} %maximum_select_fusion.1), channel_id=1, source_target_pairs={{0,2},{1,3},{2,0},{3,1},{4,6},{5,7},{6,4},{7,5},{8,10},{9,11},{10,... | collective-permute-start | bytes 147464 | tf_op jit(solution)/shard_map/ppermute | solution.py:19
  73.4 38.1 %collective-permute-start.9 = (bf16[2,3,32,128]{3,2,1,0:T(8,128)(2,1)S(1)}, bf16[2,3,32,128]{3,2,1,0:T(8,128)(2,1)S(1)}, u32[]{:S(2)}, u32[]{:S(2)}) collective-permute-start(bf16[2,3,32,128]{3,2,1,0:T(8,128)(2,1)S(1)} %maximum_select_fusion.1), channel_id=1, source_target_pairs={{0,3},{1,2},{2,1},{3,0},{4,7},{5,6},{6,5},{7,4},{8,11},{9,10},{10,... | collective-permute-start | bytes 147464 | tf_op jit(solution)/shard_map/ppermute | solution.py:19
  74.3 39.6 %collective-permute-start.10 = (bf16[2,3,32,128]{3,2,1,0:T(8,128)(2,1)S(1)}, bf16[2,3,32,128]{3,2,1,0:T(8,128)(2,1)S(1)}, u32[]{:S(2)}, u32[]{:S(2)}) collective-permute-start(bf16[2,3,32,128]{3,2,1,0:T(8,128)(2,1)S(1)} %maximum_select_fusion.1), channel_id=1, source_target_pairs={{0,4},{1,5},{2,6},{3,7},{4,0},{5,1},{6,2},{7,3},{8,12},{9,13},{10,... | collective-permute-start | bytes 147464 | tf_op jit(solution)/shard_map/ppermute | solution.py:19
  109.1 5.0 %collective-permute-start.11 = (bf16[2,3,32,128]{3,2,1,0:T(8,128)(2,1)S(1)}, bf16[2,3,32,128]{3,2,1,0:T(8,128)(2,1)S(1)}, u32[]{:S(2)}, u32[]{:S(2)}) collective-permute-start(bf16[2,3,32,128]{3,2,1,0:T(8,128)(2,1)S(1)} %maximum_select_fusion.1), channel_id=1, source_target_pairs={{0,5},{1,4},{2,7},{3,6},{4,1},{5,0},{6,3},{7,2},{8,13},{9,12},{10,... | collective-permute-start | bytes 147464 | tf_op jit(solution)/shard_map/ppermute | solution.py:19
  111.5 4.5 %collective-permute-start.12 = (bf16[2,3,32,128]{3,2,1,0:T(8,128)(2,1)S(1)}, bf16[2,3,32,128]{3,2,1,0:T(8,128)(2,1)S(1)}, u32[]{:S(2)}, u32[]{:S(2)}) collective-permute-start(bf16[2,3,32,128]{3,2,1,0:T(8,128)(2,1)S(1)} %maximum_select_fusion.1), channel_id=1, source_target_pairs={{0,6},{1,7},{2,4},{3,5},{4,2},{5,3},{6,0},{7,1},{8,14},{9,15},{10,... | collective-permute-start | bytes 147464 | tf_op jit(solution)/shard_map/ppermute | solution.py:19
  113.9 3.6 collective-permute-start.13
  120.1 17.8 %collective-permute-start.14 = (bf16[3,32,2048]{2,1,0:T(8,128)(2,1)}, bf16[3,32,2048]{2,1,0:T(8,128)(2,1)S(1)}, u32[]{:S(2)}, u32[]{:S(2)}) collective-permute-start(bf16[3,32,2048]{2,1,0:T(8,128)(2,1)} %lay.1), channel_id=1, source_target_pairs={{0,8},{8,0},{16,24},{24,16},{1,9},{9,1},{17,25},{25,17},{2,10},{10... | collective-permute-start | bytes 1179656 | tf_op jit(solution)/shard_map/ppermute | solution.py:19
  120.1 19.8 %collective-permute-start.15 = (bf16[3,32,2048]{2,1,0:T(8,128)(2,1)}, bf16[3,32,2048]{2,1,0:T(8,128)(2,1)}, u32[]{:S(2)}, u32[]{:S(2)}) collective-permute-start(bf16[3,32,2048]{2,1,0:T(8,128)(2,1)} %lay.1), channel_id=1, source_target_pairs={{0,16},{8,24},{16,0},{24,8},{1,17},{9,25},{17,1},{25,9},{2,18},{10... | collective-permute-start | bytes 1179656 | tf_op jit(solution)/shard_map/ppermute | solution.py:19
  121.8 19.0 %collective-permute-start.16 = (bf16[3,32,2048]{2,1,0:T(8,128)(2,1)}, bf16[3,32,2048]{2,1,0:T(8,128)(2,1)}, u32[]{:S(2)}, u32[]{:S(2)}) collective-permute-start(bf16[3,32,2048]{2,1,0:T(8,128)(2,1)} %lay.1), channel_id=1, source_target_pairs={{0,24},{8,16},{16,8},{24,0},{1,25},{9,17},{17,9},{25,1},{2,26},{10... | collective-permute-start | bytes 1179656 | tf_op jit(solution)/shard_map/ppermute | solution.py:19
  128.4 58.2 %all-to-all-start.2 = ((bf16[32,24,2048]{2,1,0:T(8,128)(2,1)}), bf16[32,24,2048]{2,1,0:T(8,128)(2,1)}, u32[]{:S(2)}, u32[]{:S(2)}) async-start(bf16[32,24,2048]{2,1,0:T(8,128)(2,1)} %bitcast.88), calls=%async_computation.2 | async-start | bytes 6291456 | tf_op jit(solution)/shard_map/all_to_all | solution.py:23
  147.5 15.8 %collective-permute-start.17 = (bf16[32,72,128]{2,1,0:T(8,128)(2,1)}, bf16[32,72,128]{2,1,0:T(8,128)(2,1)S(1)}, u32[]{:S(2)}, u32[]{:S(2)}) collective-permute-start(bf16[32,72,128]{2,1,0:T(8,128)(2,1)} %get-tuple-element.45), channel_id=1, source_target_pairs={{0,32},{32,0},{64,96},{96,64},{128,160},{160,128},{192,224},{224,1... | collective-permute-start | bytes 1769480 | tf_op jit(solution)/shard_map/ppermute | solution.py:19
  150.6 28.8 %collective-permute-start.18 = (bf16[32,72,128]{2,1,0:T(8,128)(2,1)}, bf16[32,72,128]{2,1,0:T(8,128)(2,1)S(1)}, u32[]{:S(2)}, u32[]{:S(2)}) collective-permute-start(bf16[32,72,128]{2,1,0:T(8,128)(2,1)} %get-tuple-element.44), channel_id=1, source_target_pairs={{0,64},{32,96},{64,0},{96,32},{128,192},{160,224},{192,128},{224,1... | collective-permute-start | bytes 1769480 | tf_op jit(solution)/shard_map/ppermute | solution.py:19
  154.5 90.7 %collective-permute-start.21 = (bf16[32,72,128]{2,1,0:T(8,128)(2,1)}, bf16[32,72,128]{2,1,0:T(8,128)(2,1)}, u32[]{:S(2)}, u32[]{:S(2)}) collective-permute-start(bf16[32,72,128]{2,1,0:T(8,128)(2,1)} %get-tuple-element.45), channel_id=1, source_target_pairs={{0,160},{32,128},{64,224},{96,192},{128,32},{160,0},{192,96},{224,... | collective-permute-start | bytes 1769480 | tf_op jit(solution)/shard_map/ppermute | solution.py:19
  155.4 89.8 %collective-permute-start.22 = (bf16[32,72,128]{2,1,0:T(8,128)(2,1)}, bf16[32,72,128]{2,1,0:T(8,128)(2,1)}, u32[]{:S(2)}, u32[]{:S(2)}) collective-permute-start(bf16[32,72,128]{2,1,0:T(8,128)(2,1)} %get-tuple-element.44), channel_id=1, source_target_pairs={{0,192},{32,224},{64,128},{96,160},{128,64},{160,96},{192,0},{224,... | collective-permute-start | bytes 1769480 | tf_op jit(solution)/shard_map/ppermute | solution.py:19
  158.5 80.8 %collective-permute-start.19 = (bf16[32,72,128]{2,1,0:T(8,128)(2,1)}, bf16[32,72,128]{2,1,0:T(8,128)(2,1)}, u32[]{:S(2)}, u32[]{:S(2)}) collective-permute-start(bf16[32,72,128]{2,1,0:T(8,128)(2,1)} %get-tuple-element.43), channel_id=1, source_target_pairs={{0,96},{32,64},{64,32},{96,0},{128,224},{160,192},{192,160},{224,1... | collective-permute-start | bytes 1769480 | tf_op jit(solution)/shard_map/ppermute | solution.py:19
  163.3 81.9 %copy-start.14 = (bf16[32,72,128]{2,1,0:T(8,128)(2,1)}, bf16[32,72,128]{2,1,0:T(8,128)(2,1)S(1)}, u32[]{:S(2)}) copy-start(bf16[32,72,128]{2,1,0:T(8,128)(2,1)S(1)} %collective-permute-done.17.refs_1_) | copy-start | bytes 1769476
  163.3 81.9 %collective-permute-start.23 = (bf16[32,72,128]{2,1,0:T(8,128)(2,1)}, bf16[32,72,128]{2,1,0:T(8,128)(2,1)}, u32[]{:S(2)}, u32[]{:S(2)}) collective-permute-start(bf16[32,72,128]{2,1,0:T(8,128)(2,1)} %get-tuple-element.43), channel_id=1, source_target_pairs={{0,224},{32,192},{64,160},{96,128},{128,96},{160,64},{192,32},{224... | collective-permute-start | bytes 1769480 | tf_op jit(solution)/shard_map/ppermute | solution.py:19
  179.4 65.8 %collective-permute-start.20 = (bf16[32,72,128]{2,1,0:T(8,128)(2,1)S(1)}, bf16[32,72,128]{2,1,0:T(8,128)(2,1)}, u32[]{:S(2)}, u32[]{:S(2)}) collective-permute-start(bf16[32,72,128]{2,1,0:T(8,128)(2,1)S(1)} %get-tuple-element.46.refs_0_), channel_id=1, source_target_pairs={{0,128},{32,160},{64,192},{96,224},{128,0},{160,32},{192,64},{224,... | collective-permute-start | bytes 1769480 | tf_op jit(solution)/shard_map/ppermute | solution.py:19
  336.4 44.6 %all-to-all-start.4 = ((bf16[32,24,2048]{2,1,0:T(8,128)(2,1)}), bf16[32,24,2048]{2,1,0:T(8,128)(2,1)}, u32[]{:S(2)}, u32[]{:S(2)}) async-start(bf16[32,24,2048]{2,1,0:T(8,128)(2,1)} %bitcast.89), calls=%async_computation.4 | async-start | bytes 6291456 | tf_op jit(solution)/shard_map/all_to_all | solution.py:23
  355.3 40.0 %collective-permute-start.24 = (bf16[128,2048]{1,0:T(8,128)(2,1)}, bf16[128,2048]{1,0:T(8,128)(2,1)S(1)}, u32[]{:S(2)}, u32[]{:S(2)}) collective-permute-start(bf16[128,2048]{1,0:T(8,128)(2,1)} %get-tuple-element.30), channel_id=1, source_target_pairs={{0,32},{32,0},{64,96},{96,64},{1,33},{33,1},{65,97},{97,65},{2,34}... | collective-permute-start | bytes 1572872 | tf_op jit(solution)/shard_map/ppermute | solution.py:19
  386.5 41.0 %collective-permute-start.25 = (bf16[128,2048]{1,0:T(8,128)(2,1)}, bf16[128,2048]{1,0:T(8,128)(2,1)S(1)}, u32[]{:S(2)}, u32[]{:S(2)}) collective-permute-start(bf16[128,2048]{1,0:T(8,128)(2,1)} %get-tuple-element.33), channel_id=1, source_target_pairs={{0,64},{32,96},{64,0},{96,32},{1,65},{33,97},{65,1},{97,33},{2,66}... | collective-permute-start | bytes 1572872 | tf_op jit(solution)/shard_map/ppermute | solution.py:19
  393.8 46.3 %collective-permute-start.26 = (bf16[128,2048]{1,0:T(8,128)(2,1)}, bf16[128,2048]{1,0:T(8,128)(2,1)S(1)}, u32[]{:S(2)}, u32[]{:S(2)}) collective-permute-start(bf16[128,2048]{1,0:T(8,128)(2,1)} %get-tuple-element.34), channel_id=1, source_target_pairs={{0,96},{32,64},{64,32},{96,0},{1,97},{33,65},{65,33},{97,1},{2,98}... | collective-permute-start | bytes 1572872 | tf_op jit(solution)/shard_map/ppermute | solution.py:19
  (15 other events, 300.6 us)

commit v2 on v1

--- a/solution.py
+++ b/solution.py
@@ -21,14 +21,6 @@
 
 def plane_exchange(array):
     return lax.all_to_all(array, PLANE, split_axis=0, concat_axis=0, tiled=True)
-
-
-def ffn_rows(x, gate, up, down):
-    contract = (((1,), (1,)), ((), ()))
-    g = lax.dot_general(x, gate, contract, preferred_element_type=f32)
-    u = lax.dot_general(x, up, contract, preferred_element_type=f32)
-    hidden = (jax.nn.silu(g) * u).astype(bf16)
-    return jnp.dot(hidden, down, preferred_element_type=f32)
 
 
 def cast_kernel(place, gain, gate, up, down, out):
@@ -60,9 +52,20 @@
     )(place, gain, gate, up, down)
 
 
-def ffn_assemble_kernel(place, x, *refs, blocks, n_y, n_xc, own_hidden, cols):
+def hidden_rows(x, gate, up):
+    contract = (((1,), (1,)), ((), ()))
+    g = lax.dot_general(x, gate, contract, preferred_element_type=f32)
+    u = lax.dot_general(x, up, contract, preferred_element_type=f32)
+    return (jax.nn.silu(g) * u).astype(bf16)
+
+
+def down_rows(hidden, down):
+    return jnp.dot(hidden, down, preferred_element_type=f32).astype(bf16)
+
+
+def assemble_kernel(place, x, *refs, compute, blocks, matrices, n_y, n_xc, own_hidden, cols):
     parts, refs = refs[:blocks], refs[blocks:]
-    out, outs, held, sems = refs[0], refs[1:4], refs[4:7], refs[7]
+    out, outs, held, sems = refs[0], refs[1 : 1 + matrices], refs[1 + matrices : -1], refs[-1]
     step = pl.program_id(0)
     n_cols = held[0].shape[0]
 
@@ -71,9 +74,9 @@
             pltpu.make_async_copy(
                 held[m].at[f],
                 outs[m].at[0, :, pl.ds(f * cols, cols)],
-                sems.at[blocks * 3 * n_y + m * n_cols + f],
+                sems.at[blocks * matrices * n_y + m * n_cols + f],
             )
-            for m in range(3)
+            for m in range(matrices)
             for f in range(n_cols)
         ]
 
@@ -83,14 +86,14 @@
         for k in range(blocks):
             row = place[2 * k] * (n_y * own_hidden)
             col = place[2 * k + 1] * n_xc
-            for m in range(3):
+            for m in range(matrices):
                 for y in range(n_y):
                     at = pl.multiple_of(row + y * own_hidden, 8)
                     reads.append(
                         pltpu.make_async_copy(
                             parts[k].at[pl.ds(y * n_xc, n_xc), pl.ds(m * own_hidden, own_hidden)],
                             held[m].at[pl.ds(col, n_xc), pl.ds(at, own_hidden)],
-                            sems.at[(k * 3 + m) * n_y + y],
+                            sems.at[(k * matrices + m) * n_y + y],
                         )
                     )
         for r in reads:
@@ -100,10 +103,8 @@
         for w in writes():
             w.start()
 
-    gate, up, down = (
-        jnp.concatenate([held[m][f] for f in range(n_cols)], axis=1) for m in range(3)
-    )
-    out[...] = ffn_rows(x[...], gate, up, down).astype(bf16)
+    whole = [jnp.concatenate([h[f] for f in range(n_cols)], axis=1) for h in held]
+    out[...] = compute(x[...], *whole)
 
     @pl.when(step == pl.num_programs(0) - 1)
     def _():
@@ -111,8 +112,8 @@
             w.wait()
 
 
-def ffn_assemble(place, x, parts, n_y, n_xc, own_hidden, tile):
-    count, features = x.shape
+def assemble(compute, place, x, parts, matrices, features, width, n_y, n_xc, own_hidden, tile):
+    count, depth = x.shape
     cols = parts[0].shape[2]
     n_cols = features // cols
     hidden = len(parts) * n_y * n_xc * own_hidden * cols // features
@@ -121,56 +122,66 @@
     spec = pltpu.PrefetchScalarGridSpec(
         num_scalar_prefetch=1,
         grid=(count // tile,),
-        in_specs=[pl.BlockSpec((tile, features), lambda i, p: (i, 0))] + [hbm] * len(parts),
-        out_specs=[pl.BlockSpec((tile, features), lambda i, p: (i, 0))] + [hbm] * 3,
-        scratch_shapes=[pltpu.VMEM((n_cols, hidden, cols), bf16)] * 3
-        + [pltpu.SemaphoreType.DMA((len(parts) * 3 * n_y + 3 * n_cols,))],
+        in_specs=[pl.BlockSpec((tile, depth), lambda i, p: (i, 0))] + [hbm] * len(parts),
+        out_specs=[pl.BlockSpec((tile, width), lambda i, p: (i, 0))] + [hbm] * matrices,
+        scratch_shapes=[pltpu.VMEM((n_cols, hidden, cols), bf16)] * matrices
+        + [pltpu.SemaphoreType.DMA((len(parts) * matrices * n_y + matrices * n_cols,))],
     )
     return pl.pallas_call(
         functools.partial(
-            ffn_assemble_kernel,
+            assemble_kernel,
+            compute=compute,
             blocks=len(parts),
+            matrices=matrices,
             n_y=n_y,
             n_xc=n_xc,
             own_hidden=own_hidden,
             cols=cols,
         ),
         grid_spec=spec,
-        out_shape=[jax.ShapeDtypeStruct((count, features), bf16)] + [matrix] * 3,
-        cost_estimate=pl.CostEstimate(
-            flops=6 * count * hidden * features,
-            bytes_accessed=4 * count * features + 12 * hidden * features,
+        out_shape=[jax.ShapeDtypeStruct((count, width), bf16)] + [matrix] * matrices,
+        cost_estimate=pl.CostEstimate(
+            flops=2 * matrices * count * hidden * features,
+            bytes_accessed=4 * count * features + 4 * matrices * hidden * features,
             transcendentals=count * hidden,
         ),
-        name="ffn_assemble",
+        name="assemble",
     )(place, x, *parts)
 
 
-def ffn_kernel(x, gate, up, down, out):
-    out[...] = ffn_rows(x[...], gate[0], up[0], down[0]).astype(bf16)
-
-
-def ffn(x, gate, up, down, tile):
-    count, features = x.shape
-    hidden = gate.shape[1]
-    whole = pl.BlockSpec((1, hidden, features), lambda i: (0, 0, 0))
-    rows = pl.BlockSpec((tile, features), lambda i: (i, 0))
-    return pl.pallas_call(
-        ffn_kernel,
+def rows_kernel(x, *refs, compute):
+    refs[-1][...] = compute(x[...], *(r[0] for r in refs[:-1]))
+
+
+def over_rows(compute, x, matrices, width, tile):
+    count, depth = x.shape
+    whole = pl.BlockSpec(matrices[0].shape, lambda i: (0, 0, 0))
+    return pl.pallas_call(
+        functools.partial(rows_kernel, compute=compute),
         grid=(count // tile,),
-        in_specs=[rows, whole, whole, whole],
-        out_specs=rows,
-        out_shape=jax.ShapeDtypeStruct((count, features), bf16),
-        cost_estimate=pl.CostEstimate(
-            flops=6 * count * hidden * features,
-            bytes_accessed=4 * count * features + 6 * hidden * features,
-            transcendentals=count * hidden,
-        ),
-        name="ffn_rows",
-    )(x, gate, up, down)
+        in_specs=[pl.BlockSpec((tile, depth), lambda i: (i, 0))] + [whole] * len(matrices),
+        out_specs=pl.BlockSpec((tile, width), lambda i: (i, 0)),
+        out_shape=jax.ShapeDtypeStruct((count, width), bf16),
+        cost_estimate=pl.CostEstimate(
+            flops=2 * count * sum(m.size for m in matrices),
+            bytes_accessed=2 * count * (depth + width) + 2 * sum(m.size for m in matrices),
+            transcendentals=count,
+        ),
+        name="over_rows",
+    )(x, *matrices)
 
 
 def selection(metas, first, experts, top, capacity):
+    span = len(metas) * capacity
+    slot = jnp.arange(experts * span, dtype=jnp.int32)
+    within = (slot % span).astype(f32)
+    spread = (slot[:, None] // span == jnp.arange(experts, dtype=jnp.int32)[None, :]).astype(bf16)
+
+    def by_token(values):
+        return lax.dot_general(
+            values, spread, (((0,), (1,)), ((), ())), preferred_element_type=f32
+        )
+
     codes, weights = [], []
     for k, meta in enumerate(metas):
         names = meta[:top] - first.astype(f32)
@@ -180,26 +191,15 @@
         n = chosen.shape[1]
         before = (jnp.arange(n)[:, None] < jnp.arange(n)[None, :]).astype(bf16)
         place = jnp.dot(chosen.astype(bf16), before, preferred_element_type=f32)
-        codes.append(jnp.where(chosen > 0, place + float(k * capacity), -1.0))
-        weights.append(weight)
-    code = jnp.concatenate(codes, axis=1).astype(bf16)
-    weight = jnp.concatenate(weights, axis=1)
-    high = weight.astype(bf16)
-    low = (weight - high.astype(f32)).astype(bf16)
-    span = len(metas) * capacity
-    slot = jnp.arange(experts * span, dtype=jnp.int32)
-    within = (slot % span).astype(f32)
-    spread = (slot[:, None] // span == jnp.arange(experts, dtype=jnp.int32)[None, :]).astype(bf16)
-
-    def by_token(values):
-        return lax.dot_general(
-            values, spread, (((0,), (1,)), ((), ())), preferred_element_type=f32
-        )
-
-    held = by_token(code) == within[None, :]
-    high = jnp.where(held, by_token(high), 0.0).astype(bf16)
-    low = jnp.where(held, by_token(low), 0.0).astype(bf16)
-    return code, high, low
+        code = jnp.where(chosen > 0, place + float(k * capacity), -1.0).astype(bf16)
+        high = weight.astype(bf16)
+        low = (weight - high.astype(f32)).astype(bf16)
+        held = by_token(code) == within[None, :]
+        high = jnp.where(held, by_token(high), 0.0).astype(bf16)
+        low = jnp.where(held, by_token(low), 0.0).astype(bf16)
+        codes.append(code)
+        weights.append((high, low))
+    return jnp.concatenate(codes, axis=1), weights
 
 
 def pick_kernel(code, one, two, out, *, span, tile):
@@ -263,17 +263,16 @@
     )(place, stack)
 
 
-def combine_kernel(high, low, back, hidden, down, one, two):
+def combine_kernel(high, low, back, hidden, down, out):
     rows = back[...]
     total = jnp.dot(high[...], rows, preferred_element_type=f32)
     total += jnp.dot(low[...], rows, preferred_element_type=f32)
     total += jnp.dot(hidden[...], down[...], preferred_element_type=f32)
-    n = one.shape[0]
-    one[...] = total[:n].astype(one.dtype)
-    two[...] = total[n:].astype(two.dtype)
-
-
-def combine(high, low, back, hidden, down, dtypes, tile):
+    out[...] = total.astype(out.dtype)
+
+
+def combine(weights, back, hidden, down, dtype, tile):
+    high, low = weights
     count, slots = high.shape
     features = back.shape[1]
     units = hidden.shape[1]
@@ -289,8 +288,8 @@
             whole(count, units),
             part(units),
         ],
-        out_specs=[part(count // 2)] * 2,
-        out_shape=[jax.ShapeDtypeStruct((count // 2, features), d) for d in dtypes],
+        out_specs=part(count),
+        out_shape=jax.ShapeDtypeStruct((count, features), dtype),
         cost_estimate=pl.CostEstimate(
             flops=2 * count * features * (2 * slots + units),
             bytes_accessed=4 * count * slots + 2 * slots * features + 4 * count * features,
@@ -342,8 +341,15 @@
     sent = cast(place, norm_gain[None, :], gate_trained, up_trained, down_trained, n_plane)
     landed = plane_exchange(sent)
     piece = 3 * own_hidden
-    moved = [landed[:, j * piece : (j + 1) * piece] for j in range(n_zl)]
-    parts = [moved[0]] + [swapped(moved[k % n_zl], ("gr", "zl"), n_gr * n_zl, k) for k in steps[1:]]
+
+    def spread(begin, end):
+        moved = [landed[:, j * piece + begin : j * piece + end] for j in range(n_zl)]
+        return [moved[0]] + [
+            swapped(moved[k % n_zl], ("gr", "zl"), n_gr * n_zl, k) for k in steps[1:]
+        ]
+
+    first_parts = spread(0, 2 * own_hidden)
+    down_parts = spread(2 * own_hidden, piece)
 
     first = zl * n_plane
     near_picks = selection(metas[:2], first, n_plane, top, capacity)
@@ -360,53 +366,42 @@
     laid = [shared] + [swapped(shared, ("x", "c"), n_xc, k) for k in range(1, n_xc)]
     across = (lax.axis_index("x") * lax.axis_size("c") + lax.axis_index("c"))[None]
     own = lay(across.astype(jnp.int32), jnp.stack(laid))
-    quarter = jnp.concatenate([own] + [swapped(own, "y", n_y, k) for k in range(1, n_y)], axis=1)
+    columns = [own] + [swapped(own, "y", n_y, k) for k in range(1, n_y)]
     shared_out = [own[m] for m in range(3)]
 
-    def shared_hidden(pair):
-        contract = (((1,), (1,)), ((), ()))
-        done = []
-        for rows in pair:
-            g = lax.dot_general(rows, quarter[0], contract, preferred_element_type=f32)
-            u = lax.dot_general(rows, quarter[1], contract, preferred_element_type=f32)
-            done.append((jax.nn.silu(g) * u).astype(bf16))
-        return jnp.concatenate(done, axis=0)
-
-    near_hidden = shared_hidden(blocks[:2])
-    far_hidden = shared_hidden(blocks[2:])
-    shared_down = quarter[2]
-    far_in, near_hidden, far_hidden, shared_down = lax.optimization_barrier(
-        (far_in, near_hidden, far_hidden, shared_down)
-    )
-
-    far_result, expert_gate, expert_up, expert_down = ffn_assemble(
-        place, far_in.reshape(-1, features), parts, n_y, n_xc, own_hidden, 256
-    )
+    hidden = own_hidden * n_zl * n_y
+    sizes = (features, hidden, n_y, n_xc, own_hidden, 256)
+    near_units, expert_gate, expert_up = assemble(
+        hidden_rows, place, near_in.reshape(-1, features), first_parts, 2, *sizes
+    )
+    far_units = over_rows(
+        hidden_rows, far_in.reshape(-1, features), (expert_gate, expert_up), hidden, 256
+    )
+    far_units, near_weights, far_weights = lax.optimization_barrier(
+        (far_units, near_picks[1], far_picks[1])
+    )
+    sizes = (features, features, n_y, n_xc, own_hidden, 256)
+    far_result, expert_down = assemble(down_rows, place, far_units, down_parts, 1, *sizes)
     far_back = plane_exchange(far_result.reshape(n_plane, 2 * capacity, features))
-    near_result = ffn(
-        near_in.reshape(-1, features), expert_gate, expert_up, expert_down, 256
-    )
+    near_result = over_rows(down_rows, near_units, (expert_down,), features, 256)
     near_back = plane_exchange(near_result.reshape(n_plane, 2 * capacity, features))
 
-    third, fourth = combine(
-        *far_picks[1:],
-        far_back.reshape(-1, features),
-        far_hidden,
-        shared_down,
-        (bf16, bf16),
-        512,
-    )
-    third = swapped(third, "zl", n_zl, 2)
-    fourth = swapped(fourth, "zl", n_zl, 3)
-    kept, second = combine(
-        *near_picks[1:],
-        near_back.reshape(-1, features),
-        near_hidden,
-        shared_down,
-        (f32, bf16),
-        512,
-    )
-    second = swapped(second, "zl", n_zl, 1)
+    columns, _ = lax.optimization_barrier((columns, far_result))
+    quarter = jnp.concatenate(columns, axis=1)
+    units = [hidden_rows(rows, quarter[0], quarter[1]) for rows in blocks]
+    far_back = far_back.reshape(-1, features)
+    near_back = near_back.reshape(-1, features)
+
+    third, fourth = (
+        swapped(
+            combine(far_weights[k - 2], far_back, units[k], quarter[2], bf16, 512), "zl", n_zl, k
+        )
+        for k in (2, 3)
+    )
+    second = swapped(
+        combine(near_weights[1], near_back, units[1], quarter[2], bf16, 512), "zl", n_zl, 1
+    )
+    kept = combine(near_weights[0], near_back, units[0], quarter[2], f32, 512)
     combined = (
         kept + second.astype(f32) + third.astype(f32) + fourth.astype(f32)
     ).astype(bf16)

time: 446 us -> 411 us (0.922)
  the two profiles are of different devices: /device:TPU:77 before, /device:TPU:16 now
where the time goes in v2:
time: 411 us; the launch traced here: 409 us
  waiting for transfers between devices  182 us (44%)
  starting transfers between devices  126 us (31%)
  Pallas kernels  63.5 us (15%)
  matrix products  17.9 us (4%)
  local copies, waits for them, and re-layouts  13.2 us (3%)
  other arithmetic  5.68 us (1%)
    ppermute x34, waiting for transfers between devices, swapped(): return lax.ppermute(array, axis, [(r, r ^ k) for r in range(size)])  156 us
    ppermute x34, starting transfers between devices, swapped(): return lax.ppermute(array, axis, [(r, r ^ k) for r in range(size)])  87.5 us
    all_to_all x5, starting transfers between devices, plane_exchange(): return lax.all_to_all(array, PLANE, split_axis=0, concat_axis=0, tiled=True)  38.1 us
    all_to_all x5, waiting for transfers between devices, plane_exchange(): return lax.all_to_all(array, PLANE, split_axis=0, concat_axis=0, tiled=True)  26.1 us
    pallas_call x4, Pallas kernels, combine(): pl.pallas_call(combine_kernel, grid=(features // tile,), in_specs=[whole(...  18.8 us
    pallas_call x2, Pallas kernels, assemble(): pl.pallas_call(functools.partial(assemble_kernel, compute=compute, blocks...  16.2 us
    pallas_call x2, Pallas kernels, over_rows(): pl.pallas_call(functools.partial(rows_kernel, compute=compute), grid=(cou...  11.8 us
    dot_general x12, matrix products, by_token(): lax.dot_general(values, spread, (((0,), (1,)), ((), ())), preferred_eleme...  10.3 us
  transfers between devices with their start and end apart: 39, of which 21 were waited for; matrix products, arithmetic and copies ran while one was open for 7% of the time, Pallas kernels for 13%

profile of v2, /device:TPU:16, one launch (start us, length us, event | category | flops | bytes accessed | tf_op | source)
XLA Modules:
  0.0 409.1 jit_solution(6408724179321301786)
XLA Ops:
  1.3 5.1 %cast.1 = bf16[32,288,128]{2,1,0:T(8,128)(2,1)} custom-call(s32[16]{0:T(128)} %stack.106.place, f32[1,128]{1,0:T(1,128)} %bitcast.99, f32[128,24,128]{2,1,0:T(8,128)} %gate.1, f32[128,24,128]{2,1,0:T(8,128)} %up.1, f32[128,24,128]{2,1,0:T(8,128)} %down.1), custom_call_target="tpu_custom_call" | custom-call | flops 1179648 | bytes 7077888 | tf_op jit(solution)/shard_map/cast/pallas_call | solution.py:44
  6.5 7.6 %all-to-all-start = ((bf16[32,288,128]{2,1,0:T(8,128)(2,1)}), bf16[32,288,128]{2,1,0:T(8,128)(2,1)S(1)}, u32[]{:S(2)}, u32[]{:S(2)}) async-start(bf16[32,288,128]{2,1,0:T(8,128)(2,1)} %cast.1), calls=%async_computation | async-start | bytes 4718592 | tf_op jit(solution)/shard_map/all_to_all | solution.py:23
  18.6 11.6 %collective-permute-done.5.two = bf16[128,2048]{1,0:T(8,128)(2,1)S(1)} collective-permute-done((bf16[128,2048]{1,0:T(8,128)(2,1)S(1)}, bf16[128,2048]{1,0:T(8,128)(2,1)S(1)}, u32[]{:S(2)}, u32[]{:S(2)}) %collective-permute-start.5) | collective-permute-done | bytes 524320 | tf_op jit(solution)/shard_map/ppermute | solution.py:19
  31.0 4.9 %pick.3 = bf16[768,2048]{1,0:T(8,128)(2,1)} custom-call(bf16[32,256]{1,0:T(8,128)(2,1)} %pad_maximum_fusion.2.code, bf16[128,2048]{1,0:T(8,128)(2,1)} %copy-done.1, bf16[128,2048]{1,0:T(8,128)(2,1)} %copy-done.6), custom_call_target="tpu_custom_call" | custom-call | flops 805306368 | bytes 4194304 | tf_op jit(solution)/shard_map/pick/pallas_call | solution.py:224
  35.9 9.0 %all-to-all-done = bf16[32,288,128]{2,1,0:T(8,128)(2,1)S(1)} async-done(((bf16[32,288,128]{2,1,0:T(8,128)(2,1)}), bf16[32,288,128]{2,1,0:T(8,128)(2,1)S(1)}, u32[]{:S(2)}, u32[]{:S(2)}) %all-to-all-start) | async-done | bytes 2359328 | tf_op jit(solution)/shard_map/all_to_all | solution.py:23
  44.9 7.2 %all-to-all-start.1 = ((bf16[32,24,2048]{2,1,0:T(8,128)(2,1)}), bf16[32,24,2048]{2,1,0:T(8,128)(2,1)}, u32[]{:S(2)}, u32[]{:S(2)}) async-start(bf16[32,24,2048]{2,1,0:T(8,128)(2,1)} %bitcast.92), calls=%async_computation.1 | async-start | bytes 6291456 | tf_op jit(solution)/shard_map/all_to_all | solution.py:23
  60.9 22.1 %collective-permute-done = f32[16,128]{1,0:T(8,128)S(1)} collective-permute-done((f32[16,128]{1,0:T(8,128)S(1)}, f32[16,128]{1,0:T(8,128)S(1)}, u32[]{:S(2)}, u32[]{:S(2)}) %collective-permute-start) | collective-permute-done | bytes 8224 | tf_op jit(solution)/shard_map/ppermute | solution.py:19
  83.9 10.3 %collective-permute-done.2.one = bf16[128,2048]{1,0:T(8,128)(2,1)S(1)} collective-permute-done((bf16[128,2048]{1,0:T(8,128)(2,1)S(1)}, bf16[128,2048]{1,0:T(8,128)(2,1)S(1)}, u32[]{:S(2)}, u32[]{:S(2)}) %collective-permute-start.2) | collective-permute-done | bytes 524320 | tf_op jit(solution)/shard_map/ppermute | solution.py:19
  95.0 4.8 %pick.2 = bf16[768,2048]{1,0:T(8,128)(2,1)} custom-call(bf16[32,256]{1,0:T(8,128)(2,1)} %pad_maximum_fusion.1.code, bf16[128,2048]{1,0:T(8,128)(2,1)} %copy-done.8, bf16[128,2048]{1,0:T(8,128)(2,1)} %collective-permute-done.3.two), custom_call_target="tpu_custom_call" | custom-call | flops 805306368 | bytes 4194304 | tf_op jit(solution)/shard_map/pick/pallas_call | solution.py:224
  99.9 7.6 %all-to-all-start.2 = ((bf16[32,24,2048]{2,1,0:T(8,128)(2,1)}), bf16[32,24,2048]{2,1,0:T(8,128)(2,1)}, u32[]{:S(2)}, u32[]{:S(2)}) async-start(bf16[32,24,2048]{2,1,0:T(8,128)(2,1)} %bitcast.91), calls=%async_computation.2 | async-start | bytes 6291456 | tf_op jit(solution)/shard_map/all_to_all | solution.py:23
  114.5 11.0 %collective-permute-start.6 = (bf16[32,48,128]{2,1,0:T(8,128)(2,1)S(1)}, bf16[32,48,128]{2,1,0:T(8,128)(2,1)S(1)}, u32[]{:S(2)}, u32[]{:S(2)}) collective-permute-start(bf16[32,48,128]{2,1,0:T(8,128)(2,1)S(1)} %get-tuple-element.61), channel_id=1, source_target_pairs={{0,32},{32,0},{64,96},{96,64},{128,160},{160,128},{192,224},{224,1... | collective-permute-start | bytes 1179656 | tf_op jit(solution)/shard_map/ppermute | solution.py:19
  126.9 5.7 %collective-permute-start.10 = (bf16[32,48,128]{2,1,0:T(8,128)(2,1)S(1)}, bf16[32,48,128]{2,1,0:T(8,128)(2,1)S(1)}, u32[]{:S(2)}, u32[]{:S(2)}) collective-permute-start(bf16[32,48,128]{2,1,0:T(8,128)(2,1)S(1)} %get-tuple-element.61), channel_id=1, source_target_pairs={{0,160},{32,128},{64,224},{96,192},{128,32},{160,0},{192,96},{224,... | collective-permute-start | bytes 1179656 | tf_op jit(solution)/shard_map/ppermute | solution.py:19
  134.6 13.2 %collective-permute-done.6.refs_1_ = bf16[32,48,128]{2,1,0:T(8,128)(2,1)S(1)} collective-permute-done((bf16[32,48,128]{2,1,0:T(8,128)(2,1)S(1)}, bf16[32,48,128]{2,1,0:T(8,128)(2,1)S(1)}, u32[]{:S(2)}, u32[]{:S(2)}) %collective-permute-start.6) | collective-permute-done | bytes 393248 | tf_op jit(solution)/shard_map/ppermute | solution.py:19
  147.7 14.7 %collective-permute-done.7.refs_2_ = bf16[32,48,128]{2,1,0:T(8,128)(2,1)S(1)} collective-permute-done((bf16[32,48,128]{2,1,0:T(8,128)(2,1)S(1)}, bf16[32,48,128]{2,1,0:T(8,128)(2,1)S(1)}, u32[]{:S(2)}, u32[]{:S(2)}) %collective-permute-start.7) | collective-permute-done | bytes 393248 | tf_op jit(solution)/shard_map/ppermute | solution.py:19
  164.3 10.4 %collective-permute-done.8.refs_3_ = bf16[32,48,128]{2,1,0:T(8,128)(2,1)S(1)} collective-permute-done((bf16[32,48,128]{2,1,0:T(8,128)(2,1)S(1)}, bf16[32,48,128]{2,1,0:T(8,128)(2,1)S(1)}, u32[]{:S(2)}, u32[]{:S(2)}) %collective-permute-start.8) | collective-permute-done | bytes 393248 | tf_op jit(solution)/shard_map/ppermute | solution.py:19
  174.7 21.1 %collective-permute-start.13 = (bf16[32,24,128]{2,1,0:T(8,128)(2,1)S(1)}, bf16[32,24,128]{2,1,0:T(8,128)(2,1)S(1)}, u32[]{:S(2)}, u32[]{:S(2)}) collective-permute-start(bf16[32,24,128]{2,1,0:T(8,128)(2,1)S(1)} %get-tuple-element.57), channel_id=1, source_target_pairs={{0,32},{32,0},{64,96},{96,64},{128,160},{160,128},{192,224},{224,1... | collective-permute-start | bytes 589832 | tf_op jit(solution)/shard_map/ppermute | solution.py:19
  205.9 9.2 %assemble.2 = (bf16[768,384]{1,0:T(8,128)(2,1)}, bf16[1,384,2048]{2,1,0:T(8,128)(2,1)}, bf16[1,384,2048]{2,1,0:T(8,128)(2,1)}) custom-call(s32[16]{0:T(128)} %stack.106.place, bf16[768,2048]{1,0:T(8,128)(2,1)} %bitcast.12.x, bf16[32,48,128]{2,1,0:T(8,128)(2,1)} %copy-done.11, bf16[32,48,128]{2,1,0:T(8,128)(2,1)} %copy-done.20, ...), custom_call_target="tpu_custom_call" | custom-call | flops 2415919104 | bytes 12582912 | tf_op jit(solution)/shard_map/assemble/pallas_call | solution.py:130
  217.0 5.2 %collective-permute-done.14.refs_2_ = bf16[32,24,128]{2,1,0:T(8,128)(2,1)S(1)} collective-permute-done((bf16[32,24,128]{2,1,0:T(8,128)(2,1)S(1)}, bf16[32,24,128]{2,1,0:T(8,128)(2,1)S(1)}, u32[]{:S(2)}, u32[]{:S(2)}) %collective-permute-start.14) | collective-permute-done | bytes 196640 | tf_op jit(solution)/shard_map/ppermute | solution.py:19
  222.2 5.8 %collective-permute-start.16 = (bf16[32,24,128]{2,1,0:T(8,128)(2,1)S(1)}, bf16[32,24,128]{2,1,0:T(8,128)(2,1)S(1)}, u32[]{:S(2)}, u32[]{:S(2)}) collective-permute-start(bf16[32,24,128]{2,1,0:T(8,128)(2,1)S(1)} %get-tuple-element.58.refs_0_), channel_id=1, source_target_pairs={{0,128},{32,160},{64,192},{96,224},{128,0},{160,32},{192,64},{224,... | collective-permute-start | bytes 589832 | tf_op jit(solution)/shard_map/ppermute | solution.py:19
  228.0 6.7 %over_rows.2.x = bf16[768,384]{1,0:T(8,128)(2,1)} custom-call(bf16[768,2048]{1,0:T(8,128)(2,1)} %bitcast.11.x, bf16[1,384,2048]{2,1,0:T(8,128)(2,1)} %get-tuple-element.21.refs_0_, bf16[1,384,2048]{2,1,0:T(8,128)(2,1)} %get-tuple-element.22.refs_1_), custom_call_target="tpu_custom_call" | custom-call | flops 2415919104 | bytes 6881280 | tf_op jit(solution)/shard_map/over_rows/pallas_call | solution.py:159
  238.3 7.0 %assemble.3 = (bf16[768,2048]{1,0:T(8,128)(2,1)}, bf16[1,384,2048]{2,1,0:T(8,128)(2,1)}) custom-call(s32[16]{0:T(128)} %stack.106.place, bf16[768,384]{1,0:T(8,128)(2,1)} %over_rows.2.x, bf16[32,24,128]{2,1,0:T(8,128)(2,1)} %copy-done.12, bf16[32,24,128]{2,1,0:T(8,128)(2,1)} %copy-done.27, bf16[32,24,128]{2,1,0:T(8,128)(2,1)} %copy-done.29, ...), custom_call_target="tpu_custom_call" | custom-call | flops 1207959552 | bytes 9437184 | tf_op jit(solution)/shard_map/assemble/pallas_call | solution.py:130
  245.3 7.5 %all-to-all-start.4 = ((bf16[32,24,2048]{2,1,0:T(8,128)(2,1)}), bf16[32,24,2048]{2,1,0:T(8,128)(2,1)S(1)}, u32[]{:S(2)}, u32[]{:S(2)}) async-start(bf16[32,24,2048]{2,1,0:T(8,128)(2,1)} %bitcast.94), calls=%async_computation.4 | async-start | bytes 6291456 | tf_op jit(solution)/shard_map/all_to_all | solution.py:23
  253.0 5.1 %collective-permute-start.20 = (bf16[3,32,128]{2,1,0:T(8,128)(2,1)S(1)}, bf16[3,32,128]{2,1,0:T(8,128)(2,1)S(1)}, u32[]{:S(2)}, u32[]{:S(2)}) collective-permute-start(bf16[3,32,128]{2,1,0:T(8,128)(2,1)S(1)} %pad_maximum_fusion), channel_id=1, source_target_pairs={{0,128},{128,0},{1,129},{129,1},{2,130},{130,2},{3,131},{131,3},{4... | collective-permute-start | bytes 73736 | tf_op jit(solution)/shard_map/ppermute | solution.py:19
  269.6 21.5 %collective-permute-done.22 = bf16[2,3,32,128]{3,2,1,0:T(8,128)(2,1)S(1)} collective-permute-done((bf16[2,3,32,128]{3,2,1,0:T(8,128)(2,1)S(1)}, bf16[2,3,32,128]{3,2,1,0:T(8,128)(2,1)S(1)}, u32[]{:S(2)}, u32[]{:S(2)}) %collective-permute-start.22) | collective-permute-done | bytes 49184 | tf_op jit(solution)/shard_map/ppermute | solution.py:19
  305.4 7.0 %collective-permute-done.28 = bf16[3,32,2048]{2,1,0:T(8,128)(2,1)} collective-permute-done((bf16[3,32,2048]{2,1,0:T(8,128)(2,1)}, bf16[3,32,2048]{2,1,0:T(8,128)(2,1)}, u32[]{:S(2)}, u32[]{:S(2)}) %collective-permute-start.28) | collective-permute-done | bytes 393248 | tf_op jit(solution)/shard_map/ppermute | solution.py:19
  312.5 8.2 %collective-permute-done.29 = bf16[3,32,2048]{2,1,0:T(8,128)(2,1)} collective-permute-done((bf16[3,32,2048]{2,1,0:T(8,128)(2,1)}, bf16[3,32,2048]{2,1,0:T(8,128)(2,1)}, u32[]{:S(2)}, u32[]{:S(2)}) %collective-permute-start.29) | collective-permute-done | bytes 393248 | tf_op jit(solution)/shard_map/ppermute | solution.py:19
  322.1 5.1 %over_rows.3 = bf16[768,2048]{1,0:T(8,128)(2,1)} custom-call(bf16[768,384]{1,0:T(8,128)(2,1)} %get-tuple-element.33.x, bf16[1,384,2048]{2,1,0:T(8,128)(2,1)} %get-tuple-element.23.refs_0_), custom_call_target="tpu_custom_call" | custom-call | flops 1207959552 | bytes 5308416 | tf_op jit(solution)/shard_map/over_rows/pallas_call | solution.py:159
  328.9 8.2 %all-to-all-start.3 = ((bf16[32,24,2048]{2,1,0:T(8,128)(2,1)}), bf16[32,24,2048]{2,1,0:T(8,128)(2,1)}, u32[]{:S(2)}, u32[]{:S(2)}) async-start(bf16[32,24,2048]{2,1,0:T(8,128)(2,1)} %bitcast.93), calls=%async_computation.3 | async-start | bytes 6291456 | tf_op jit(solution)/shard_map/all_to_all | solution.py:23
  359.8 17.1 %all-to-all-done.3 = bf16[32,24,2048]{2,1,0:T(8,128)(2,1)} async-done(((bf16[32,24,2048]{2,1,0:T(8,128)(2,1)}), bf16[32,24,2048]{2,1,0:T(8,128)(2,1)}, u32[]{:S(2)}, u32[]{:S(2)}) %all-to-all-start.3) | async-done | bytes 3145760 | tf_op jit(solution)/shard_map/all_to_all | solution.py:23
  384.6 4.7 %combine.4 = f32[128,2048]{1,0:T(8,128)} custom-call(bf16[128,768]{1,0:T(8,128)(2,1)} %fusion.high, bf16[128,768]{1,0:T(8,128)(2,1)} %fusion.1.low, bf16[768,2048]{1,0:T(8,128)(2,1)} %bitcast.14.back, bf16[128,128]{1,0:T(8,128)(2,1)} %fusion.8.hidden, bf16[128,2048]{1,0:T(8,128)(2,1)} %slice_bitcast_fusion.down), custom_call_target="tpu_custom_call" | custom-call | flops 872415232 | bytes 4587520 | tf_op jit(solution)/shard_map/combine/pallas_call | solution.py:281
  389.3 11.7 %collective-permute-done.32 = bf16[128,2048]{1,0:T(8,128)(2,1)S(1)} collective-permute-done((bf16[128,2048]{1,0:T(8,128)(2,1)}, bf16[128,2048]{1,0:T(8,128)(2,1)S(1)}, u32[]{:S(2)}, u32[]{:S(2)}) %collective-permute-start.32) | collective-permute-done | bytes 524320 | tf_op jit(solution)/shard_map/ppermute | solution.py:19
  401.0 5.6 %collective-permute-done.31 = bf16[128,2048]{1,0:T(8,128)(2,1)} collective-permute-done((bf16[128,2048]{1,0:T(8,128)(2,1)}, bf16[128,2048]{1,0:T(8,128)(2,1)}, u32[]{:S(2)}, u32[]{:S(2)}) %collective-permute-start.31) | collective-permute-done | bytes 524320 | tf_op jit(solution)/shard_map/ppermute | solution.py:19
  (192 shorter events, 105.9 us)
Async XLA Ops:
  6.5 38.4 %all-to-all-start = ((bf16[32,288,128]{2,1,0:T(8,128)(2,1)}), bf16[32,288,128]{2,1,0:T(8,128)(2,1)S(1)}, u32[]{:S(2)}, u32[]{:S(2)}) async-start(bf16[32,288,128]{2,1,0:T(8,128)(2,1)} %cast.1), calls=%async_computation | async-start | bytes 4718592 | tf_op jit(solution)/shard_map/all_to_all | solution.py:23
  44.9 55.0 %all-to-all-start.1 = ((bf16[32,24,2048]{2,1,0:T(8,128)(2,1)}), bf16[32,24,2048]{2,1,0:T(8,128)(2,1)}, u32[]{:S(2)}, u32[]{:S(2)}) async-start(bf16[32,24,2048]{2,1,0:T(8,128)(2,1)} %bitcast.92), calls=%async_computation.1 | async-start | bytes 6291456 | tf_op jit(solution)/shard_map/all_to_all | solution.py:23
  56.8 26.2 %collective-permute-start = (f32[16,128]{1,0:T(8,128)S(1)}, f32[16,128]{1,0:T(8,128)S(1)}, u32[]{:S(2)}, u32[]{:S(2)}) collective-permute-start(f32[16,128]{1,0:T(8,128)S(1)} %pad_maximum_fusion.3), channel_id=1, source_target_pairs={{0,64},{32,96},{64,0},{96,32},{1,65},{33,97},{65,1},{97,33},{2,66}... | collective-permute-start | bytes 24584 | tf_op jit(solution)/shard_map/ppermute | solution.py:19
  56.8 37.4 %collective-permute-start.2 = (bf16[128,2048]{1,0:T(8,128)(2,1)S(1)}, bf16[128,2048]{1,0:T(8,128)(2,1)S(1)}, u32[]{:S(2)}, u32[]{:S(2)}) collective-permute-start(bf16[128,2048]{1,0:T(8,128)(2,1)S(1)} %copy-done.2), channel_id=1, source_target_pairs={{0,64},{32,96},{64,0},{96,32},{1,65},{33,97},{65,1},{97,33},{2,66}... | collective-permute-start | bytes 1572872 | tf_op jit(solution)/shard_map/ppermute | solution.py:19
  59.7 34.5 %collective-permute-start.3 = (bf16[128,2048]{1,0:T(8,128)(2,1)S(1)}, bf16[128,2048]{1,0:T(8,128)(2,1)}, u32[]{:S(2)}, u32[]{:S(2)}) collective-permute-start(bf16[128,2048]{1,0:T(8,128)(2,1)S(1)} %copy-done.2), channel_id=1, source_target_pairs={{0,96},{32,64},{64,32},{96,0},{1,97},{33,65},{65,33},{97,1},{2,98}... | collective-permute-start | bytes 1572872 | tf_op jit(solution)/shard_map/ppermute | solution.py:19
  99.9 128.2 %all-to-all-start.2 = ((bf16[32,24,2048]{2,1,0:T(8,128)(2,1)}), bf16[32,24,2048]{2,1,0:T(8,128)(2,1)}, u32[]{:S(2)}, u32[]{:S(2)}) async-start(bf16[32,24,2048]{2,1,0:T(8,128)(2,1)} %bitcast.91), calls=%async_computation.2 | async-start | bytes 6291456 | tf_op jit(solution)/shard_map/all_to_all | solution.py:23
  114.5 33.3 %collective-permute-start.6 = (bf16[32,48,128]{2,1,0:T(8,128)(2,1)S(1)}, bf16[32,48,128]{2,1,0:T(8,128)(2,1)S(1)}, u32[]{:S(2)}, u32[]{:S(2)}) collective-permute-start(bf16[32,48,128]{2,1,0:T(8,128)(2,1)S(1)} %get-tuple-element.61), channel_id=1, source_target_pairs={{0,32},{32,0},{64,96},{96,64},{128,160},{160,128},{192,224},{224,1... | collective-permute-start | bytes 1179656 | tf_op jit(solution)/shard_map/ppermute | solution.py:19
  125.4 36.9 %collective-permute-start.7 = (bf16[32,48,128]{2,1,0:T(8,128)(2,1)S(1)}, bf16[32,48,128]{2,1,0:T(8,128)(2,1)S(1)}, u32[]{:S(2)}, u32[]{:S(2)}) collective-permute-start(bf16[32,48,128]{2,1,0:T(8,128)(2,1)S(1)} %get-tuple-element.60), channel_id=1, source_target_pairs={{0,64},{32,96},{64,0},{96,32},{128,192},{160,224},{192,128},{224,1... | collective-permute-start | bytes 1179656 | tf_op jit(solution)/shard_map/ppermute | solution.py:19
  126.9 73.3 %collective-permute-start.10 = (bf16[32,48,128]{2,1,0:T(8,128)(2,1)S(1)}, bf16[32,48,128]{2,1,0:T(8,128)(2,1)S(1)}, u32[]{:S(2)}, u32[]{:S(2)}) collective-permute-start(bf16[32,48,128]{2,1,0:T(8,128)(2,1)S(1)} %get-tuple-element.61), channel_id=1, source_target_pairs={{0,160},{32,128},{64,224},{96,192},{128,32},{160,0},{192,96},{224,... | collective-permute-start | bytes 1179656 | tf_op jit(solution)/shard_map/ppermute | solution.py:19
  132.6 70.0 %collective-permute-start.11 = (bf16[32,48,128]{2,1,0:T(8,128)(2,1)S(1)}, bf16[32,48,128]{2,1,0:T(8,128)(2,1)S(1)}, u32[]{:S(2)}, u32[]{:S(2)}) collective-permute-start(bf16[32,48,128]{2,1,0:T(8,128)(2,1)S(1)} %get-tuple-element.60), channel_id=1, source_target_pairs={{0,192},{32,224},{64,128},{96,160},{128,64},{160,96},{192,0},{224,... | collective-permute-start | bytes 1179656 | tf_op jit(solution)/shard_map/ppermute | solution.py:19
  132.6 42.0 %collective-permute-start.8 = (bf16[32,48,128]{2,1,0:T(8,128)(2,1)S(1)}, bf16[32,48,128]{2,1,0:T(8,128)(2,1)S(1)}, u32[]{:S(2)}, u32[]{:S(2)}) collective-permute-start(bf16[32,48,128]{2,1,0:T(8,128)(2,1)S(1)} %get-tuple-element.59), channel_id=1, source_target_pairs={{0,96},{32,64},{64,32},{96,0},{128,224},{160,192},{192,160},{224,1... | collective-permute-start | bytes 1179656 | tf_op jit(solution)/shard_map/ppermute | solution.py:19
  147.7 56.2 %collective-permute-start.12 = (bf16[32,48,128]{2,1,0:T(8,128)(2,1)S(1)}, bf16[32,48,128]{2,1,0:T(8,128)(2,1)S(1)}, u32[]{:S(2)}, u32[]{:S(2)}) collective-permute-start(bf16[32,48,128]{2,1,0:T(8,128)(2,1)S(1)} %get-tuple-element.59), channel_id=1, source_target_pairs={{0,224},{32,192},{64,160},{96,128},{128,96},{160,64},{192,32},{224... | collective-permute-start | bytes 1179656 | tf_op jit(solution)/shard_map/ppermute | solution.py:19
  162.4 36.8 %collective-permute-start.9 = (bf16[32,48,128]{2,1,0:T(8,128)(2,1)S(1)}, bf16[32,48,128]{2,1,0:T(8,128)(2,1)S(1)}, u32[]{:S(2)}, u32[]{:S(2)}) collective-permute-start(bf16[32,48,128]{2,1,0:T(8,128)(2,1)S(1)} %get-tuple-element.62.refs_0_), channel_id=1, source_target_pairs={{0,128},{32,160},{64,192},{96,224},{128,0},{160,32},{192,64},{224,... | collective-permute-start | bytes 1179656 | tf_op jit(solution)/shard_map/ppermute | solution.py:19
  174.7 40.4 %collective-permute-start.13 = (bf16[32,24,128]{2,1,0:T(8,128)(2,1)S(1)}, bf16[32,24,128]{2,1,0:T(8,128)(2,1)S(1)}, u32[]{:S(2)}, u32[]{:S(2)}) collective-permute-start(bf16[32,24,128]{2,1,0:T(8,128)(2,1)S(1)} %get-tuple-element.57), channel_id=1, source_target_pairs={{0,32},{32,0},{64,96},{96,64},{128,160},{160,128},{192,224},{224,1... | collective-permute-start | bytes 589832 | tf_op jit(solution)/shard_map/ppermute | solution.py:19
  199.2 37.6 %collective-permute-start.17 = (bf16[32,24,128]{2,1,0:T(8,128)(2,1)S(1)}, bf16[32,24,128]{2,1,0:T(8,128)(2,1)S(1)}, u32[]{:S(2)}, u32[]{:S(2)}) collective-permute-start(bf16[32,24,128]{2,1,0:T(8,128)(2,1)S(1)} %get-tuple-element.57), channel_id=1, source_target_pairs={{0,160},{32,128},{64,224},{96,192},{128,32},{160,0},{192,96},{224,... | collective-permute-start | bytes 589832 | tf_op jit(solution)/shard_map/ppermute | solution.py:19
  200.2 22.0 %collective-permute-start.14 = (bf16[32,24,128]{2,1,0:T(8,128)(2,1)S(1)}, bf16[32,24,128]{2,1,0:T(8,128)(2,1)S(1)}, u32[]{:S(2)}, u32[]{:S(2)}) collective-permute-start(bf16[32,24,128]{2,1,0:T(8,128)(2,1)S(1)} %get-tuple-element.56), channel_id=1, source_target_pairs={{0,64},{32,96},{64,0},{96,32},{128,192},{160,224},{192,128},{224,1... | collective-permute-start | bytes 589832 | tf_op jit(solution)/shard_map/ppermute | solution.py:19
  202.6 34.1 %collective-permute-start.18 = (bf16[32,24,128]{2,1,0:T(8,128)(2,1)S(1)}, bf16[32,24,128]{2,1,0:T(8,128)(2,1)S(1)}, u32[]{:S(2)}, u32[]{:S(2)}) collective-permute-start(bf16[32,24,128]{2,1,0:T(8,128)(2,1)S(1)} %get-tuple-element.56), channel_id=1, source_target_pairs={{0,192},{32,224},{64,128},{96,160},{128,64},{160,96},{192,0},{224,... | collective-permute-start | bytes 589832 | tf_op jit(solution)/shard_map/ppermute | solution.py:19
  203.9 30.9 %collective-permute-start.15 = (bf16[32,24,128]{2,1,0:T(8,128)(2,1)S(1)}, bf16[32,24,128]{2,1,0:T(8,128)(2,1)S(1)}, u32[]{:S(2)}, u32[]{:S(2)}) collective-permute-start(bf16[32,24,128]{2,1,0:T(8,128)(2,1)S(1)} %get-tuple-element.55), channel_id=1, source_target_pairs={{0,96},{32,64},{64,32},{96,0},{128,224},{160,192},{192,160},{224,1... | collective-permute-start | bytes 589832 | tf_op jit(solution)/shard_map/ppermute | solution.py:19
  215.1 21.7 %collective-permute-start.19 = (bf16[32,24,128]{2,1,0:T(8,128)(2,1)S(1)}, bf16[32,24,128]{2,1,0:T(8,128)(2,1)S(1)}, u32[]{:S(2)}, u32[]{:S(2)}) collective-permute-start(bf16[32,24,128]{2,1,0:T(8,128)(2,1)S(1)} %get-tuple-element.55), channel_id=1, source_target_pairs={{0,224},{32,192},{64,160},{96,128},{128,96},{160,64},{192,32},{224... | collective-permute-start | bytes 589832 | tf_op jit(solution)/shard_map/ppermute | solution.py:19
  222.2 14.5 %collective-permute-start.16 = (bf16[32,24,128]{2,1,0:T(8,128)(2,1)S(1)}, bf16[32,24,128]{2,1,0:T(8,128)(2,1)S(1)}, u32[]{:S(2)}, u32[]{:S(2)}) collective-permute-start(bf16[32,24,128]{2,1,0:T(8,128)(2,1)S(1)} %get-tuple-element.58.refs_0_), channel_id=1, source_target_pairs={{0,128},{32,160},{64,192},{96,224},{128,0},{160,32},{192,64},{224,... | collective-permute-start | bytes 589832 | tf_op jit(solution)/shard_map/ppermute | solution.py:19
  245.3 81.9 %all-to-all-start.4 = ((bf16[32,24,2048]{2,1,0:T(8,128)(2,1)}), bf16[32,24,2048]{2,1,0:T(8,128)(2,1)S(1)}, u32[]{:S(2)}, u32[]{:S(2)}) async-start(bf16[32,24,2048]{2,1,0:T(8,128)(2,1)} %bitcast.94), calls=%async_computation.4 | async-start | bytes 6291456 | tf_op jit(solution)/shard_map/all_to_all | solution.py:23
  260.9 30.2 %collective-permute-start.22 = (bf16[2,3,32,128]{3,2,1,0:T(8,128)(2,1)S(1)}, bf16[2,3,32,128]{3,2,1,0:T(8,128)(2,1)S(1)}, u32[]{:S(2)}, u32[]{:S(2)}) collective-permute-start(bf16[2,3,32,128]{3,2,1,0:T(8,128)(2,1)S(1)} %maximum_select_fusion.1), channel_id=1, source_target_pairs={{0,2},{1,3},{2,0},{3,1},{4,6},{5,7},{6,4},{7,5},{8,10},{9,11},{10,... | collective-permute-start | bytes 147464 | tf_op jit(solution)/shard_map/ppermute | solution.py:19
  262.4 30.4 %collective-permute-start.23 = (bf16[2,3,32,128]{3,2,1,0:T(8,128)(2,1)S(1)}, bf16[2,3,32,128]{3,2,1,0:T(8,128)(2,1)S(1)}, u32[]{:S(2)}, u32[]{:S(2)}) collective-permute-start(bf16[2,3,32,128]{3,2,1,0:T(8,128)(2,1)S(1)} %maximum_select_fusion.1), channel_id=1, source_target_pairs={{0,3},{1,2},{2,1},{3,0},{4,7},{5,6},{6,5},{7,4},{8,11},{9,10},{10,... | collective-permute-start | bytes 147464 | tf_op jit(solution)/shard_map/ppermute | solution.py:19
  262.7 33.4 %collective-permute-start.24 = (bf16[2,3,32,128]{3,2,1,0:T(8,128)(2,1)S(1)}, bf16[2,3,32,128]{3,2,1,0:T(8,128)(2,1)S(1)}, u32[]{:S(2)}, u32[]{:S(2)}) collective-permute-start(bf16[2,3,32,128]{3,2,1,0:T(8,128)(2,1)S(1)} %maximum_select_fusion.1), channel_id=1, source_target_pairs={{0,4},{1,5},{2,6},{3,7},{4,0},{5,1},{6,2},{7,3},{8,12},{9,13},{10,... | collective-permute-start | bytes 147464 | tf_op jit(solution)/shard_map/ppermute | solution.py:19
  265.7 30.5 %collective-permute-start.25 = (bf16[2,3,32,128]{3,2,1,0:T(8,128)(2,1)S(1)}, bf16[2,3,32,128]{3,2,1,0:T(8,128)(2,1)S(1)}, u32[]{:S(2)}, u32[]{:S(2)}) collective-permute-start(bf16[2,3,32,128]{3,2,1,0:T(8,128)(2,1)S(1)} %maximum_select_fusion.1), channel_id=1, source_target_pairs={{0,5},{1,4},{2,7},{3,6},{4,1},{5,0},{6,3},{7,2},{8,13},{9,12},{10,... | collective-permute-start | bytes 147464 | tf_op jit(solution)/shard_map/ppermute | solution.py:19
  266.8 29.4 %collective-permute-start.26 = (bf16[2,3,32,128]{3,2,1,0:T(8,128)(2,1)S(1)}, bf16[2,3,32,128]{3,2,1,0:T(8,128)(2,1)S(1)}, u32[]{:S(2)}, u32[]{:S(2)}) collective-permute-start(bf16[2,3,32,128]{3,2,1,0:T(8,128)(2,1)S(1)} %maximum_select_fusion.1), channel_id=1, source_target_pairs={{0,6},{1,7},{2,4},{3,5},{4,2},{5,3},{6,0},{7,1},{8,14},{9,15},{10,... | collective-permute-start | bytes 147464 | tf_op jit(solution)/shard_map/ppermute | solution.py:19
  301.7 19.0 %collective-permute-start.29 = (bf16[3,32,2048]{2,1,0:T(8,128)(2,1)}, bf16[3,32,2048]{2,1,0:T(8,128)(2,1)}, u32[]{:S(2)}, u32[]{:S(2)}) collective-permute-start(bf16[3,32,2048]{2,1,0:T(8,128)(2,1)} %lay.1), channel_id=1, source_target_pairs={{0,16},{8,24},{16,0},{24,8},{1,17},{9,25},{17,1},{25,9},{2,18},{10... | collective-permute-start | bytes 1179656 | tf_op jit(solution)/shard_map/ppermute | solution.py:19
  302.8 19.3 %collective-permute-start.30 = (bf16[3,32,2048]{2,1,0:T(8,128)(2,1)}, bf16[3,32,2048]{2,1,0:T(8,128)(2,1)}, u32[]{:S(2)}, u32[]{:S(2)}) collective-permute-start(bf16[3,32,2048]{2,1,0:T(8,128)(2,1)} %lay.1), channel_id=1, source_target_pairs={{0,24},{8,16},{16,8},{24,0},{1,25},{9,17},{17,9},{25,1},{2,26},{10... | collective-permute-start | bytes 1179656 | tf_op jit(solution)/shard_map/ppermute | solution.py:19
  328.9 48.0 %all-to-all-start.3 = ((bf16[32,24,2048]{2,1,0:T(8,128)(2,1)}), bf16[32,24,2048]{2,1,0:T(8,128)(2,1)}, u32[]{:S(2)}, u32[]{:S(2)}) async-start(bf16[32,24,2048]{2,1,0:T(8,128)(2,1)} %bitcast.93), calls=%async_computation.3 | async-start | bytes 6291456 | tf_op jit(solution)/shard_map/all_to_all | solution.py:23
  351.9 37.5 %collective-permute-start.33 = (bf16[128,2048]{1,0:T(8,128)(2,1)}, bf16[128,2048]{1,0:T(8,128)(2,1)S(1)}, u32[]{:S(2)}, u32[]{:S(2)}) collective-permute-start(bf16[128,2048]{1,0:T(8,128)(2,1)} %combine.7), channel_id=1, source_target_pairs={{0,96},{32,64},{64,32},{96,0},{1,97},{33,65},{65,33},{97,1},{2,98}... | collective-permute-start | bytes 1572872 | tf_op jit(solution)/shard_map/ppermute | solution.py:19
  358.2 42.9 %collective-permute-start.32 = (bf16[128,2048]{1,0:T(8,128)(2,1)}, bf16[128,2048]{1,0:T(8,128)(2,1)S(1)}, u32[]{:S(2)}, u32[]{:S(2)}) collective-permute-start(bf16[128,2048]{1,0:T(8,128)(2,1)} %combine.6), channel_id=1, source_target_pairs={{0,64},{32,96},{64,0},{96,32},{1,65},{33,97},{65,1},{97,33},{2,66}... | collective-permute-start | bytes 1572872 | tf_op jit(solution)/shard_map/ppermute | solution.py:19
  381.6 25.1 %collective-permute-start.31 = (bf16[128,2048]{1,0:T(8,128)(2,1)}, bf16[128,2048]{1,0:T(8,128)(2,1)}, u32[]{:S(2)}, u32[]{:S(2)}) collective-permute-start(bf16[128,2048]{1,0:T(8,128)(2,1)} %combine.5), channel_id=1, source_target_pairs={{0,32},{32,0},{64,96},{96,64},{1,33},{33,1},{65,97},{97,65},{2,34}... | collective-permute-start | bytes 1572872 | tf_op jit(solution)/shard_map/ppermute | solution.py:19
  (42 other events, 427.4 us)

commit v3 on v2

--- a/solution.py
+++ b/solution.py
@@ -191,15 +191,16 @@
         n = chosen.shape[1]
         before = (jnp.arange(n)[:, None] < jnp.arange(n)[None, :]).astype(bf16)
         place = jnp.dot(chosen.astype(bf16), before, preferred_element_type=f32)
-        code = jnp.where(chosen > 0, place + float(k * capacity), -1.0).astype(bf16)
-        high = weight.astype(bf16)
-        low = (weight - high.astype(f32)).astype(bf16)
-        held = by_token(code) == within[None, :]
-        high = jnp.where(held, by_token(high), 0.0).astype(bf16)
-        low = jnp.where(held, by_token(low), 0.0).astype(bf16)
-        codes.append(code)
-        weights.append((high, low))
-    return jnp.concatenate(codes, axis=1), weights
+        codes.append(jnp.where(chosen > 0, place + float(k * capacity), -1.0))
+        weights.append(weight)
+    code = jnp.concatenate(codes, axis=1).astype(bf16)
+    weight = jnp.concatenate(weights, axis=1)
+    high = weight.astype(bf16)
+    low = (weight - high.astype(f32)).astype(bf16)
+    held = by_token(code) == within[None, :]
+    high = jnp.where(held, by_token(high), 0.0).astype(bf16)
+    low = jnp.where(held, by_token(low), 0.0).astype(bf16)
+    return code, (high, low)
 
 
 def pick_kernel(code, one, two, out, *, span, tile):
@@ -236,42 +237,78 @@
     )(code, one, two)
 
 
-def lay_kernel(place, stack, out):
-    n, groups, _, _, cols = stack.shape
-    for g in range(groups):
-        for i in range(n):
-            at = (g * n + i) * cols
-            out[:, :, at : at + cols] = stack[i ^ place[0], g]
-
-
-def lay(place, stack):
-    n, groups, matrices, rows, cols = stack.shape
+def lay_kernel(place, *refs):
+    pieces, out, held = refs[:-2], refs[-2], refs[-1]
+    n = len(pieces)
+    groups, _, _, cols = pieces[0].shape
+    for k in range(n):
+        for g in range(groups):
+            held[g * n + (k ^ place[0])] = pieces[k][g]
+    for f in range(groups * n):
+        out[:, :, f * cols : (f + 1) * cols] = held[f]
+
+
+def lay(place, pieces):
+    n = len(pieces)
+    groups, matrices, rows, cols = pieces[0].shape
+    piece = pl.BlockSpec(pieces[0].shape, lambda i, p: (0,) * 4)
     spec = pltpu.PrefetchScalarGridSpec(
         num_scalar_prefetch=1,
         grid=(1,),
-        in_specs=[pl.BlockSpec(stack.shape, lambda i, p: (0,) * 5)],
+        in_specs=[piece] * n,
         out_specs=pl.BlockSpec((matrices, rows, groups * n * cols), lambda i, p: (0, 0, 0)),
+        scratch_shapes=[pltpu.VMEM((groups * n, matrices, rows, cols), bf16)],
     )
     return pl.pallas_call(
         lay_kernel,
         grid_spec=spec,
         out_shape=jax.ShapeDtypeStruct((matrices, rows, groups * n * cols), bf16),
         cost_estimate=pl.CostEstimate(
-            flops=stack.size, bytes_accessed=4 * stack.size, transcendentals=0
+            flops=n * pieces[0].size, bytes_accessed=4 * n * pieces[0].size, transcendentals=0
         ),
         name="lay",
-    )(place, stack)
-
-
-def combine_kernel(high, low, back, hidden, down, out):
+    )(place, *pieces)
+
+
+def units_kernel(*refs, blocks):
+    tokens, refs = refs[:blocks], refs[blocks:]
+    columns, (near, far, down) = refs[:-3], refs[-3:]
+    gate, up, last = (jnp.concatenate([c[m] for c in columns], axis=0) for m in range(3))
+    down[...] = last
+    half = blocks // 2
+    for out, pair in ((near, tokens[:half]), (far, tokens[half:])):
+        rows = jnp.concatenate([t[...] for t in pair], axis=0)
+        out[...] = hidden_rows(rows, gate, up)
+
+
+def shared_units(tokens, columns):
+    count, features = tokens[0].shape
+    units = len(columns) * columns[0].shape[1]
+    half = len(tokens) // 2 * count
+    return pl.pallas_call(
+        functools.partial(units_kernel, blocks=len(tokens)),
+        out_shape=[jax.ShapeDtypeStruct((half, units), bf16)] * 2
+        + [jax.ShapeDtypeStruct((units, features), bf16)],
+        cost_estimate=pl.CostEstimate(
+            flops=8 * half * units * features,
+            bytes_accessed=4 * half * features + 8 * units * features,
+            transcendentals=2 * half * units,
+        ),
+        name="shared_units",
+    )(*tokens, *columns)
+
+
+def combine_kernel(high, low, back, hidden, down, one, two):
     rows = back[...]
     total = jnp.dot(high[...], rows, preferred_element_type=f32)
     total += jnp.dot(low[...], rows, preferred_element_type=f32)
     total += jnp.dot(hidden[...], down[...], preferred_element_type=f32)
-    out[...] = total.astype(out.dtype)
-
-
-def combine(weights, back, hidden, down, dtype, tile):
+    n = one.shape[0]
+    one[...] = total[:n].astype(one.dtype)
+    two[...] = total[n:].astype(two.dtype)
+
+
+def combine(weights, back, hidden, down, dtypes, tile):
     high, low = weights
     count, slots = high.shape
     features = back.shape[1]
@@ -288,8 +325,8 @@
             whole(count, units),
             part(units),
         ],
-        out_specs=part(count),
-        out_shape=jax.ShapeDtypeStruct((count, features), dtype),
+        out_specs=[part(count // 2)] * 2,
+        out_shape=[jax.ShapeDtypeStruct((count // 2, features), d) for d in dtypes],
         cost_estimate=pl.CostEstimate(
             flops=2 * count * features * (2 * slots + units),
             bytes_accessed=4 * count * slots + 2 * slots * features + 4 * count * features,
@@ -365,7 +402,7 @@
 
     laid = [shared] + [swapped(shared, ("x", "c"), n_xc, k) for k in range(1, n_xc)]
     across = (lax.axis_index("x") * lax.axis_size("c") + lax.axis_index("c"))[None]
-    own = lay(across.astype(jnp.int32), jnp.stack(laid))
+    own = lay(across.astype(jnp.int32), laid)
     columns = [own] + [swapped(own, "y", n_y, k) for k in range(1, n_y)]
     shared_out = [own[m] for m in range(3)]
 
@@ -387,21 +424,15 @@
     near_back = plane_exchange(near_result.reshape(n_plane, 2 * capacity, features))
 
     columns, _ = lax.optimization_barrier((columns, far_result))
-    quarter = jnp.concatenate(columns, axis=1)
-    units = [hidden_rows(rows, quarter[0], quarter[1]) for rows in blocks]
+    near_units, far_units, shared_down = shared_units(blocks, columns)
     far_back = far_back.reshape(-1, features)
     near_back = near_back.reshape(-1, features)
 
-    third, fourth = (
-        swapped(
-            combine(far_weights[k - 2], far_back, units[k], quarter[2], bf16, 512), "zl", n_zl, k
-        )
-        for k in (2, 3)
-    )
-    second = swapped(
-        combine(near_weights[1], near_back, units[1], quarter[2], bf16, 512), "zl", n_zl, 1
-    )
-    kept = combine(near_weights[0], near_back, units[0], quarter[2], f32, 512)
+    third, fourth = combine(far_weights, far_back, far_units, shared_down, (bf16, bf16), 512)
+    third = swapped(third, "zl", n_zl, 2)
+    fourth = swapped(fourth, "zl", n_zl, 3)
+    kept, second = combine(near_weights, near_back, near_units, shared_down, (f32, bf16), 512)
+    second = swapped(second, "zl", n_zl, 1)
     combined = (
         kept + second.astype(f32) + third.astype(f32) + fourth.astype(f32)
     ).astype(bf16)

time: 411 us -> 430 us (1.046)
  the two profiles are of different devices: /device:TPU:16 before, /device:TPU:1 now
where the time goes in v3:
time: 430 us; the launch traced here: 429 us
  waiting for transfers between devices  223 us (52%)
  starting transfers between devices  125 us (29%)
  Pallas kernels  59.5 us (14%)
  local copies, waits for them, and re-layouts  9.39 us (2%)
  matrix products  6.12 us (1%)
  other arithmetic  5.17 us (1%)
    ppermute x34, waiting for transfers between devices, swapped(): return lax.ppermute(array, axis, [(r, r ^ k) for r in range(size)])  177 us
    ppermute x34, starting transfers between devices, swapped(): return lax.ppermute(array, axis, [(r, r ^ k) for r in range(size)])  87.9 us
    all_to_all x5, waiting for transfers between devices, plane_exchange(): return lax.all_to_all(array, PLANE, split_axis=0, concat_axis=0, tiled=True)  45.4 us
    all_to_all x5, starting transfers between devices, plane_exchange(): return lax.all_to_all(array, PLANE, split_axis=0, concat_axis=0, tiled=True)  36.8 us
    pallas_call x2, Pallas kernels, assemble(): pl.pallas_call(functools.partial(assemble_kernel, compute=compute, blocks...  16.2 us
    pallas_call x2, Pallas kernels, over_rows(): pl.pallas_call(functools.partial(rows_kernel, compute=compute), grid=(cou...  11.8 us
    pallas_call x2, Pallas kernels, combine(): pl.pallas_call(combine_kernel, grid=(features // tile,), in_specs=[whole(...  10.8 us
    pallas_call x2, Pallas kernels, pick(): pl.pallas_call(functools.partial(pick_kernel, span=span, tile=tile), grid...  9.7 us
  transfers between devices with their start and end apart: 39, of which 22 were waited for; matrix products, arithmetic and copies ran while one was open for 2% of the time, Pallas kernels for 11%

profile of v3, /device:TPU:1, one launch (start us, length us, event | category | flops | bytes accessed | tf_op | source)
XLA Modules:
  0.0 428.7 jit_solution(18001574461948870735)
XLA Ops:
  1.3 5.1 %cast.1 = bf16[32,288,128]{2,1,0:T(8,128)(2,1)} custom-call(s32[16]{0:T(128)} %stack.73.place, f32[1,128]{1,0:T(1,128)} %bitcast.49, f32[128,24,128]{2,1,0:T(8,128)} %gate.1, f32[128,24,128]{2,1,0:T(8,128)} %up.1, f32[128,24,128]{2,1,0:T(8,128)} %down.1), custom_call_target="tpu_custom_call" | custom-call | flops 1179648 | bytes 7077888 | tf_op jit(solution)/shard_map/cast/pallas_call | solution.py:44
  6.4 8.7 %all-to-all-start = ((bf16[32,288,128]{2,1,0:T(8,128)(2,1)}), bf16[32,288,128]{2,1,0:T(8,128)(2,1)S(1)}, u32[]{:S(2)}, u32[]{:S(2)}) async-start(bf16[32,288,128]{2,1,0:T(8,128)(2,1)} %cast.1), calls=%async_computation | async-start | bytes 4718592 | tf_op jit(solution)/shard_map/all_to_all | solution.py:23
  19.0 11.3 %collective-permute-done.5.two.refs_1_ = bf16[128,2048]{1,0:T(8,128)(2,1)S(1)} collective-permute-done((bf16[128,2048]{1,0:T(8,128)(2,1)S(1)}, bf16[128,2048]{1,0:T(8,128)(2,1)S(1)}, u32[]{:S(2)}, u32[]{:S(2)}) %collective-permute-start.5) | collective-permute-done | bytes 524320 | tf_op jit(solution)/shard_map/ppermute | solution.py:19
  31.1 4.9 %pick.3 = bf16[768,2048]{1,0:T(8,128)(2,1)} custom-call(bf16[32,256]{1,0:T(8,128)(2,1)} %pad_maximum_fusion.4.code, bf16[128,2048]{1,0:T(8,128)(2,1)} %copy-done, bf16[128,2048]{1,0:T(8,128)(2,1)} %copy-done.6), custom_call_target="tpu_custom_call" | custom-call | flops 805306368 | bytes 4194304 | tf_op jit(solution)/shard_map/pick/pallas_call | solution.py:225
  36.0 10.7 %all-to-all-done = bf16[32,288,128]{2,1,0:T(8,128)(2,1)S(1)} async-done(((bf16[32,288,128]{2,1,0:T(8,128)(2,1)}), bf16[32,288,128]{2,1,0:T(8,128)(2,1)S(1)}, u32[]{:S(2)}, u32[]{:S(2)}) %all-to-all-start) | async-done | bytes 2359328 | tf_op jit(solution)/shard_map/all_to_all | solution.py:23
  46.6 6.4 %all-to-all-start.1 = ((bf16[32,24,2048]{2,1,0:T(8,128)(2,1)}), bf16[32,24,2048]{2,1,0:T(8,128)(2,1)}, u32[]{:S(2)}, u32[]{:S(2)}) async-start(bf16[32,24,2048]{2,1,0:T(8,128)(2,1)} %bitcast.41), calls=%async_computation.1 | async-start | bytes 6291456 | tf_op jit(solution)/shard_map/all_to_all | solution.py:23
  62.3 32.6 %collective-permute-done.2.one.refs_2_ = bf16[128,2048]{1,0:T(8,128)(2,1)S(1)} collective-permute-done((bf16[128,2048]{1,0:T(8,128)(2,1)S(1)}, bf16[128,2048]{1,0:T(8,128)(2,1)S(1)}, u32[]{:S(2)}, u32[]{:S(2)}) %collective-permute-start.2) | collective-permute-done | bytes 524320 | tf_op jit(solution)/shard_map/ppermute | solution.py:19
  95.7 4.8 %pick.2 = bf16[768,2048]{1,0:T(8,128)(2,1)} custom-call(bf16[32,256]{1,0:T(8,128)(2,1)} %pad_maximum_fusion.3.code, bf16[128,2048]{1,0:T(8,128)(2,1)} %copy-done.7, bf16[128,2048]{1,0:T(8,128)(2,1)} %collective-permute-done.3.two.refs_3_), custom_call_target="tpu_custom_call" | custom-call | flops 805306368 | bytes 4194304 | tf_op jit(solution)/shard_map/pick/pallas_call | solution.py:225
  100.5 7.8 %all-to-all-start.2 = ((bf16[32,24,2048]{2,1,0:T(8,128)(2,1)}), bf16[32,24,2048]{2,1,0:T(8,128)(2,1)}, u32[]{:S(2)}, u32[]{:S(2)}) async-start(bf16[32,24,2048]{2,1,0:T(8,128)(2,1)} %bitcast.40), calls=%async_computation.2 | async-start | bytes 6291456 | tf_op jit(solution)/shard_map/all_to_all | solution.py:23
  111.3 10.7 %collective-permute-start.6 = (bf16[32,48,128]{2,1,0:T(8,128)(2,1)S(1)}, bf16[32,48,128]{2,1,0:T(8,128)(2,1)S(1)}, u32[]{:S(2)}, u32[]{:S(2)}) collective-permute-start(bf16[32,48,128]{2,1,0:T(8,128)(2,1)S(1)} %get-tuple-element.67), channel_id=1, source_target_pairs={{0,32},{32,0},{64,96},{96,64},{128,160},{160,128},{192,224},{224,1... | collective-permute-start | bytes 1179656 | tf_op jit(solution)/shard_map/ppermute | solution.py:19
  123.7 5.2 %collective-permute-start.10 = (bf16[32,48,128]{2,1,0:T(8,128)(2,1)S(1)}, bf16[32,48,128]{2,1,0:T(8,128)(2,1)S(1)}, u32[]{:S(2)}, u32[]{:S(2)}) collective-permute-start(bf16[32,48,128]{2,1,0:T(8,128)(2,1)S(1)} %get-tuple-element.67), channel_id=1, source_target_pairs={{0,160},{32,128},{64,224},{96,192},{128,32},{160,0},{192,96},{224,... | collective-permute-start | bytes 1179656 | tf_op jit(solution)/shard_map/ppermute | solution.py:19
  130.5 11.5 %collective-permute-done.6.refs_1_ = bf16[32,48,128]{2,1,0:T(8,128)(2,1)S(1)} collective-permute-done((bf16[32,48,128]{2,1,0:T(8,128)(2,1)S(1)}, bf16[32,48,128]{2,1,0:T(8,128)(2,1)S(1)}, u32[]{:S(2)}, u32[]{:S(2)}) %collective-permute-start.6) | collective-permute-done | bytes 393248 | tf_op jit(solution)/shard_map/ppermute | solution.py:19
  142.0 14.4 %collective-permute-done.7.refs_2_ = bf16[32,48,128]{2,1,0:T(8,128)(2,1)S(1)} collective-permute-done((bf16[32,48,128]{2,1,0:T(8,128)(2,1)S(1)}, bf16[32,48,128]{2,1,0:T(8,128)(2,1)S(1)}, u32[]{:S(2)}, u32[]{:S(2)}) %collective-permute-start.7) | collective-permute-done | bytes 393248 | tf_op jit(solution)/shard_map/ppermute | solution.py:19
  158.5 9.9 %collective-permute-done.8.refs_3_ = bf16[32,48,128]{2,1,0:T(8,128)(2,1)S(1)} collective-permute-done((bf16[32,48,128]{2,1,0:T(8,128)(2,1)S(1)}, bf16[32,48,128]{2,1,0:T(8,128)(2,1)S(1)}, u32[]{:S(2)}, u32[]{:S(2)}) %collective-permute-start.8) | collective-permute-done | bytes 393248 | tf_op jit(solution)/shard_map/ppermute | solution.py:19
  168.3 20.1 %collective-permute-start.13 = (bf16[32,24,128]{2,1,0:T(8,128)(2,1)S(1)}, bf16[32,24,128]{2,1,0:T(8,128)(2,1)S(1)}, u32[]{:S(2)}, u32[]{:S(2)}) collective-permute-start(bf16[32,24,128]{2,1,0:T(8,128)(2,1)S(1)} %get-tuple-element.63), channel_id=1, source_target_pairs={{0,32},{32,0},{64,96},{96,64},{128,160},{160,128},{192,224},{224,1... | collective-permute-start | bytes 589832 | tf_op jit(solution)/shard_map/ppermute | solution.py:19
  188.4 6.0 %collective-permute-done.9.refs_4_ = bf16[32,48,128]{2,1,0:T(8,128)(2,1)S(1)} collective-permute-done((bf16[32,48,128]{2,1,0:T(8,128)(2,1)S(1)}, bf16[32,48,128]{2,1,0:T(8,128)(2,1)S(1)}, u32[]{:S(2)}, u32[]{:S(2)}) %collective-permute-start.9) | collective-permute-done | bytes 393248 | tf_op jit(solution)/shard_map/ppermute | solution.py:19
  200.3 9.2 %assemble.2 = (bf16[768,384]{1,0:T(8,128)(2,1)}, bf16[1,384,2048]{2,1,0:T(8,128)(2,1)}, bf16[1,384,2048]{2,1,0:T(8,128)(2,1)}) custom-call(s32[16]{0:T(128)} %stack.73.place, bf16[768,2048]{1,0:T(8,128)(2,1)} %bitcast.12.x, bf16[32,48,128]{2,1,0:T(8,128)(2,1)} %copy-done.8, bf16[32,48,128]{2,1,0:T(8,128)(2,1)} %copy-done.22, ...), custom_call_target="tpu_custom_call" | custom-call | flops 2415919104 | bytes 12582912 | tf_op jit(solution)/shard_map/assemble/pallas_call | solution.py:130
  212.4 7.9 %collective-permute-start.16 = (bf16[32,24,128]{2,1,0:T(8,128)(2,1)S(1)}, bf16[32,24,128]{2,1,0:T(8,128)(2,1)S(1)}, u32[]{:S(2)}, u32[]{:S(2)}) collective-permute-start(bf16[32,24,128]{2,1,0:T(8,128)(2,1)S(1)} %get-tuple-element.64.refs_0_), channel_id=1, source_target_pairs={{0,128},{32,160},{64,192},{96,224},{128,0},{160,32},{192,64},{224,... | collective-permute-start | bytes 589832 | tf_op jit(solution)/shard_map/ppermute | solution.py:19
  220.4 6.7 %over_rows.2.x = bf16[768,384]{1,0:T(8,128)(2,1)} custom-call(bf16[768,2048]{1,0:T(8,128)(2,1)} %bitcast.11.x, bf16[1,384,2048]{2,1,0:T(8,128)(2,1)} %get-tuple-element.24.refs_0_, bf16[1,384,2048]{2,1,0:T(8,128)(2,1)} %get-tuple-element.25.refs_1_), custom_call_target="tpu_custom_call" | custom-call | flops 2415919104 | bytes 6881280 | tf_op jit(solution)/shard_map/over_rows/pallas_call | solution.py:159
  227.1 6.3 %collective-permute-done.16.refs_4_ = bf16[32,24,128]{2,1,0:T(8,128)(2,1)S(1)} collective-permute-done((bf16[32,24,128]{2,1,0:T(8,128)(2,1)S(1)}, bf16[32,24,128]{2,1,0:T(8,128)(2,1)S(1)}, u32[]{:S(2)}, u32[]{:S(2)}) %collective-permute-start.16) | collective-permute-done | bytes 196640 | tf_op jit(solution)/shard_map/ppermute | solution.py:19
  235.0 7.0 %assemble.3 = (bf16[768,2048]{1,0:T(8,128)(2,1)}, bf16[1,384,2048]{2,1,0:T(8,128)(2,1)}) custom-call(s32[16]{0:T(128)} %stack.73.place, bf16[768,384]{1,0:T(8,128)(2,1)} %over_rows.2.x, bf16[32,24,128]{2,1,0:T(8,128)(2,1)} %copy-done.10, bf16[32,24,128]{2,1,0:T(8,128)(2,1)} %copy-done.29, bf16[32,24,128]{2,1,0:T(8,128)(2,1)} %copy-done.31, ...), custom_call_target="tpu_custom_call" | custom-call | flops 1207959552 | bytes 9437184 | tf_op jit(solution)/shard_map/assemble/pallas_call | solution.py:130
  242.0 7.7 %all-to-all-start.4 = ((bf16[32,24,2048]{2,1,0:T(8,128)(2,1)}), bf16[32,24,2048]{2,1,0:T(8,128)(2,1)S(1)}, u32[]{:S(2)}, u32[]{:S(2)}) async-start(bf16[32,24,2048]{2,1,0:T(8,128)(2,1)} %bitcast.45), calls=%async_computation.4 | async-start | bytes 6291456 | tf_op jit(solution)/shard_map/all_to_all | solution.py:23
  249.7 5.1 %over_rows.3 = bf16[768,2048]{1,0:T(8,128)(2,1)} custom-call(bf16[768,384]{1,0:T(8,128)(2,1)} %get-tuple-element.36.x, bf16[1,384,2048]{2,1,0:T(8,128)(2,1)} %get-tuple-element.26.refs_0_), custom_call_target="tpu_custom_call" | custom-call | flops 1207959552 | bytes 5308416 | tf_op jit(solution)/shard_map/over_rows/pallas_call | solution.py:159
  254.8 34.7 %all-to-all-done.4 = bf16[32,24,2048]{2,1,0:T(8,128)(2,1)S(1)} async-done(((bf16[32,24,2048]{2,1,0:T(8,128)(2,1)}), bf16[32,24,2048]{2,1,0:T(8,128)(2,1)S(1)}, u32[]{:S(2)}, u32[]{:S(2)}) %all-to-all-start.4) | async-done | bytes 3145760 | tf_op jit(solution)/shard_map/all_to_all | solution.py:23
  291.2 6.2 %all-to-all-start.3 = ((bf16[32,24,2048]{2,1,0:T(8,128)(2,1)}), bf16[32,24,2048]{2,1,0:T(8,128)(2,1)S(1)}, u32[]{:S(2)}, u32[]{:S(2)}) async-start(bf16[32,24,2048]{2,1,0:T(8,128)(2,1)} %bitcast.42), calls=%async_computation.3 | async-start | bytes 6291456 | tf_op jit(solution)/shard_map/all_to_all | solution.py:23
  314.4 20.0 %collective-permute-done.22.refs_2_ = bf16[2,3,32,128]{3,2,1,0:T(8,128)(2,1)S(1)} collective-permute-done((bf16[2,3,32,128]{3,2,1,0:T(8,128)(2,1)S(1)}, bf16[2,3,32,128]{3,2,1,0:T(8,128)(2,1)S(1)}, u32[]{:S(2)}, u32[]{:S(2)}) %collective-permute-start.22) | collective-permute-done | bytes 49184 | tf_op jit(solution)/shard_map/ppermute | solution.py:19
  334.4 5.1 %collective-permute-start.27 = (bf16[2,3,32,128]{3,2,1,0:T(8,128)(2,1)S(1)}, bf16[2,3,32,128]{3,2,1,0:T(8,128)(2,1)S(1)}, u32[]{:S(2)}, u32[]{:S(2)}) collective-permute-start(bf16[2,3,32,128]{3,2,1,0:T(8,128)(2,1)S(1)} %maximum_select_fusion.refs_0_), channel_id=1, source_target_pairs={{0,7},{1,6},{2,5},{3,4},{4,3},{5,2},{6,1},{7,0},{8,15},{9,14},{10,... | collective-permute-start | bytes 147464 | tf_op jit(solution)/shard_map/ppermute | solution.py:19
  349.0 6.9 %collective-permute-done.28.refs_5_ = bf16[3,32,2048]{2,1,0:T(8,128)(2,1)S(1)} collective-permute-done((bf16[3,32,2048]{2,1,0:T(8,128)(2,1)}, bf16[3,32,2048]{2,1,0:T(8,128)(2,1)S(1)}, u32[]{:S(2)}, u32[]{:S(2)}) %collective-permute-start.28) | collective-permute-done | bytes 393248 | tf_op jit(solution)/shard_map/ppermute | solution.py:19
  355.8 10.6 %collective-permute-done.29.refs_6_ = bf16[3,32,2048]{2,1,0:T(8,128)(2,1)} collective-permute-done((bf16[3,32,2048]{2,1,0:T(8,128)(2,1)}, bf16[3,32,2048]{2,1,0:T(8,128)(2,1)}, u32[]{:S(2)}, u32[]{:S(2)}) %collective-permute-start.29) | collective-permute-done | bytes 393248 | tf_op jit(solution)/shard_map/ppermute | solution.py:19
  372.5 5.3 %combine.3 = (bf16[128,2048]{1,0:T(8,128)(2,1)}, bf16[128,2048]{1,0:T(8,128)(2,1)}) custom-call(bf16[256,768]{1,0:T(8,128)(2,1)} %fusion.2.high, bf16[256,768]{1,0:T(8,128)(2,1)} %fusion.3.low, bf16[768,2048]{1,0:T(8,128)(2,1)} %bitcast.44, bf16[256,128]{1,0:T(8,128)(2,1)} %get-tuple-element.50.hidden, bf16[128,2048]{1,0:T(8,128)(2,1)} %get-tuple-element.45.down), custom_call_target="tpu_custom_call" | custom-call | flops 1744830464 | bytes 6029312 | tf_op jit(solution)/shard_map/combine/pallas_call | solution.py:318
  382.0 5.5 %combine.2 = (f32[128,2048]{1,0:T(8,128)}, bf16[128,2048]{1,0:T(8,128)(2,1)}) custom-call(bf16[256,768]{1,0:T(8,128)(2,1)} %fusion.high, bf16[256,768]{1,0:T(8,128)(2,1)} %fusion.1.low, bf16[768,2048]{1,0:T(8,128)(2,1)} %bitcast.43, bf16[256,128]{1,0:T(8,128)(2,1)} %get-tuple-element.44.hidden, bf16[128,2048]{1,0:T(8,128)(2,1)} %get-tuple-element.45.down), custom_call_target="tpu_custom_call" | custom-call | flops 1744830464 | bytes 6029312 | tf_op jit(solution)/shard_map/combine/pallas_call | solution.py:318
  391.7 34.3 %collective-permute-done.32 = bf16[128,2048]{1,0:T(8,128)(2,1)} collective-permute-done((bf16[128,2048]{1,0:T(8,128)(2,1)}, bf16[128,2048]{1,0:T(8,128)(2,1)}, u32[]{:S(2)}, u32[]{:S(2)}) %collective-permute-start.32) | collective-permute-done | bytes 524320 | tf_op jit(solution)/shard_map/ppermute | solution.py:19
  (164 shorter events, 79.0 us)
Async XLA Ops:
  6.4 40.2 %all-to-all-start = ((bf16[32,288,128]{2,1,0:T(8,128)(2,1)}), bf16[32,288,128]{2,1,0:T(8,128)(2,1)S(1)}, u32[]{:S(2)}, u32[]{:S(2)}) async-start(bf16[32,288,128]{2,1,0:T(8,128)(2,1)} %cast.1), calls=%async_computation | async-start | bytes 4718592 | tf_op jit(solution)/shard_map/all_to_all | solution.py:23
  17.3 13.1 %collective-permute-start.5 = (bf16[128,2048]{1,0:T(8,128)(2,1)S(1)}, bf16[128,2048]{1,0:T(8,128)(2,1)S(1)}, u32[]{:S(2)}, u32[]{:S(2)}) collective-permute-start(bf16[128,2048]{1,0:T(8,128)(2,1)S(1)} %fusion.11.one.refs_0_), channel_id=1, source_target_pairs={{0,32},{32,0},{64,96},{96,64},{1,33},{33,1},{65,97},{97,65},{2,34}... | collective-permute-start | bytes 1572872 | tf_op jit(solution)/shard_map/ppermute | solution.py:19
  46.6 53.9 %all-to-all-start.1 = ((bf16[32,24,2048]{2,1,0:T(8,128)(2,1)}), bf16[32,24,2048]{2,1,0:T(8,128)(2,1)}, u32[]{:S(2)}, u32[]{:S(2)}) async-start(bf16[32,24,2048]{2,1,0:T(8,128)(2,1)} %bitcast.41), calls=%async_computation.1 | async-start | bytes 6291456 | tf_op jit(solution)/shard_map/all_to_all | solution.py:23
  57.5 37.4 %collective-permute-start.2 = (bf16[128,2048]{1,0:T(8,128)(2,1)S(1)}, bf16[128,2048]{1,0:T(8,128)(2,1)S(1)}, u32[]{:S(2)}, u32[]{:S(2)}) collective-permute-start(bf16[128,2048]{1,0:T(8,128)(2,1)S(1)} %copy-done.1), channel_id=1, source_target_pairs={{0,64},{32,96},{64,0},{96,32},{1,65},{33,97},{65,1},{97,33},{2,66}... | collective-permute-start | bytes 1572872 | tf_op jit(solution)/shard_map/ppermute | solution.py:19
  59.9 35.0 %collective-permute-start.3 = (bf16[128,2048]{1,0:T(8,128)(2,1)S(1)}, bf16[128,2048]{1,0:T(8,128)(2,1)}, u32[]{:S(2)}, u32[]{:S(2)}) collective-permute-start(bf16[128,2048]{1,0:T(8,128)(2,1)S(1)} %copy-done.1), channel_id=1, source_target_pairs={{0,96},{32,64},{64,32},{96,0},{1,97},{33,65},{65,33},{97,1},{2,98}... | collective-permute-start | bytes 1572872 | tf_op jit(solution)/shard_map/ppermute | solution.py:19
  100.5 119.9 %all-to-all-start.2 = ((bf16[32,24,2048]{2,1,0:T(8,128)(2,1)}), bf16[32,24,2048]{2,1,0:T(8,128)(2,1)}, u32[]{:S(2)}, u32[]{:S(2)}) async-start(bf16[32,24,2048]{2,1,0:T(8,128)(2,1)} %bitcast.40), calls=%async_computation.2 | async-start | bytes 6291456 | tf_op jit(solution)/shard_map/all_to_all | solution.py:23
  111.3 30.7 %collective-permute-start.6 = (bf16[32,48,128]{2,1,0:T(8,128)(2,1)S(1)}, bf16[32,48,128]{2,1,0:T(8,128)(2,1)S(1)}, u32[]{:S(2)}, u32[]{:S(2)}) collective-permute-start(bf16[32,48,128]{2,1,0:T(8,128)(2,1)S(1)} %get-tuple-element.67), channel_id=1, source_target_pairs={{0,32},{32,0},{64,96},{96,64},{128,160},{160,128},{192,224},{224,1... | collective-permute-start | bytes 1179656 | tf_op jit(solution)/shard_map/ppermute | solution.py:19
  122.1 34.4 %collective-permute-start.7 = (bf16[32,48,128]{2,1,0:T(8,128)(2,1)S(1)}, bf16[32,48,128]{2,1,0:T(8,128)(2,1)S(1)}, u32[]{:S(2)}, u32[]{:S(2)}) collective-permute-start(bf16[32,48,128]{2,1,0:T(8,128)(2,1)S(1)} %get-tuple-element.66), channel_id=1, source_target_pairs={{0,64},{32,96},{64,0},{96,32},{128,192},{160,224},{192,128},{224,1... | collective-permute-start | bytes 1179656 | tf_op jit(solution)/shard_map/ppermute | solution.py:19
  123.7 70.7 %collective-permute-start.10 = (bf16[32,48,128]{2,1,0:T(8,128)(2,1)S(1)}, bf16[32,48,128]{2,1,0:T(8,128)(2,1)S(1)}, u32[]{:S(2)}, u32[]{:S(2)}) collective-permute-start(bf16[32,48,128]{2,1,0:T(8,128)(2,1)S(1)} %get-tuple-element.67), channel_id=1, source_target_pairs={{0,160},{32,128},{64,224},{96,192},{128,32},{160,0},{192,96},{224,... | collective-permute-start | bytes 1179656 | tf_op jit(solution)/shard_map/ppermute | solution.py:19
  128.9 65.7 %collective-permute-start.11 = (bf16[32,48,128]{2,1,0:T(8,128)(2,1)S(1)}, bf16[32,48,128]{2,1,0:T(8,128)(2,1)S(1)}, u32[]{:S(2)}, u32[]{:S(2)}) collective-permute-start(bf16[32,48,128]{2,1,0:T(8,128)(2,1)S(1)} %get-tuple-element.66), channel_id=1, source_target_pairs={{0,192},{32,224},{64,128},{96,160},{128,64},{160,96},{192,0},{224,... | collective-permute-start | bytes 1179656 | tf_op jit(solution)/shard_map/ppermute | solution.py:19
  128.9 39.4 %collective-permute-start.8 = (bf16[32,48,128]{2,1,0:T(8,128)(2,1)S(1)}, bf16[32,48,128]{2,1,0:T(8,128)(2,1)S(1)}, u32[]{:S(2)}, u32[]{:S(2)}) collective-permute-start(bf16[32,48,128]{2,1,0:T(8,128)(2,1)S(1)} %get-tuple-element.65), channel_id=1, source_target_pairs={{0,96},{32,64},{64,32},{96,0},{128,224},{160,192},{192,160},{224,1... | collective-permute-start | bytes 1179656 | tf_op jit(solution)/shard_map/ppermute | solution.py:19
  142.0 56.3 %collective-permute-start.12 = (bf16[32,48,128]{2,1,0:T(8,128)(2,1)S(1)}, bf16[32,48,128]{2,1,0:T(8,128)(2,1)S(1)}, u32[]{:S(2)}, u32[]{:S(2)}) collective-permute-start(bf16[32,48,128]{2,1,0:T(8,128)(2,1)S(1)} %get-tuple-element.65), channel_id=1, source_target_pairs={{0,224},{32,192},{64,160},{96,128},{128,96},{160,64},{192,32},{224... | collective-permute-start | bytes 1179656 | tf_op jit(solution)/shard_map/ppermute | solution.py:19
  156.4 38.0 %collective-permute-start.9 = (bf16[32,48,128]{2,1,0:T(8,128)(2,1)S(1)}, bf16[32,48,128]{2,1,0:T(8,128)(2,1)S(1)}, u32[]{:S(2)}, u32[]{:S(2)}) collective-permute-start(bf16[32,48,128]{2,1,0:T(8,128)(2,1)S(1)} %get-tuple-element.68.refs_0_), channel_id=1, source_target_pairs={{0,128},{32,160},{64,192},{96,224},{128,0},{160,32},{192,64},{224,... | collective-permute-start | bytes 1179656 | tf_op jit(solution)/shard_map/ppermute | solution.py:19
  168.3 41.2 %collective-permute-start.13 = (bf16[32,24,128]{2,1,0:T(8,128)(2,1)S(1)}, bf16[32,24,128]{2,1,0:T(8,128)(2,1)S(1)}, u32[]{:S(2)}, u32[]{:S(2)}) collective-permute-start(bf16[32,24,128]{2,1,0:T(8,128)(2,1)S(1)} %get-tuple-element.63), channel_id=1, source_target_pairs={{0,32},{32,0},{64,96},{96,64},{128,160},{160,128},{192,224},{224,1... | collective-permute-start | bytes 589832 | tf_op jit(solution)/shard_map/ppermute | solution.py:19
  194.4 39.0 %collective-permute-start.17 = (bf16[32,24,128]{2,1,0:T(8,128)(2,1)S(1)}, bf16[32,24,128]{2,1,0:T(8,128)(2,1)S(1)}, u32[]{:S(2)}, u32[]{:S(2)}) collective-permute-start(bf16[32,24,128]{2,1,0:T(8,128)(2,1)S(1)} %get-tuple-element.63), channel_id=1, source_target_pairs={{0,160},{32,128},{64,224},{96,192},{128,32},{160,0},{192,96},{224,... | collective-permute-start | bytes 589832 | tf_op jit(solution)/shard_map/ppermute | solution.py:19
  194.5 18.0 %collective-permute-start.14 = (bf16[32,24,128]{2,1,0:T(8,128)(2,1)S(1)}, bf16[32,24,128]{2,1,0:T(8,128)(2,1)S(1)}, u32[]{:S(2)}, u32[]{:S(2)}) collective-permute-start(bf16[32,24,128]{2,1,0:T(8,128)(2,1)S(1)} %get-tuple-element.62), channel_id=1, source_target_pairs={{0,64},{32,96},{64,0},{96,32},{128,192},{160,224},{192,128},{224,1... | collective-permute-start | bytes 589832 | tf_op jit(solution)/shard_map/ppermute | solution.py:19
  194.6 38.9 %collective-permute-start.18 = (bf16[32,24,128]{2,1,0:T(8,128)(2,1)S(1)}, bf16[32,24,128]{2,1,0:T(8,128)(2,1)S(1)}, u32[]{:S(2)}, u32[]{:S(2)}) collective-permute-start(bf16[32,24,128]{2,1,0:T(8,128)(2,1)S(1)} %get-tuple-element.62), channel_id=1, source_target_pairs={{0,192},{32,224},{64,128},{96,160},{128,64},{160,96},{192,0},{224,... | collective-permute-start | bytes 589832 | tf_op jit(solution)/shard_map/ppermute | solution.py:19
  198.4 28.7 %collective-permute-start.15 = (bf16[32,24,128]{2,1,0:T(8,128)(2,1)S(1)}, bf16[32,24,128]{2,1,0:T(8,128)(2,1)S(1)}, u32[]{:S(2)}, u32[]{:S(2)}) collective-permute-start(bf16[32,24,128]{2,1,0:T(8,128)(2,1)S(1)} %get-tuple-element.61), channel_id=1, source_target_pairs={{0,96},{32,64},{64,32},{96,0},{128,224},{160,192},{192,160},{224,1... | collective-permute-start | bytes 589832 | tf_op jit(solution)/shard_map/ppermute | solution.py:19
  209.6 23.9 %collective-permute-start.19 = (bf16[32,24,128]{2,1,0:T(8,128)(2,1)S(1)}, bf16[32,24,128]{2,1,0:T(8,128)(2,1)S(1)}, u32[]{:S(2)}, u32[]{:S(2)}) collective-permute-start(bf16[32,24,128]{2,1,0:T(8,128)(2,1)S(1)} %get-tuple-element.61), channel_id=1, source_target_pairs={{0,224},{32,192},{64,160},{96,128},{128,96},{160,64},{192,32},{224... | collective-permute-start | bytes 589832 | tf_op jit(solution)/shard_map/ppermute | solution.py:19
  212.4 21.0 %collective-permute-start.16 = (bf16[32,24,128]{2,1,0:T(8,128)(2,1)S(1)}, bf16[32,24,128]{2,1,0:T(8,128)(2,1)S(1)}, u32[]{:S(2)}, u32[]{:S(2)}) collective-permute-start(bf16[32,24,128]{2,1,0:T(8,128)(2,1)S(1)} %get-tuple-element.64.refs_0_), channel_id=1, source_target_pairs={{0,128},{32,160},{64,192},{96,224},{128,0},{160,32},{192,64},{224,... | collective-permute-start | bytes 589832 | tf_op jit(solution)/shard_map/ppermute | solution.py:19
  242.0 47.5 %all-to-all-start.4 = ((bf16[32,24,2048]{2,1,0:T(8,128)(2,1)}), bf16[32,24,2048]{2,1,0:T(8,128)(2,1)S(1)}, u32[]{:S(2)}, u32[]{:S(2)}) async-start(bf16[32,24,2048]{2,1,0:T(8,128)(2,1)} %bitcast.45), calls=%async_computation.4 | async-start | bytes 6291456 | tf_op jit(solution)/shard_map/all_to_all | solution.py:23
  291.2 89.2 %all-to-all-start.3 = ((bf16[32,24,2048]{2,1,0:T(8,128)(2,1)}), bf16[32,24,2048]{2,1,0:T(8,128)(2,1)S(1)}, u32[]{:S(2)}, u32[]{:S(2)}) async-start(bf16[32,24,2048]{2,1,0:T(8,128)(2,1)} %bitcast.42), calls=%async_computation.3 | async-start | bytes 6291456 | tf_op jit(solution)/shard_map/all_to_all | solution.py:23
  306.7 27.7 %collective-permute-start.22 = (bf16[2,3,32,128]{3,2,1,0:T(8,128)(2,1)S(1)}, bf16[2,3,32,128]{3,2,1,0:T(8,128)(2,1)S(1)}, u32[]{:S(2)}, u32[]{:S(2)}) collective-permute-start(bf16[2,3,32,128]{3,2,1,0:T(8,128)(2,1)S(1)} %maximum_select_fusion.refs_0_), channel_id=1, source_target_pairs={{0,2},{1,3},{2,0},{3,1},{4,6},{5,7},{6,4},{7,5},{8,10},{9,11},{10,... | collective-permute-start | bytes 147464 | tf_op jit(solution)/shard_map/ppermute | solution.py:19
  308.1 31.4 %collective-permute-start.23 = (bf16[2,3,32,128]{3,2,1,0:T(8,128)(2,1)S(1)}, bf16[2,3,32,128]{3,2,1,0:T(8,128)(2,1)S(1)}, u32[]{:S(2)}, u32[]{:S(2)}) collective-permute-start(bf16[2,3,32,128]{3,2,1,0:T(8,128)(2,1)S(1)} %maximum_select_fusion.refs_0_), channel_id=1, source_target_pairs={{0,3},{1,2},{2,1},{3,0},{4,7},{5,6},{6,5},{7,4},{8,11},{9,10},{10,... | collective-permute-start | bytes 147464 | tf_op jit(solution)/shard_map/ppermute | solution.py:19
  308.4 31.2 %collective-permute-start.24 = (bf16[2,3,32,128]{3,2,1,0:T(8,128)(2,1)S(1)}, bf16[2,3,32,128]{3,2,1,0:T(8,128)(2,1)S(1)}, u32[]{:S(2)}, u32[]{:S(2)}) collective-permute-start(bf16[2,3,32,128]{3,2,1,0:T(8,128)(2,1)S(1)} %maximum_select_fusion.refs_0_), channel_id=1, source_target_pairs={{0,4},{1,5},{2,6},{3,7},{4,0},{5,1},{6,2},{7,3},{8,12},{9,13},{10,... | collective-permute-start | bytes 147464 | tf_op jit(solution)/shard_map/ppermute | solution.py:19
  311.4 30.0 %collective-permute-start.25 = (bf16[2,3,32,128]{3,2,1,0:T(8,128)(2,1)S(1)}, bf16[2,3,32,128]{3,2,1,0:T(8,128)(2,1)S(1)}, u32[]{:S(2)}, u32[]{:S(2)}) collective-permute-start(bf16[2,3,32,128]{3,2,1,0:T(8,128)(2,1)S(1)} %maximum_select_fusion.refs_0_), channel_id=1, source_target_pairs={{0,5},{1,4},{2,7},{3,6},{4,1},{5,0},{6,3},{7,2},{8,13},{9,12},{10,... | collective-permute-start | bytes 147464 | tf_op jit(solution)/shard_map/ppermute | solution.py:19
  311.7 29.6 %collective-permute-start.26 = (bf16[2,3,32,128]{3,2,1,0:T(8,128)(2,1)S(1)}, bf16[2,3,32,128]{3,2,1,0:T(8,128)(2,1)S(1)}, u32[]{:S(2)}, u32[]{:S(2)}) collective-permute-start(bf16[2,3,32,128]{3,2,1,0:T(8,128)(2,1)S(1)} %maximum_select_fusion.refs_0_), channel_id=1, source_target_pairs={{0,6},{1,7},{2,4},{3,5},{4,2},{5,3},{6,0},{7,1},{8,14},{9,15},{10,... | collective-permute-start | bytes 147464 | tf_op jit(solution)/shard_map/ppermute | solution.py:19
  346.6 19.9 %collective-permute-start.29 = (bf16[3,32,2048]{2,1,0:T(8,128)(2,1)}, bf16[3,32,2048]{2,1,0:T(8,128)(2,1)}, u32[]{:S(2)}, u32[]{:S(2)}) collective-permute-start(bf16[3,32,2048]{2,1,0:T(8,128)(2,1)} %lay.1.refs_4_), channel_id=1, source_target_pairs={{0,16},{8,24},{16,0},{24,8},{1,17},{9,25},{17,1},{25,9},{2,18},{10... | collective-permute-start | bytes 1179656 | tf_op jit(solution)/shard_map/ppermute | solution.py:19
  348.8 19.7 %collective-permute-start.30 = (bf16[3,32,2048]{2,1,0:T(8,128)(2,1)}, bf16[3,32,2048]{2,1,0:T(8,128)(2,1)}, u32[]{:S(2)}, u32[]{:S(2)}) collective-permute-start(bf16[3,32,2048]{2,1,0:T(8,128)(2,1)} %lay.1.refs_4_), channel_id=1, source_target_pairs={{0,24},{8,16},{16,8},{24,0},{1,25},{9,17},{17,9},{25,1},{2,26},{10... | collective-permute-start | bytes 1179656 | tf_op jit(solution)/shard_map/ppermute | solution.py:19
  377.9 13.9 %collective-permute-start.33 = (bf16[128,2048]{1,0:T(8,128)(2,1)}, bf16[128,2048]{1,0:T(8,128)(2,1)}, u32[]{:S(2)}, u32[]{:S(2)}) collective-permute-start(bf16[128,2048]{1,0:T(8,128)(2,1)} %get-tuple-element.52), channel_id=1, source_target_pairs={{0,96},{32,64},{64,32},{96,0},{1,97},{33,65},{65,33},{97,1},{2,98}... | collective-permute-start | bytes 1572872 | tf_op jit(solution)/shard_map/ppermute | solution.py:19
  379.1 46.9 %collective-permute-start.32 = (bf16[128,2048]{1,0:T(8,128)(2,1)}, bf16[128,2048]{1,0:T(8,128)(2,1)}, u32[]{:S(2)}, u32[]{:S(2)}) collective-permute-start(bf16[128,2048]{1,0:T(8,128)(2,1)} %get-tuple-element.51), channel_id=1, source_target_pairs={{0,64},{32,96},{64,0},{96,32},{1,65},{33,97},{65,1},{97,33},{2,66}... | collective-permute-start | bytes 1572872 | tf_op jit(solution)/shard_map/ppermute | solution.py:19
  387.5 38.6 %collective-permute-start.31 = (bf16[128,2048]{1,0:T(8,128)(2,1)}, bf16[128,2048]{1,0:T(8,128)(2,1)S(1)}, u32[]{:S(2)}, u32[]{:S(2)}) collective-permute-start(bf16[128,2048]{1,0:T(8,128)(2,1)} %get-tuple-element.47), channel_id=1, source_target_pairs={{0,32},{32,0},{64,96},{96,64},{1,33},{33,1},{65,97},{97,65},{2,34}... | collective-permute-start | bytes 1572872 | tf_op jit(solution)/shard_map/ppermute | solution.py:19
  (43 other events, 462.1 us)

commit v4 on v3

--- a/solution.py
+++ b/solution.py
@@ -428,13 +428,14 @@
     far_back = far_back.reshape(-1, features)
     near_back = near_back.reshape(-1, features)
 
-    third, fourth = combine(far_weights, far_back, far_units, shared_down, (bf16, bf16), 512)
-    third = swapped(third, "zl", n_zl, 2)
-    fourth = swapped(fourth, "zl", n_zl, 3)
+    across, beside = combine(far_weights, far_back, far_units, shared_down, (f32, bf16), 512)
+    beside = swapped(beside, "zl", n_zl, 1)
+    across = (across + beside.astype(f32)).astype(bf16)
+    across = swapped(across, "zl", n_zl, 2)
     kept, second = combine(near_weights, near_back, near_units, shared_down, (f32, bf16), 512)
     second = swapped(second, "zl", n_zl, 1)
     combined = (
-        kept + second.astype(f32) + third.astype(f32) + fourth.astype(f32)
+        kept + second.astype(f32) + across.astype(f32)
     ).astype(bf16)
     return (combined, expert_gate, expert_up, expert_down, *shared_out)
 

time: 430 us -> 417 us (0.970)
  the two profiles are of different devices: /device:TPU:1 before, /device:TPU:8 now
where the time goes in v4:
time: 417 us; the launch traced here: 416 us
  waiting for transfers between devices  214 us (51%)
  starting transfers between devices  122 us (29%)
  Pallas kernels  59.6 us (14%)
  local copies, waits for them, and re-layouts  9.46 us (2%)
  matrix products  6.11 us (1%)
  other arithmetic  4.23 us (1%)
    ppermute x34, waiting for transfers between devices, swapped(): return lax.ppermute(array, axis, [(r, r ^ k) for r in range(size)])  172 us
    ppermute x34, starting transfers between devices, swapped(): return lax.ppermute(array, axis, [(r, r ^ k) for r in range(size)])  84.3 us
    all_to_all x5, waiting for transfers between devices, plane_exchange(): return lax.all_to_all(array, PLANE, split_axis=0, concat_axis=0, tiled=True)  42.3 us
    all_to_all x5, starting transfers between devices, plane_exchange(): return lax.all_to_all(array, PLANE, split_axis=0, concat_axis=0, tiled=True)  37.4 us
    pallas_call x2, Pallas kernels, assemble(): pl.pallas_call(functools.partial(assemble_kernel, compute=compute, blocks...  16.2 us
    pallas_call x2, Pallas kernels, over_rows(): pl.pallas_call(functools.partial(rows_kernel, compute=compute), grid=(cou...  11.8 us
    pallas_call x2, Pallas kernels, combine(): pl.pallas_call(combine_kernel, grid=(features // tile,), in_specs=[whole(...  10.9 us
    pallas_call x2, Pallas kernels, pick(): pl.pallas_call(functools.partial(pick_kernel, span=span, tile=tile), grid...  9.7 us
  transfers between devices with their start and end apart: 39, of which 22 were waited for; matrix products, arithmetic and copies ran while one was open for 2% of the time, Pallas kernels for 11%

profile of v4, /device:TPU:8, one launch (start us, length us, event | category | flops | bytes accessed | tf_op | source)
XLA Modules:
  0.0 416.2 jit_solution(242069510240860316)
XLA Ops:
  1.3 5.1 %cast.1 = bf16[32,288,128]{2,1,0:T(8,128)(2,1)} custom-call(s32[16]{0:T(128)} %stack.73.place, f32[1,128]{1,0:T(1,128)} %bitcast.49, f32[128,24,128]{2,1,0:T(8,128)} %gate.1, f32[128,24,128]{2,1,0:T(8,128)} %up.1, f32[128,24,128]{2,1,0:T(8,128)} %down.1), custom_call_target="tpu_custom_call" | custom-call | flops 1179648 | bytes 7077888 | tf_op jit(solution)/shard_map/cast/pallas_call | solution.py:44
  6.4 7.7 %all-to-all-start = ((bf16[32,288,128]{2,1,0:T(8,128)(2,1)}), bf16[32,288,128]{2,1,0:T(8,128)(2,1)S(1)}, u32[]{:S(2)}, u32[]{:S(2)}) async-start(bf16[32,288,128]{2,1,0:T(8,128)(2,1)} %cast.1), calls=%async_computation | async-start | bytes 4718592 | tf_op jit(solution)/shard_map/all_to_all | solution.py:23
  18.7 11.6 %collective-permute-done.5.two.refs_1_ = bf16[128,2048]{1,0:T(8,128)(2,1)S(1)} collective-permute-done((bf16[128,2048]{1,0:T(8,128)(2,1)S(1)}, bf16[128,2048]{1,0:T(8,128)(2,1)S(1)}, u32[]{:S(2)}, u32[]{:S(2)}) %collective-permute-start.5) | collective-permute-done | bytes 524320 | tf_op jit(solution)/shard_map/ppermute | solution.py:19
  36.0 8.2 %all-to-all-done = bf16[32,288,128]{2,1,0:T(8,128)(2,1)S(1)} async-done(((bf16[32,288,128]{2,1,0:T(8,128)(2,1)}), bf16[32,288,128]{2,1,0:T(8,128)(2,1)S(1)}, u32[]{:S(2)}, u32[]{:S(2)}) %all-to-all-start) | async-done | bytes 2359328 | tf_op jit(solution)/shard_map/all_to_all | solution.py:23
  44.2 7.9 %all-to-all-start.1 = ((bf16[32,24,2048]{2,1,0:T(8,128)(2,1)}), bf16[32,24,2048]{2,1,0:T(8,128)(2,1)}, u32[]{:S(2)}, u32[]{:S(2)}) async-start(bf16[32,24,2048]{2,1,0:T(8,128)(2,1)} %bitcast.41), calls=%async_computation.1 | async-start | bytes 6291456 | tf_op jit(solution)/shard_map/all_to_all | solution.py:23
  59.9 23.1 %collective-permute-done = f32[16,128]{1,0:T(8,128)S(1)} collective-permute-done((f32[16,128]{1,0:T(8,128)S(1)}, f32[16,128]{1,0:T(8,128)S(1)}, u32[]{:S(2)}, u32[]{:S(2)}) %collective-permute-start) | collective-permute-done | bytes 8224 | tf_op jit(solution)/shard_map/ppermute | solution.py:19
  84.0 10.3 %collective-permute-done.2.one.refs_2_ = bf16[128,2048]{1,0:T(8,128)(2,1)S(1)} collective-permute-done((bf16[128,2048]{1,0:T(8,128)(2,1)S(1)}, bf16[128,2048]{1,0:T(8,128)(2,1)S(1)}, u32[]{:S(2)}, u32[]{:S(2)}) %collective-permute-start.2) | collective-permute-done | bytes 524320 | tf_op jit(solution)/shard_map/ppermute | solution.py:19
  99.9 7.5 %all-to-all-start.2 = ((bf16[32,24,2048]{2,1,0:T(8,128)(2,1)}), bf16[32,24,2048]{2,1,0:T(8,128)(2,1)}, u32[]{:S(2)}, u32[]{:S(2)}) async-start(bf16[32,24,2048]{2,1,0:T(8,128)(2,1)} %bitcast.40), calls=%async_computation.2 | async-start | bytes 6291456 | tf_op jit(solution)/shard_map/all_to_all | solution.py:23
  110.3 11.0 %collective-permute-start.6 = (bf16[32,48,128]{2,1,0:T(8,128)(2,1)S(1)}, bf16[32,48,128]{2,1,0:T(8,128)(2,1)S(1)}, u32[]{:S(2)}, u32[]{:S(2)}) collective-permute-start(bf16[32,48,128]{2,1,0:T(8,128)(2,1)S(1)} %get-tuple-element.67), channel_id=1, source_target_pairs={{0,32},{32,0},{64,96},{96,64},{128,160},{160,128},{192,224},{224,1... | collective-permute-start | bytes 1179656 | tf_op jit(solution)/shard_map/ppermute | solution.py:19
  123.0 5.7 %collective-permute-start.10 = (bf16[32,48,128]{2,1,0:T(8,128)(2,1)S(1)}, bf16[32,48,128]{2,1,0:T(8,128)(2,1)S(1)}, u32[]{:S(2)}, u32[]{:S(2)}) collective-permute-start(bf16[32,48,128]{2,1,0:T(8,128)(2,1)S(1)} %get-tuple-element.67), channel_id=1, source_target_pairs={{0,160},{32,128},{64,224},{96,192},{128,32},{160,0},{192,96},{224,... | collective-permute-start | bytes 1179656 | tf_op jit(solution)/shard_map/ppermute | solution.py:19
  130.6 12.8 %collective-permute-done.6.refs_1_ = bf16[32,48,128]{2,1,0:T(8,128)(2,1)S(1)} collective-permute-done((bf16[32,48,128]{2,1,0:T(8,128)(2,1)S(1)}, bf16[32,48,128]{2,1,0:T(8,128)(2,1)S(1)}, u32[]{:S(2)}, u32[]{:S(2)}) %collective-permute-start.6) | collective-permute-done | bytes 393248 | tf_op jit(solution)/shard_map/ppermute | solution.py:19
  143.4 14.8 %collective-permute-done.7.refs_2_ = bf16[32,48,128]{2,1,0:T(8,128)(2,1)S(1)} collective-permute-done((bf16[32,48,128]{2,1,0:T(8,128)(2,1)S(1)}, bf16[32,48,128]{2,1,0:T(8,128)(2,1)S(1)}, u32[]{:S(2)}, u32[]{:S(2)}) %collective-permute-start.7) | collective-permute-done | bytes 393248 | tf_op jit(solution)/shard_map/ppermute | solution.py:19
  160.2 10.2 %collective-permute-done.8.refs_3_ = bf16[32,48,128]{2,1,0:T(8,128)(2,1)S(1)} collective-permute-done((bf16[32,48,128]{2,1,0:T(8,128)(2,1)S(1)}, bf16[32,48,128]{2,1,0:T(8,128)(2,1)S(1)}, u32[]{:S(2)}, u32[]{:S(2)}) %collective-permute-start.8) | collective-permute-done | bytes 393248 | tf_op jit(solution)/shard_map/ppermute | solution.py:19
  170.4 21.1 %collective-permute-start.13 = (bf16[32,24,128]{2,1,0:T(8,128)(2,1)S(1)}, bf16[32,24,128]{2,1,0:T(8,128)(2,1)S(1)}, u32[]{:S(2)}, u32[]{:S(2)}) collective-permute-start(bf16[32,24,128]{2,1,0:T(8,128)(2,1)S(1)} %get-tuple-element.63), channel_id=1, source_target_pairs={{0,32},{32,0},{64,96},{96,64},{128,160},{160,128},{192,224},{224,1... | collective-permute-start | bytes 589832 | tf_op jit(solution)/shard_map/ppermute | solution.py:19
  201.8 9.2 %assemble.2 = (bf16[768,384]{1,0:T(8,128)(2,1)}, bf16[1,384,2048]{2,1,0:T(8,128)(2,1)}, bf16[1,384,2048]{2,1,0:T(8,128)(2,1)}) custom-call(s32[16]{0:T(128)} %stack.73.place, bf16[768,2048]{1,0:T(8,128)(2,1)} %bitcast.12.x, bf16[32,48,128]{2,1,0:T(8,128)(2,1)} %copy-done.9, bf16[32,48,128]{2,1,0:T(8,128)(2,1)} %copy-done.26, ...), custom_call_target="tpu_custom_call" | custom-call | flops 2415919104 | bytes 12582912 | tf_op jit(solution)/shard_map/assemble/pallas_call | solution.py:130
  213.1 5.0 %collective-permute-done.14.refs_2_ = bf16[32,24,128]{2,1,0:T(8,128)(2,1)S(1)} collective-permute-done((bf16[32,24,128]{2,1,0:T(8,128)(2,1)S(1)}, bf16[32,24,128]{2,1,0:T(8,128)(2,1)S(1)}, u32[]{:S(2)}, u32[]{:S(2)}) %collective-permute-start.14) | collective-permute-done | bytes 196640 | tf_op jit(solution)/shard_map/ppermute | solution.py:19
  218.1 5.8 %collective-permute-start.16 = (bf16[32,24,128]{2,1,0:T(8,128)(2,1)S(1)}, bf16[32,24,128]{2,1,0:T(8,128)(2,1)S(1)}, u32[]{:S(2)}, u32[]{:S(2)}) collective-permute-start(bf16[32,24,128]{2,1,0:T(8,128)(2,1)S(1)} %get-tuple-element.64.refs_0_), channel_id=1, source_target_pairs={{0,128},{32,160},{64,192},{96,224},{128,0},{160,32},{192,64},{224,... | collective-permute-start | bytes 589832 | tf_op jit(solution)/shard_map/ppermute | solution.py:19
  223.9 6.7 %over_rows.2.x = bf16[768,384]{1,0:T(8,128)(2,1)} custom-call(bf16[768,2048]{1,0:T(8,128)(2,1)} %bitcast.11.x, bf16[1,384,2048]{2,1,0:T(8,128)(2,1)} %get-tuple-element.24.refs_0_, bf16[1,384,2048]{2,1,0:T(8,128)(2,1)} %get-tuple-element.25.refs_1_), custom_call_target="tpu_custom_call" | custom-call | flops 2415919104 | bytes 6881280 | tf_op jit(solution)/shard_map/over_rows/pallas_call | solution.py:159
  234.3 7.0 %assemble.3 = (bf16[768,2048]{1,0:T(8,128)(2,1)}, bf16[1,384,2048]{2,1,0:T(8,128)(2,1)}) custom-call(s32[16]{0:T(128)} %stack.73.place, bf16[768,384]{1,0:T(8,128)(2,1)} %over_rows.2.x, bf16[32,24,128]{2,1,0:T(8,128)(2,1)} %copy-done.11, bf16[32,24,128]{2,1,0:T(8,128)(2,1)} %copy-done.33, bf16[32,24,128]{2,1,0:T(8,128)(2,1)} %copy-done.35, ...), custom_call_target="tpu_custom_call" | custom-call | flops 1207959552 | bytes 9437184 | tf_op jit(solution)/shard_map/assemble/pallas_call | solution.py:130
  241.3 7.4 %all-to-all-start.4 = ((bf16[32,24,2048]{2,1,0:T(8,128)(2,1)}), bf16[32,24,2048]{2,1,0:T(8,128)(2,1)S(1)}, u32[]{:S(2)}, u32[]{:S(2)}) async-start(bf16[32,24,2048]{2,1,0:T(8,128)(2,1)} %bitcast.45), calls=%async_computation.4 | async-start | bytes 6291456 | tf_op jit(solution)/shard_map/all_to_all | solution.py:23
  248.7 5.1 %over_rows.3 = bf16[768,2048]{1,0:T(8,128)(2,1)} custom-call(bf16[768,384]{1,0:T(8,128)(2,1)} %get-tuple-element.36.x, bf16[1,384,2048]{2,1,0:T(8,128)(2,1)} %get-tuple-element.26.refs_0_), custom_call_target="tpu_custom_call" | custom-call | flops 1207959552 | bytes 5308416 | tf_op jit(solution)/shard_map/over_rows/pallas_call | solution.py:159
  253.8 34.0 %all-to-all-done.4 = bf16[32,24,2048]{2,1,0:T(8,128)(2,1)S(1)} async-done(((bf16[32,24,2048]{2,1,0:T(8,128)(2,1)}), bf16[32,24,2048]{2,1,0:T(8,128)(2,1)S(1)}, u32[]{:S(2)}, u32[]{:S(2)}) %all-to-all-start.4) | async-done | bytes 3145760 | tf_op jit(solution)/shard_map/all_to_all | solution.py:23
  289.5 6.9 %all-to-all-start.3 = ((bf16[32,24,2048]{2,1,0:T(8,128)(2,1)}), bf16[32,24,2048]{2,1,0:T(8,128)(2,1)S(1)}, u32[]{:S(2)}, u32[]{:S(2)}) async-start(bf16[32,24,2048]{2,1,0:T(8,128)(2,1)} %bitcast.42), calls=%async_computation.3 | async-start | bytes 6291456 | tf_op jit(solution)/shard_map/all_to_all | solution.py:23
  296.5 5.1 %collective-permute-start.20 = (bf16[3,32,128]{2,1,0:T(8,128)(2,1)S(1)}, bf16[3,32,128]{2,1,0:T(8,128)(2,1)S(1)}, u32[]{:S(2)}, u32[]{:S(2)}) collective-permute-start(bf16[3,32,128]{2,1,0:T(8,128)(2,1)S(1)} %pad_maximum_fusion.2), channel_id=1, source_target_pairs={{0,128},{128,0},{1,129},{129,1},{2,130},{130,2},{3,131},{131,3},{4... | collective-permute-start | bytes 73736 | tf_op jit(solution)/shard_map/ppermute | solution.py:19
  312.3 23.4 %collective-permute-done.22.refs_2_ = bf16[2,3,32,128]{3,2,1,0:T(8,128)(2,1)S(1)} collective-permute-done((bf16[2,3,32,128]{3,2,1,0:T(8,128)(2,1)S(1)}, bf16[2,3,32,128]{3,2,1,0:T(8,128)(2,1)S(1)}, u32[]{:S(2)}, u32[]{:S(2)}) %collective-permute-start.22) | collective-permute-done | bytes 49184 | tf_op jit(solution)/shard_map/ppermute | solution.py:19
  347.7 8.7 %collective-permute-done.28.refs_5_ = bf16[3,32,2048]{2,1,0:T(8,128)(2,1)S(1)} collective-permute-done((bf16[3,32,2048]{2,1,0:T(8,128)(2,1)}, bf16[3,32,2048]{2,1,0:T(8,128)(2,1)S(1)}, u32[]{:S(2)}, u32[]{:S(2)}) %collective-permute-start.28) | collective-permute-done | bytes 393248 | tf_op jit(solution)/shard_map/ppermute | solution.py:19
  356.4 8.2 %collective-permute-done.29.refs_6_ = bf16[3,32,2048]{2,1,0:T(8,128)(2,1)} collective-permute-done((bf16[3,32,2048]{2,1,0:T(8,128)(2,1)}, bf16[3,32,2048]{2,1,0:T(8,128)(2,1)}, u32[]{:S(2)}, u32[]{:S(2)}) %collective-permute-start.29) | collective-permute-done | bytes 393248 | tf_op jit(solution)/shard_map/ppermute | solution.py:19
  370.0 5.4 %combine.3 = (f32[128,2048]{1,0:T(8,128)}, bf16[128,2048]{1,0:T(8,128)(2,1)}) custom-call(bf16[256,768]{1,0:T(8,128)(2,1)} %fusion.2.high, bf16[256,768]{1,0:T(8,128)(2,1)} %fusion.3.low, bf16[768,2048]{1,0:T(8,128)(2,1)} %bitcast.44, bf16[256,128]{1,0:T(8,128)(2,1)} %get-tuple-element.50.hidden, bf16[128,2048]{1,0:T(8,128)(2,1)} %get-tuple-element.45.down), custom_call_target="tpu_custom_call" | custom-call | flops 1744830464 | bytes 6029312 | tf_op jit(solution)/shard_map/combine/pallas_call | solution.py:318
  378.7 5.4 %combine.2 = (f32[128,2048]{1,0:T(8,128)}, bf16[128,2048]{1,0:T(8,128)(2,1)}) custom-call(bf16[256,768]{1,0:T(8,128)(2,1)} %fusion.high, bf16[256,768]{1,0:T(8,128)(2,1)} %fusion.1.low, bf16[768,2048]{1,0:T(8,128)(2,1)} %bitcast.43, bf16[256,128]{1,0:T(8,128)(2,1)} %get-tuple-element.44.hidden, bf16[128,2048]{1,0:T(8,128)(2,1)} %get-tuple-element.45.down), custom_call_target="tpu_custom_call" | custom-call | flops 1744830464 | bytes 6029312 | tf_op jit(solution)/shard_map/combine/pallas_call | solution.py:318
  384.6 11.1 %collective-permute-done.32 = bf16[128,2048]{1,0:T(8,128)(2,1)} collective-permute-done((bf16[128,2048]{1,0:T(8,128)(2,1)}, bf16[128,2048]{1,0:T(8,128)(2,1)}, u32[]{:S(2)}, u32[]{:S(2)}) %collective-permute-start.32) | collective-permute-done | bytes 524320 | tf_op jit(solution)/shard_map/ppermute | solution.py:19
  398.1 6.2 %collective-permute-done.31 = bf16[128,2048]{1,0:T(8,128)(2,1)S(1)} collective-permute-done((bf16[128,2048]{1,0:T(8,128)(2,1)}, bf16[128,2048]{1,0:T(8,128)(2,1)S(1)}, u32[]{:S(2)}, u32[]{:S(2)}) %collective-permute-start.31) | collective-permute-done | bytes 524320 | tf_op jit(solution)/shard_map/ppermute | solution.py:19
  404.3 10.9 %collective-permute-done.33 = bf16[128,2048]{1,0:T(8,128)(2,1)S(1)} collective-permute-done((bf16[128,2048]{1,0:T(8,128)(2,1)S(1)}, bf16[128,2048]{1,0:T(8,128)(2,1)S(1)}, u32[]{:S(2)}, u32[]{:S(2)}) %collective-permute-start.33) | collective-permute-done | bytes 524320 | tf_op jit(solution)/shard_map/ppermute | solution.py:19
  (173 shorter events, 86.6 us)
Async XLA Ops:
  6.4 37.8 %all-to-all-start = ((bf16[32,288,128]{2,1,0:T(8,128)(2,1)}), bf16[32,288,128]{2,1,0:T(8,128)(2,1)S(1)}, u32[]{:S(2)}, u32[]{:S(2)}) async-start(bf16[32,288,128]{2,1,0:T(8,128)(2,1)} %cast.1), calls=%async_computation | async-start | bytes 4718592 | tf_op jit(solution)/shard_map/all_to_all | solution.py:23
  44.2 55.7 %all-to-all-start.1 = ((bf16[32,24,2048]{2,1,0:T(8,128)(2,1)}), bf16[32,24,2048]{2,1,0:T(8,128)(2,1)}, u32[]{:S(2)}, u32[]{:S(2)}) async-start(bf16[32,24,2048]{2,1,0:T(8,128)(2,1)} %bitcast.41), calls=%async_computation.1 | async-start | bytes 6291456 | tf_op jit(solution)/shard_map/all_to_all | solution.py:23
  56.8 26.2 %collective-permute-start = (f32[16,128]{1,0:T(8,128)S(1)}, f32[16,128]{1,0:T(8,128)S(1)}, u32[]{:S(2)}, u32[]{:S(2)}) collective-permute-start(f32[16,128]{1,0:T(8,128)S(1)} %pad_maximum_fusion.5), channel_id=1, source_target_pairs={{0,64},{32,96},{64,0},{96,32},{1,65},{33,97},{65,1},{97,33},{2,66}... | collective-permute-start | bytes 24584 | tf_op jit(solution)/shard_map/ppermute | solution.py:19
  56.8 37.4 %collective-permute-start.2 = (bf16[128,2048]{1,0:T(8,128)(2,1)S(1)}, bf16[128,2048]{1,0:T(8,128)(2,1)S(1)}, u32[]{:S(2)}, u32[]{:S(2)}) collective-permute-start(bf16[128,2048]{1,0:T(8,128)(2,1)S(1)} %copy-done.1), channel_id=1, source_target_pairs={{0,64},{32,96},{64,0},{96,32},{1,65},{33,97},{65,1},{97,33},{2,66}... | collective-permute-start | bytes 1572872 | tf_op jit(solution)/shard_map/ppermute | solution.py:19
  59.8 34.5 %collective-permute-start.3 = (bf16[128,2048]{1,0:T(8,128)(2,1)S(1)}, bf16[128,2048]{1,0:T(8,128)(2,1)}, u32[]{:S(2)}, u32[]{:S(2)}) collective-permute-start(bf16[128,2048]{1,0:T(8,128)(2,1)S(1)} %copy-done.1), channel_id=1, source_target_pairs={{0,96},{32,64},{64,32},{96,0},{1,97},{33,65},{65,33},{97,1},{2,98}... | collective-permute-start | bytes 1572872 | tf_op jit(solution)/shard_map/ppermute | solution.py:19
  99.9 124.0 %all-to-all-start.2 = ((bf16[32,24,2048]{2,1,0:T(8,128)(2,1)}), bf16[32,24,2048]{2,1,0:T(8,128)(2,1)}, u32[]{:S(2)}, u32[]{:S(2)}) async-start(bf16[32,24,2048]{2,1,0:T(8,128)(2,1)} %bitcast.40), calls=%async_computation.2 | async-start | bytes 6291456 | tf_op jit(solution)/shard_map/all_to_all | solution.py:23
  110.3 33.0 %collective-permute-start.6 = (bf16[32,48,128]{2,1,0:T(8,128)(2,1)S(1)}, bf16[32,48,128]{2,1,0:T(8,128)(2,1)S(1)}, u32[]{:S(2)}, u32[]{:S(2)}) collective-permute-start(bf16[32,48,128]{2,1,0:T(8,128)(2,1)S(1)} %get-tuple-element.67), channel_id=1, source_target_pairs={{0,32},{32,0},{64,96},{96,64},{128,160},{160,128},{192,224},{224,1... | collective-permute-start | bytes 1179656 | tf_op jit(solution)/shard_map/ppermute | solution.py:19
  121.3 36.9 %collective-permute-start.7 = (bf16[32,48,128]{2,1,0:T(8,128)(2,1)S(1)}, bf16[32,48,128]{2,1,0:T(8,128)(2,1)S(1)}, u32[]{:S(2)}, u32[]{:S(2)}) collective-permute-start(bf16[32,48,128]{2,1,0:T(8,128)(2,1)S(1)} %get-tuple-element.66), channel_id=1, source_target_pairs={{0,64},{32,96},{64,0},{96,32},{128,192},{160,224},{192,128},{224,1... | collective-permute-start | bytes 1179656 | tf_op jit(solution)/shard_map/ppermute | solution.py:19
  123.0 73.1 %collective-permute-start.10 = (bf16[32,48,128]{2,1,0:T(8,128)(2,1)S(1)}, bf16[32,48,128]{2,1,0:T(8,128)(2,1)S(1)}, u32[]{:S(2)}, u32[]{:S(2)}) collective-permute-start(bf16[32,48,128]{2,1,0:T(8,128)(2,1)S(1)} %get-tuple-element.67), channel_id=1, source_target_pairs={{0,160},{32,128},{64,224},{96,192},{128,32},{160,0},{192,96},{224,... | collective-permute-start | bytes 1179656 | tf_op jit(solution)/shard_map/ppermute | solution.py:19
  128.7 69.8 %collective-permute-start.11 = (bf16[32,48,128]{2,1,0:T(8,128)(2,1)S(1)}, bf16[32,48,128]{2,1,0:T(8,128)(2,1)S(1)}, u32[]{:S(2)}, u32[]{:S(2)}) collective-permute-start(bf16[32,48,128]{2,1,0:T(8,128)(2,1)S(1)} %get-tuple-element.66), channel_id=1, source_target_pairs={{0,192},{32,224},{64,128},{96,160},{128,64},{160,96},{192,0},{224,... | collective-permute-start | bytes 1179656 | tf_op jit(solution)/shard_map/ppermute | solution.py:19
  128.7 41.7 %collective-permute-start.8 = (bf16[32,48,128]{2,1,0:T(8,128)(2,1)S(1)}, bf16[32,48,128]{2,1,0:T(8,128)(2,1)S(1)}, u32[]{:S(2)}, u32[]{:S(2)}) collective-permute-start(bf16[32,48,128]{2,1,0:T(8,128)(2,1)S(1)} %get-tuple-element.65), channel_id=1, source_target_pairs={{0,96},{32,64},{64,32},{96,0},{128,224},{160,192},{192,160},{224,1... | collective-permute-start | bytes 1179656 | tf_op jit(solution)/shard_map/ppermute | solution.py:19
  143.4 56.4 %collective-permute-start.12 = (bf16[32,48,128]{2,1,0:T(8,128)(2,1)S(1)}, bf16[32,48,128]{2,1,0:T(8,128)(2,1)S(1)}, u32[]{:S(2)}, u32[]{:S(2)}) collective-permute-start(bf16[32,48,128]{2,1,0:T(8,128)(2,1)S(1)} %get-tuple-element.65), channel_id=1, source_target_pairs={{0,224},{32,192},{64,160},{96,128},{128,96},{160,64},{192,32},{224... | collective-permute-start | bytes 1179656 | tf_op jit(solution)/shard_map/ppermute | solution.py:19
  158.2 36.9 %collective-permute-start.9 = (bf16[32,48,128]{2,1,0:T(8,128)(2,1)S(1)}, bf16[32,48,128]{2,1,0:T(8,128)(2,1)S(1)}, u32[]{:S(2)}, u32[]{:S(2)}) collective-permute-start(bf16[32,48,128]{2,1,0:T(8,128)(2,1)S(1)} %get-tuple-element.68.refs_0_), channel_id=1, source_target_pairs={{0,128},{32,160},{64,192},{96,224},{128,0},{160,32},{192,64},{224,... | collective-permute-start | bytes 1179656 | tf_op jit(solution)/shard_map/ppermute | solution.py:19
  170.4 40.6 %collective-permute-start.13 = (bf16[32,24,128]{2,1,0:T(8,128)(2,1)S(1)}, bf16[32,24,128]{2,1,0:T(8,128)(2,1)S(1)}, u32[]{:S(2)}, u32[]{:S(2)}) collective-permute-start(bf16[32,24,128]{2,1,0:T(8,128)(2,1)S(1)} %get-tuple-element.63), channel_id=1, source_target_pairs={{0,32},{32,0},{64,96},{96,64},{128,160},{160,128},{192,224},{224,1... | collective-permute-start | bytes 589832 | tf_op jit(solution)/shard_map/ppermute | solution.py:19
  195.1 37.7 %collective-permute-start.17 = (bf16[32,24,128]{2,1,0:T(8,128)(2,1)S(1)}, bf16[32,24,128]{2,1,0:T(8,128)(2,1)S(1)}, u32[]{:S(2)}, u32[]{:S(2)}) collective-permute-start(bf16[32,24,128]{2,1,0:T(8,128)(2,1)S(1)} %get-tuple-element.63), channel_id=1, source_target_pairs={{0,160},{32,128},{64,224},{96,192},{128,32},{160,0},{192,96},{224,... | collective-permute-start | bytes 589832 | tf_op jit(solution)/shard_map/ppermute | solution.py:19
  196.1 22.0 %collective-permute-start.14 = (bf16[32,24,128]{2,1,0:T(8,128)(2,1)S(1)}, bf16[32,24,128]{2,1,0:T(8,128)(2,1)S(1)}, u32[]{:S(2)}, u32[]{:S(2)}) collective-permute-start(bf16[32,24,128]{2,1,0:T(8,128)(2,1)S(1)} %get-tuple-element.62), channel_id=1, source_target_pairs={{0,64},{32,96},{64,0},{96,32},{128,192},{160,224},{192,128},{224,1... | collective-permute-start | bytes 589832 | tf_op jit(solution)/shard_map/ppermute | solution.py:19
  198.5 34.2 %collective-permute-start.18 = (bf16[32,24,128]{2,1,0:T(8,128)(2,1)S(1)}, bf16[32,24,128]{2,1,0:T(8,128)(2,1)S(1)}, u32[]{:S(2)}, u32[]{:S(2)}) collective-permute-start(bf16[32,24,128]{2,1,0:T(8,128)(2,1)S(1)} %get-tuple-element.62), channel_id=1, source_target_pairs={{0,192},{32,224},{64,128},{96,160},{128,64},{160,96},{192,0},{224,... | collective-permute-start | bytes 589832 | tf_op jit(solution)/shard_map/ppermute | solution.py:19
  199.8 30.9 %collective-permute-start.15 = (bf16[32,24,128]{2,1,0:T(8,128)(2,1)S(1)}, bf16[32,24,128]{2,1,0:T(8,128)(2,1)S(1)}, u32[]{:S(2)}, u32[]{:S(2)}) collective-permute-start(bf16[32,24,128]{2,1,0:T(8,128)(2,1)S(1)} %get-tuple-element.61), channel_id=1, source_target_pairs={{0,96},{32,64},{64,32},{96,0},{128,224},{160,192},{192,160},{224,1... | collective-permute-start | bytes 589832 | tf_op jit(solution)/shard_map/ppermute | solution.py:19
  211.0 21.7 %collective-permute-start.19 = (bf16[32,24,128]{2,1,0:T(8,128)(2,1)S(1)}, bf16[32,24,128]{2,1,0:T(8,128)(2,1)S(1)}, u32[]{:S(2)}, u32[]{:S(2)}) collective-permute-start(bf16[32,24,128]{2,1,0:T(8,128)(2,1)S(1)} %get-tuple-element.61), channel_id=1, source_target_pairs={{0,224},{32,192},{64,160},{96,128},{128,96},{160,64},{192,32},{224... | collective-permute-start | bytes 589832 | tf_op jit(solution)/shard_map/ppermute | solution.py:19
  218.1 14.6 %collective-permute-start.16 = (bf16[32,24,128]{2,1,0:T(8,128)(2,1)S(1)}, bf16[32,24,128]{2,1,0:T(8,128)(2,1)S(1)}, u32[]{:S(2)}, u32[]{:S(2)}) collective-permute-start(bf16[32,24,128]{2,1,0:T(8,128)(2,1)S(1)} %get-tuple-element.64.refs_0_), channel_id=1, source_target_pairs={{0,128},{32,160},{64,192},{96,224},{128,0},{160,32},{192,64},{224,... | collective-permute-start | bytes 589832 | tf_op jit(solution)/shard_map/ppermute | solution.py:19
  241.3 46.6 %all-to-all-start.4 = ((bf16[32,24,2048]{2,1,0:T(8,128)(2,1)}), bf16[32,24,2048]{2,1,0:T(8,128)(2,1)S(1)}, u32[]{:S(2)}, u32[]{:S(2)}) async-start(bf16[32,24,2048]{2,1,0:T(8,128)(2,1)} %bitcast.45), calls=%async_computation.4 | async-start | bytes 6291456 | tf_op jit(solution)/shard_map/all_to_all | solution.py:23
  289.5 87.5 %all-to-all-start.3 = ((bf16[32,24,2048]{2,1,0:T(8,128)(2,1)}), bf16[32,24,2048]{2,1,0:T(8,128)(2,1)S(1)}, u32[]{:S(2)}, u32[]{:S(2)}) async-start(bf16[32,24,2048]{2,1,0:T(8,128)(2,1)} %bitcast.42), calls=%async_computation.3 | async-start | bytes 6291456 | tf_op jit(solution)/shard_map/all_to_all | solution.py:23
  304.5 31.2 %collective-permute-start.22 = (bf16[2,3,32,128]{3,2,1,0:T(8,128)(2,1)S(1)}, bf16[2,3,32,128]{3,2,1,0:T(8,128)(2,1)S(1)}, u32[]{:S(2)}, u32[]{:S(2)}) collective-permute-start(bf16[2,3,32,128]{3,2,1,0:T(8,128)(2,1)S(1)} %maximum_select_fusion.refs_0_), channel_id=1, source_target_pairs={{0,2},{1,3},{2,0},{3,1},{4,6},{5,7},{6,4},{7,5},{8,10},{9,11},{10,... | collective-permute-start | bytes 147464 | tf_op jit(solution)/shard_map/ppermute | solution.py:19
  306.0 31.0 %collective-permute-start.23 = (bf16[2,3,32,128]{3,2,1,0:T(8,128)(2,1)S(1)}, bf16[2,3,32,128]{3,2,1,0:T(8,128)(2,1)S(1)}, u32[]{:S(2)}, u32[]{:S(2)}) collective-permute-start(bf16[2,3,32,128]{3,2,1,0:T(8,128)(2,1)S(1)} %maximum_select_fusion.refs_0_), channel_id=1, source_target_pairs={{0,3},{1,2},{2,1},{3,0},{4,7},{5,6},{6,5},{7,4},{8,11},{9,10},{10,... | collective-permute-start | bytes 147464 | tf_op jit(solution)/shard_map/ppermute | solution.py:19
  306.3 33.9 %collective-permute-start.24 = (bf16[2,3,32,128]{3,2,1,0:T(8,128)(2,1)S(1)}, bf16[2,3,32,128]{3,2,1,0:T(8,128)(2,1)S(1)}, u32[]{:S(2)}, u32[]{:S(2)}) collective-permute-start(bf16[2,3,32,128]{3,2,1,0:T(8,128)(2,1)S(1)} %maximum_select_fusion.refs_0_), channel_id=1, source_target_pairs={{0,4},{1,5},{2,6},{3,7},{4,0},{5,1},{6,2},{7,3},{8,12},{9,13},{10,... | collective-permute-start | bytes 147464 | tf_op jit(solution)/shard_map/ppermute | solution.py:19
  309.3 30.9 %collective-permute-start.25 = (bf16[2,3,32,128]{3,2,1,0:T(8,128)(2,1)S(1)}, bf16[2,3,32,128]{3,2,1,0:T(8,128)(2,1)S(1)}, u32[]{:S(2)}, u32[]{:S(2)}) collective-permute-start(bf16[2,3,32,128]{3,2,1,0:T(8,128)(2,1)S(1)} %maximum_select_fusion.refs_0_), channel_id=1, source_target_pairs={{0,5},{1,4},{2,7},{3,6},{4,1},{5,0},{6,3},{7,2},{8,13},{9,12},{10,... | collective-permute-start | bytes 147464 | tf_op jit(solution)/shard_map/ppermute | solution.py:19
  309.5 30.7 %collective-permute-start.26 = (bf16[2,3,32,128]{3,2,1,0:T(8,128)(2,1)S(1)}, bf16[2,3,32,128]{3,2,1,0:T(8,128)(2,1)S(1)}, u32[]{:S(2)}, u32[]{:S(2)}) collective-permute-start(bf16[2,3,32,128]{3,2,1,0:T(8,128)(2,1)S(1)} %maximum_select_fusion.refs_0_), channel_id=1, source_target_pairs={{0,6},{1,7},{2,4},{3,5},{4,2},{5,3},{6,0},{7,1},{8,14},{9,15},{10,... | collective-permute-start | bytes 147464 | tf_op jit(solution)/shard_map/ppermute | solution.py:19
  344.3 20.2 %collective-permute-start.29 = (bf16[3,32,2048]{2,1,0:T(8,128)(2,1)}, bf16[3,32,2048]{2,1,0:T(8,128)(2,1)}, u32[]{:S(2)}, u32[]{:S(2)}) collective-permute-start(bf16[3,32,2048]{2,1,0:T(8,128)(2,1)} %lay.1.refs_4_), channel_id=1, source_target_pairs={{0,16},{8,24},{16,0},{24,8},{1,17},{9,25},{17,1},{25,9},{2,18},{10... | collective-permute-start | bytes 1179656 | tf_op jit(solution)/shard_map/ppermute | solution.py:19
  346.6 19.3 %collective-permute-start.30 = (bf16[3,32,2048]{2,1,0:T(8,128)(2,1)}, bf16[3,32,2048]{2,1,0:T(8,128)(2,1)}, u32[]{:S(2)}, u32[]{:S(2)}) collective-permute-start(bf16[3,32,2048]{2,1,0:T(8,128)(2,1)} %lay.1.refs_4_), channel_id=1, source_target_pairs={{0,24},{8,16},{16,8},{24,0},{1,25},{9,17},{17,9},{25,1},{2,26},{10... | collective-permute-start | bytes 1179656 | tf_op jit(solution)/shard_map/ppermute | solution.py:19
  375.4 20.3 %collective-permute-start.32 = (bf16[128,2048]{1,0:T(8,128)(2,1)}, bf16[128,2048]{1,0:T(8,128)(2,1)}, u32[]{:S(2)}, u32[]{:S(2)}) collective-permute-start(bf16[128,2048]{1,0:T(8,128)(2,1)} %get-tuple-element.52), channel_id=1, source_target_pairs={{0,32},{32,0},{64,96},{96,64},{1,33},{33,1},{65,97},{97,65},{2,34}... | collective-permute-start | bytes 1572872 | tf_op jit(solution)/shard_map/ppermute | solution.py:19
  384.2 20.1 %collective-permute-start.31 = (bf16[128,2048]{1,0:T(8,128)(2,1)}, bf16[128,2048]{1,0:T(8,128)(2,1)S(1)}, u32[]{:S(2)}, u32[]{:S(2)}) collective-permute-start(bf16[128,2048]{1,0:T(8,128)(2,1)} %get-tuple-element.47), channel_id=1, source_target_pairs={{0,32},{32,0},{64,96},{96,64},{1,33},{33,1},{65,97},{97,65},{2,34}... | collective-permute-start | bytes 1572872 | tf_op jit(solution)/shard_map/ppermute | solution.py:19
  397.2 18.0 %collective-permute-start.33 = (bf16[128,2048]{1,0:T(8,128)(2,1)S(1)}, bf16[128,2048]{1,0:T(8,128)(2,1)S(1)}, u32[]{:S(2)}, u32[]{:S(2)}) collective-permute-start(bf16[128,2048]{1,0:T(8,128)(2,1)S(1)} %add_convert_fusion.1), channel_id=1, source_target_pairs={{0,64},{32,96},{64,0},{96,32},{1,65},{33,97},{65,1},{97,33},{2,66}... | collective-permute-start | bytes 1572872 | tf_op jit(solution)/shard_map/ppermute | solution.py:19
  (47 other events, 533.8 us)
